TPU v7x, 256 devices: a whole 4x4x8 slice. The times are simulated.
256 devices in a mesh: fs: 32 (over z, y), tp: 8 (over x, core).
Axes of the slice: x: 4, y: 4, z: 8, core: 2. Of those that a mesh axis runs over, the one named last changes fastest.
Arguments:
- inputs: bfloat16 [8192, 2048], P('fs', 'tp'), may hold values from -6 to 6
- cotangent: bfloat16 [8192, 2048], P('fs', 'tp'), may hold values from -8 to 8
- gate_weight: bfloat16 [2048, 5632], P('fs', 'tp'), may hold values from -0.125 to 0.125
- up_weight: bfloat16 [2048, 5632], P('fs', 'tp'), may hold values from -0.125 to 0.125
- down_weight: bfloat16 [5632, 2048], P('tp', 'fs'), may hold values from -0.078125 to 0.078125
Outputs:
- grad_inputs: bfloat16 [8192, 2048], P('fs', 'tp')
- grad_gate: float32 [2048, 5632], P('fs', 'tp')
- grad_up: float32 [2048, 5632], P('fs', 'tp')
- grad_down: float32 [5632, 2048], P('tp', 'fs')
All inputs are finite; a program needn't handle non-finite values.
Results may differ from a plain program's by a relative error of at most 0.015.
Values may be sent and summed in bfloat16 or wider, within the bound.
No kernel may reach another device: no remote copies, remote signals or barrier semaphores. Data moves between devices by JAX's collectives and lax.ppermute only.
A program may use at most 64 MiB of HBM per device.

v0:
```python
import jax
import jax.numpy as jnp
from jax import lax
from jax.sharding import Mesh
from jax.sharding import PartitionSpec as P

FS = ("fs_0", "fs_1")


def in_one_piece(arrays, axis, dim, along):
    ends, at = ([], 0)
    for a in arrays[:-1]:
        at += a.shape[along]
        ends.append(at)
    both = jnp.concatenate(arrays, axis=along)
    return tuple(jnp.split(lax.all_gather(both, axis, axis=dim, tiled=True), ends, axis=along))


def gather_axes(array, axes, dim):
    result = array
    for number in range(len(axes) - 1, -1, -1):
        result = lax.all_gather(result, axes[number], axis=dim, tiled=True)
    return result


def cut_along(array, dim, size):
    before, after = (array.shape[:dim], array.shape[dim + 1 :])
    return jnp.moveaxis(array.reshape(*before, size, -1, *after), dim, 0)


def sent_and_summed(array, axis, dim):
    parts = cut_along(array, dim, lax.axis_size(axis))
    arrived = lax.all_to_all(parts, axis, split_axis=0, concat_axis=0, tiled=True)
    return arrived.astype(jnp.float32).sum(axis=0)


def summed_rows(terms, axes):
    subtotal = terms.astype(jnp.bfloat16)
    for axis in axes:
        subtotal = lax.psum_scatter(subtotal, axis, scatter_dimension=0, tiled=True)
    return subtotal.astype(jnp.float32)


def contract_rows(left, right):
    return lax.dot_general(
        left, right, (((0,), (0,)), ((), ())), preferred_element_type=jnp.float32
    )


def contract_cols(left, right):
    return lax.dot_general(
        left, right, (((1,), (1,)), ((), ())), preferred_element_type=jnp.float32
    )


def per_device(inputs, cotangent, gate_weight, up_weight, down_weight):
    whole_inputs, whole_cotangent = in_one_piece((inputs, cotangent), "tp", 1, 0)
    gate_whole, up_whole = in_one_piece((gate_weight, up_weight), FS, 0, 1)
    gate_pre = jnp.dot(whole_inputs, gate_whole, preferred_element_type=jnp.float32)
    up_pre = jnp.dot(whole_inputs, up_whole, preferred_element_type=jnp.float32)
    gate_sig = jax.nn.sigmoid(gate_pre)
    gate_act = gate_pre * gate_sig
    hidden = (gate_act * up_pre).astype(jnp.bfloat16)
    grad_hidden = contract_cols(whole_cotangent, gather_axes(down_weight, FS, 1))
    grad_gate_pre = (grad_hidden * up_pre * gate_sig * (1.0 + gate_pre * (1.0 - gate_sig))).astype(
        jnp.bfloat16
    )
    grad_up_pre = (grad_hidden * gate_act).astype(jnp.bfloat16)
    pre_grads = jnp.concatenate([grad_gate_pre, grad_up_pre], axis=1)
    width = gate_weight.shape[1]
    partial_sum = contract_cols(grad_gate_pre, gate_whole) + contract_cols(grad_up_pre, up_whole)
    grad_inputs = sent_and_summed(partial_sum.astype(jnp.bfloat16), "tp", 1).astype(jnp.bfloat16)
    expand = summed_rows(contract_rows(whole_inputs, pre_grads), FS)
    down = sent_and_summed(contract_rows(whole_cotangent, hidden).astype(jnp.bfloat16), FS, 0)
    grad_gate = expand[:, :width]
    grad_up = expand[:, width:]
    grad_down = down.T
    return (grad_inputs, grad_gate, grad_up, grad_down)


def solution(mesh):
    finer = Mesh(mesh.devices.reshape(8, 4, mesh.shape["tp"]), ("fs_0", "fs_1", "tp"))
    placed = (P(FS, "tp"), P(FS, "tp"), P(FS, "tp"), P(FS, "tp"), P("tp", FS))
    return jax.shard_map(
        per_device,
        mesh=finer,
        in_specs=placed,
        out_specs=(P(FS, "tp"), P(FS, "tp"), P(FS, "tp"), P("tp", FS)),
        check_vma=False,
    )
```

profile of v0, /device:TPU:2, one launch (start us, length us, event | category | flops | bytes accessed | tf_op | source)
XLA Modules:
  0.0 354.6 jit_solution(18237689862459750541)
XLA Ops:
  7.2 0.0 all-gather.4.cloned.1.call-start
  7.2 1.7 pad_maximum_fusion
  8.9 0.0 all-gather.4.cloned.1.call-update
  8.9 0.0 all-gather.8.cloned.1.call-start
  9.0 1.7 pad_maximum_fusion.1
  10.7 0.0 all-gather.8.cloned.1.call-update
  10.7 0.0 all-gather.6.cloned.1.call-start
  10.8 14.8 %all_gather.13 = bf16[704,256]{0,1:T(8,128)(2,1)} all-gather(bf16[704,64]{0,1:T(8,128)(2,1)} %param.9), channel_id=1, replica_groups=mesh['fs_0'=8,'fs_1'=4,'tp'=8] {'fs_1'}, dimensions={1}, use_global_device_ids=true | all-gather | bytes 450560 | tf_op jit(solution)/shard_map/all_gather | solution.py:22
  25.5 0.0 all-gather.6.cloned.1.call-update
  25.6 0.0 reduce-scatter.3.cloned.1.call-start
  25.6 16.0 %all-gather.4.cloned.1.call-done = bf16[512,2048]{1,0:T(8,128)(2,1)} async-done(((bf16[512,256]{1,0:T(8,128)(2,1)}), bf16[512,2048]{1,0:T(8,128)(2,1)}) %all-gather.4.cloned.1.call-update) | async-done | bytes 2097168 | tf_op jit(solution)/shard_map/all_gather | solution.py:16
  41.6 91.2 %all-gather.8.cloned.1.call-done = bf16[2048,1408]{1,0:T(8,128)(2,1)} async-done(((bf16[64,1408]{1,0:T(8,128)(2,1)}), bf16[2048,1408]{1,0:T(8,128)(2,1)}) %all-gather.8.cloned.1.call-update) | async-done | bytes 5767184 | tf_op jit(solution)/shard_map/all_gather | solution.py:16
  132.8 0.0 copy-start.1
  132.8 3.7 %fusion.2 = f32[256,704]{0,1:T(8,128)S(1)} fusion(bf16[2048,1408]{1,0:T(8,128)(2,1)} %all-gather.8.cloned.1.call-done, bf16[512,2048]{1,0:T(8,128)(2,1)} %all-gather.4.cloned.1.call-done), kind=kOutput, calls=%fused_computation.5 | convolution fusion | flops 738197504 | bytes 4915200 | tf_op jit(solution)/shard_map/dot_general | solution.py:59
  136.5 0.2 copy-done.1
  136.7 0.0 copy-start.3
  136.7 0.0 copy-start.2
  136.7 5.1 %fusion.6 = f32[256,704]{0,1:T(8,128)} fusion(bf16[2048,1408]{1,0:T(8,128)(2,1)S(1)} %copy-done.1, bf16[512,2048]{1,0:T(8,128)(2,1)} %all-gather.4.cloned.1.call-done), kind=kOutput, calls=%fused_computation.9 | convolution fusion | flops 738197504 | bytes 4915200 | tf_op jit(solution)/shard_map/dot_general | solution.py:60
  141.9 34.5 %all-gather.6.cloned.1.call-done = bf16[704,2048]{0,1:T(8,128)(2,1)} async-done(((bf16[704,256]{0,1:T(8,128)(2,1)}), bf16[704,2048]{0,1:T(8,128)(2,1)}) %all-gather.6.cloned.1.call-update) | async-done | bytes 2883600 | tf_op jit(solution)/shard_map/all_gather | solution.py:22
  176.4 0.0 copy-done.3
  176.4 0.0 copy-done.2
  176.4 3.5 multiply_convert_fusion.1
  179.9 4.4 %convolution_convert_fusion = bf16[2048,1408]{1,0:T(8,128)(2,1)} fusion(bf16[512,2048]{1,0:T(8,128)(2,1)S(1)} %copy-done.2, bf16[256,704]{0,1:T(8,128)(2,1)S(1)} %get-tuple-element.4, bf16[256,704]{0,1:T(8,128)(2,1)S(1)} %get-tuple-element.5), kind=kOutput, calls=%fused_computation | convolution fusion | flops 1480720384 | bytes 7536640 | tf_op jit(solution)/shard_map/dot_general | solution.py:45
  184.2 0.0 reduce-scatter.3.cloned.1.call-update
  184.3 2.9 fusion
  187.2 3.9 %fusion.11 = bf16[256,2048]{1,0:T(8,128)(2,1)S(1)} fusion(f32[256,2048]{1,0:T(8,128)S(1)} %fusion, bf16[256,704]{0,1:T(8,128)(2,1)S(1)} %get-tuple-element.4, bf16[2048,1408]{1,0:T(8,128)(2,1)} %all-gather.8.cloned.1.call-done), kind=kOutput, calls=%fused_computation.12 | convolution fusion | flops 739246080 | bytes 6651904 | tf_op jit(solution)/shard_map/dot_general | solution.py:51
  191.1 1.1 copy.14
  192.1 4.8 %all-to-all-start = ((bf16[8,256,256]{2,1,0:T(8,128)(2,1)}), bf16[8,256,256]{2,1,0:T(8,128)(2,1)S(1)}, u32[]{:S(2)}, u32[]{:S(2)}) async-start(bf16[8,256,256]{2,1,0:T(8,128)(2,1)} %bitcast.11), calls=%async_computation | async-start | bytes 2097152 | tf_op jit(solution)/shard_map/all_to_all | solution.py:33
  197.0 3.9 %convolution_convert_fusion.1 = bf16[2048,704]{0,1:T(8,128)(2,1)} fusion(bf16[512,2048]{1,0:T(8,128)(2,1)S(1)} %copy-done.2, f32[256,704]{0,1:T(8,128)} %fusion.6, f32[256,704]{0,1:T(8,128)} %copy-done.3), kind=kOutput, calls=%fused_computation.2 | convolution fusion | flops 740720640 | bytes 5373952 | tf_op jit(solution)/shard_map/dot_general | solution.py:45
  200.9 4.6 %copy.11 = bf16[2048,704]{1,0:T(8,128)(2,1)} copy(bf16[2048,704]{0,1:T(8,128)(2,1)} %convolution_convert_fusion.1) | data formatting | bytes 5767168 | tf_op jit(solution)/shard_map/convert_element_type | solution.py:74
  205.5 5.9 %all-to-all-done = bf16[8,256,256]{2,1,0:T(8,128)(2,1)S(1)} async-done(((bf16[8,256,256]{2,1,0:T(8,128)(2,1)}), bf16[8,256,256]{2,1,0:T(8,128)(2,1)S(1)}, u32[]{:S(2)}, u32[]{:S(2)}) %all-to-all-start) | async-done | bytes 1048608 | tf_op jit(solution)/shard_map/all_to_all | solution.py:33
  211.4 0.0 copy-start
  211.4 1.0 copy-done
  212.4 7.2 %all-to-all-start.1 = ((bf16[32,64,704]{2,1,0:T(8,128)(2,1)}), bf16[32,64,704]{2,1,0:T(8,128)(2,1)S(1)}, u32[]{:S(2)}, u32[]{:S(2)}) async-start(bf16[32,64,704]{2,1,0:T(8,128)(2,1)} %bitcast.1), calls=%async_computation.3 | async-start | bytes 6291456 | tf_op jit(solution)/shard_map/all_to_all | solution.py:33
  219.6 0.0 reduce-scatter.5.cloned.1.call-start
  219.7 94.6 %reduce-scatter.3.cloned.1.call-done = bf16[256,1408]{1,0:T(8,128)(2,1)} async-done(((bf16[2048,1408]{1,0:T(8,128)(2,1)}), bf16[256,1408]{1,0:T(8,128)(2,1)}) %reduce-scatter.3.cloned.1.call-update) | async-done | bytes 720912 | tf_op jit(solution)/shard_map/reduce_scatter | solution.py:40
  314.2 0.0 reduce-scatter.5.cloned.1.call-update
  314.3 2.1 reduce_sum.21
  316.3 5.5 %all-to-all-done.1 = bf16[32,64,704]{2,1,0:T(8,128)(2,1)S(1)} async-done(((bf16[32,64,704]{2,1,0:T(8,128)(2,1)}), bf16[32,64,704]{2,1,0:T(8,128)(2,1)S(1)}, u32[]{:S(2)}, u32[]{:S(2)}) %all-to-all-start.1) | async-done | bytes 2883616 | tf_op jit(solution)/shard_map/all_to_all | solution.py:33
  321.8 1.1 convert_reduce_fusion
  322.9 23.4 %reduce-scatter.5.cloned.1.call-done = bf16[64,1408]{1,0:T(8,128)(2,1)} async-done(((bf16[256,1408]{1,0:T(8,128)(2,1)}), bf16[64,1408]{1,0:T(8,128)(2,1)}) %reduce-scatter.5.cloned.1.call-update) | async-done | bytes 180240 | tf_op jit(solution)/shard_map/reduce_scatter | solution.py:40
  346.3 1.7 fusion.27
Async XLA Ops:
  7.2 34.5 %all-gather.4.cloned.1.call-start = ((), (), s32[]{:S(2)}) async-start(), calls=%async_computation.4 | async-start | bytes 2359296 | tf_op jit(solution)/shard_map/all_gather | solution.py:16
  8.9 123.9 %all-gather.8.cloned.1.call-start = ((), (), s32[]{:S(2)}) async-start(), calls=%async_computation.6 | async-start | bytes 5947392 | tf_op jit(solution)/shard_map/all_gather | solution.py:16
  10.7 165.7 %all-gather.6.cloned.1.call-start = ((), (), s32[]{:S(2)}) async-start(), calls=%async_computation.5 | async-start | bytes 3538944 | tf_op jit(solution)/shard_map/all_gather | solution.py:22
  25.6 288.7 %reduce-scatter.3.cloned.1.call-start = ((), (), s32[]{:S(2)}) async-start(), calls=%async_computation.7 | async-start | bytes 6488064 | tf_op jit(solution)/shard_map/reduce_scatter | solution.py:40
  132.8 3.9 %copy-start.1 = (bf16[2048,1408]{1,0:T(8,128)(2,1)S(1)}, bf16[2048,1408]{1,0:T(8,128)(2,1)}, u32[]{:S(2)}) copy-start(bf16[2048,1408]{1,0:T(8,128)(2,1)} %all-gather.8.cloned.1.call-done) | copy-start | bytes 17301508
  136.7 39.6 %copy-start.3 = (f32[256,704]{0,1:T(8,128)}, f32[256,704]{0,1:T(8,128)S(1)}, u32[]{:S(2)}) copy-start(f32[256,704]{0,1:T(8,128)S(1)} %fusion.2) | copy-start | bytes 2162692
  136.7 39.6 %copy-start.2 = (bf16[512,2048]{1,0:T(8,128)(2,1)S(1)}, bf16[512,2048]{1,0:T(8,128)(2,1)}, u32[]{:S(2)}) copy-start(bf16[512,2048]{1,0:T(8,128)(2,1)} %all-gather.4.cloned.1.call-done) | copy-start | bytes 6291460
  192.1 19.3 %all-to-all-start = ((bf16[8,256,256]{2,1,0:T(8,128)(2,1)}), bf16[8,256,256]{2,1,0:T(8,128)(2,1)S(1)}, u32[]{:S(2)}, u32[]{:S(2)}) async-start(bf16[8,256,256]{2,1,0:T(8,128)(2,1)} %bitcast.11), calls=%async_computation | async-start | bytes 2097152 | tf_op jit(solution)/shard_map/all_to_all | solution.py:33
  211.4 1.0 copy-start
  212.4 109.4 %all-to-all-start.1 = ((bf16[32,64,704]{2,1,0:T(8,128)(2,1)}), bf16[32,64,704]{2,1,0:T(8,128)(2,1)S(1)}, u32[]{:S(2)}, u32[]{:S(2)}) async-start(bf16[32,64,704]{2,1,0:T(8,128)(2,1)} %bitcast.1), calls=%async_computation.3 | async-start | bytes 6291456 | tf_op jit(solution)/shard_map/all_to_all | solution.py:33
  219.6 126.7 %reduce-scatter.5.cloned.1.call-start = ((), (), s32[]{:S(2)}) async-start(), calls=%async_computation.8 | async-start | bytes 901120 | tf_op jit(solution)/shard_map/reduce_scatter | solution.py:40
Sparse Core Ops, SparseCore 0:
  9.8 31.7 all-gather.3
  44.8 88.0 all-gather.7
  134.6 41.6 all-gather.5
  184.4 129.8 reduce-scatter.2
  316.6 29.6 reduce-scatter.4
where the time goes:
time: 355 us
  waiting for transfers between devices  271 us (76%)
  matrix products  27.3 us (8%)
  blocking collectives  14.8 us (4%)
  between operations  13.8 us (4%)
  starting transfers between devices  12.2 us (3%)
  local copies, waits for them, and re-layouts  8.69 us (2%)
  other arithmetic  6.59 us (2%)
    reduce_scatter x2, waiting for transfers between devices, summed_rows(): subtotal = lax.psum_scatter(subtotal, axis, scatter_dimension=0, tiled=True)  118 us
    all_gather x2, waiting for transfers between devices, in_one_piece(): lax.all_gather(both, axis, axis=dim, tiled=True)  107 us
    all_gather x1, waiting for transfers between devices, gather_axes(): result = lax.all_gather(result, axes[number], axis=dim, tiled=True)  34.5 us
    all_gather x1, blocking collectives, gather_axes(): result = lax.all_gather(result, axes[number], axis=dim, tiled=True)  14.8 us
    all_to_all x2, starting transfers between devices, sent_and_summed(): lax.all_to_all(parts, axis, split_axis=0, concat_axis=0, tiled=True)  12 us
    all_to_all x2, waiting for transfers between devices, sent_and_summed(): lax.all_to_all(parts, axis, split_axis=0, concat_axis=0, tiled=True)  11.4 us
    dot_general x3, matrix products, contract_cols(): lax.dot_general(left, right, (((1,), (1,)), ((), ())), preferred_element_...  10.3 us
    dot_general x2, matrix products, contract_rows(): lax.dot_general(left, right, (((0,), (0,)), ((), ())), preferred_element_...  8.31 us
  transfers between devices with their start and end apart: 7, of which 7 were waited for; matrix products, arithmetic and copies ran while one was open for 8% of the time, Pallas kernels for 0%

commit v1 on v0

v1 whole, which is shorter than its diff:
```python
import jax
import jax.numpy as jnp
from jax import lax
from jax.experimental import pallas as pl
from jax.experimental.pallas import tpu as pltpu
from jax.sharding import Mesh
from jax.sharding import PartitionSpec as P


NZ, NY, NX = 8, 4, 4
RING = 4
BLOCK = 176
COLS = 3 * BLOCK
HALF = 128
ROWS = NY * HALF
SWAP = [(0, 1), (1, 0)]
ORDER = (0, -1, 1, 2)
VMEM = pl.BlockSpec(memory_space=pltpu.VMEM)
SMEM = pl.BlockSpec(memory_space=pltpu.SMEM)
ANY = pl.BlockSpec(memory_space=pl.ANY)


def dot(left, right, dims):
    return lax.dot_general(
        left, right, (dims, ((), ())), preferred_element_type=jnp.float32
    )


def call(kernel, outs, specs, *args, dtype=jnp.bfloat16, scratch=(), aliases={}, out_specs=None):
    return pl.pallas_call(
        kernel,
        out_shape=[jax.ShapeDtypeStruct(s, dtype) for s in outs],
        in_specs=specs,
        out_specs=out_specs or [VMEM] * len(outs),
        scratch_shapes=[pltpu.VMEM(s, jnp.bfloat16) for s in scratch],
        input_output_aliases=aliases,
        compiler_params=pltpu.CompilerParams(vmem_limit_bytes=56 * 1024 * 1024),
    )(*args)


def shift(array, axis, by):
    return lax.ppermute(array, axis, [(i, (i + by) % RING) for i in range(RING)])


def around(own, axis):
    return own, shift(own, axis, 1), shift(own, axis, -1), shift(own, axis, 2)


def around_in_halves(own, axis):
    low, high = shift(own, axis, 1), shift(own, axis, -1)
    far_first = shift(low[:2], axis, 1)
    far_last = shift(high[2:], axis, -1)
    return own, low, high, far_first, far_last


def front_kernel(
    place, gate, up, down, inputs, cotangent, came, keep, to_next, to_prev, to_far, inp, cot, pieces
):
    for y in range(NY):
        for part, array in enumerate((gate, up, down)):
            pieces[y, :, part * BLOCK : (part + 1) * BLOCK] = array[
                :, y * BLOCK : (y + 1) * BLOCK
            ]
    for out, by in ((keep, 0), (to_next, 1), (to_prev, NY - 1), (to_far, 2)):
        out[...] = pieces[(place[0] + by) % NY]
    for core in range(2):

        @pl.when(place[2] == core)
        def _():
            own = slice(core * 256, (core + 1) * 256)
            other = slice((1 - core) * 256, (2 - core) * 256)
            for which, (array, out) in enumerate(((inputs, inp), (cotangent, cot))):
                out[:, own] = array[core * HALF : (core + 1) * HALF, :]
                out[:, other] = came[which]


def join_kernel(place, kept, from_prev, from_next, from_far, out, pieces):
    for array, by in ((kept, 0), (from_prev, NY - 1), (from_next, 1), (from_far, 2)):
        pieces[(place[0] + by) % NY] = array[...]
    rows = jnp.concatenate([pieces[y] for y in range(NY)], axis=0)
    out[...] = rows.T


def split_kernel(place, grads, keep, to_next, to_prev, to_far, pieces):
    rows = grads[...].T
    for y in range(NY):
        pieces[y] = rows[y * 64 : (y + 1) * 64]
    for out, by in ((keep, 0), (to_next, 1), (to_prev, NY - 1), (to_far, 2)):
        out[...] = pieces[(place[0] + by) % NY]


def finish_kernel(place, kept, from_prev, from_next, from_far, gate, up, down, pieces):
    for array, by in ((kept, 0), (from_prev, NY - 1), (from_next, 1), (from_far, 2)):
        pieces[(place[0] + by) % NY] = array[...]
    for y in range(NY):
        for part, out in enumerate((gate, up, down)):
            out[:, y * BLOCK : (y + 1) * BLOCK] = pieces[
                y, :, part * BLOCK : (part + 1) * BLOCK
            ].astype(jnp.float32)


def exchange(pieces):
    keep, to_next, to_prev, to_far = pieces
    return keep, shift(to_next, "y", 1), shift(to_prev, "y", -1), shift(to_far, "y", 2)


def main_kernel(place, *refs):
    inp, cot = refs[0:5], refs[5:10]
    weights = refs[10:12]
    hid, grads_other, grads_own, acts, whole, flipped = refs[12:18]
    spots = ((0, 0, 4), (3, 0, 4), (1, 0, 4), (2, 0, 2), (2, 2, 4))
    for which, arrays in enumerate((inp, cot)):
        for array, (by, first, last) in zip(arrays, spots):
            for slot in range(first, last):
                near, far = place[1 - which] + ORDER[slot] + RING, place[which] + by
                x, y = (near, far) if which == 0 else (far, near)
                acts[
                    which,
                    pl.ds(pl.multiple_of((y % NY) * HALF, HALF), HALF),
                    pl.ds(pl.multiple_of((x % NX) * 512, 512), 512),
                ] = array[slot - first]
    for block, array in enumerate(weights):
        for z in range(NZ):
            whole[:, z * 256 : (z + 1) * 256] = array[z]
        gate_pre = dot(acts[0], whole[0:BLOCK, :], ((1,), (1,)))
        up_pre = dot(acts[0], whole[BLOCK : 2 * BLOCK, :], ((1,), (1,)))
        grad_hidden = dot(acts[1], whole[2 * BLOCK :, :], ((1,), (1,)))
        gate_sig = jax.nn.sigmoid(gate_pre)
        gate_act = gate_pre * gate_sig
        hid[block, 0] = (
            grad_hidden * up_pre * gate_sig * (1.0 + gate_pre * (1.0 - gate_sig))
        ).astype(jnp.bfloat16)
        hid[block, 1] = (grad_hidden * gate_act).astype(jnp.bfloat16)
        hid[block, 2] = (gate_act * up_pre).astype(jnp.bfloat16)
        for part in range(3):
            flipped[block, part] = hid[block, part].T

    def step(z, carry):
        lanes = pl.ds(pl.multiple_of(z * 256, 256), 256)
        for block, out in enumerate((grads_other, grads_own)):
            for part, which in ((0, 0), (1, 0), (2, 1)):
                out[z, part * BLOCK : (part + 1) * BLOCK, :] = dot(
                    flipped[block, part], acts[which, :, lanes], ((1,), (0,))
                ).astype(jnp.bfloat16)
        return carry

    lax.fori_loop(0, NZ, step, 0)


def inputs_kernel(hid, weights_a, weights_b, out):
    for z in range(NZ):
        total = jnp.zeros((ROWS, 256), jnp.float32)
        for block, array in enumerate((weights_a, weights_b)):
            for part in range(2):
                total = total + dot(
                    hid[block, part],
                    array[z, part * BLOCK : (part + 1) * BLOCK, :],
                    ((1,), (0,)),
                )
        for y in range(NY):
            out[y * NX + z // 2, :, (z % 2) * 256 : (z % 2 + 1) * 256] = total[
                y * HALF : (y + 1) * HALF
            ].astype(jnp.bfloat16)


def add_kernel(own, other, partial, out, partial_out):
    del partial, partial_out
    out[...] = (own[...].astype(jnp.float32) + other[...].astype(jnp.float32)).astype(jnp.bfloat16)


def hold_kernel(*refs):
    del refs


def per_device(inputs, cotangent, gate_weight, up_weight, down_weight):
    core = lax.axis_index("core")
    place = jnp.stack([lax.axis_index("y"), lax.axis_index("x"), core]).astype(jnp.int32)

    both = jnp.stack([inputs, cotangent]).reshape(2, 2, HALF, 256)
    sent = jnp.where(core == 0, both[:, 1], both[:, 0])
    came = lax.ppermute(sent, "core", SWAP)

    piece = (64, COLS)
    *pieces, inp, cot = call(
        front_kernel,
        [piece] * 4 + [(HALF, 512)] * 2,
        [SMEM] + [VMEM] * 6,
        place,
        gate_weight,
        up_weight,
        down_weight.T,
        inputs,
        cotangent,
        came,
        scratch=[(NY, *piece)],
    )

    moved = exchange(pieces)
    (rows,) = call(
        join_kernel,
        [(COLS, 256)],
        [SMEM] + [VMEM] * 4,
        place,
        *moved,
        scratch=[(NY, *piece)],
    )
    w_own = lax.all_gather(rows, "z", axis=0, tiled=False)

    inp_near, cot_near = around(inp, "x"), around(cot, "y")
    inp_blocks = around_in_halves(jnp.stack(inp_near), "y")
    cot_blocks = around_in_halves(jnp.stack(cot_near), "x")

    held = call(
        hold_kernel,
        [(NZ, COLS, 256)],
        [ANY] * 5,
        w_own,
        *inp_blocks[1:3],
        *cot_blocks[1:3],
        aliases={0: 0},
        out_specs=[ANY],
    )
    w_own = held[0]
    w_other = lax.ppermute(w_own, "core", SWAP)

    hid, grads_other, grads_own = call(
        main_kernel,
        [(2, 3, ROWS, BLOCK), (NZ, COLS, 256), (NZ, COLS, 256)],
        [SMEM] + [VMEM] * 12,
        place,
        *inp_blocks,
        *cot_blocks,
        w_other,
        w_own,
        scratch=[(2, ROWS, 2048), (COLS, 2048), (2, 3, BLOCK, ROWS)],
    )
    grads_came = lax.ppermute(grads_other, "core", SWAP)
    (partial,) = call(
        inputs_kernel, [(NY * NX, HALF, 512)], [VMEM] * 3, hid, w_other, w_own
    )
    grads, partial = call(
        add_kernel,
        [(NZ, COLS, 256), (NY * NX, HALF, 512)],
        [VMEM, VMEM, ANY],
        grads_own,
        grads_came,
        partial,
        aliases={2: 1},
        out_specs=[VMEM, ANY],
    )

    summed = lax.psum_scatter(grads, "z", scatter_dimension=0, tiled=False)
    pieces = call(
        split_kernel, [piece] * 4, [SMEM, VMEM], place, summed, scratch=[(NY, *piece)]
    )
    grad_gate, grad_up, grad_down = call(
        finish_kernel,
        [(64, NY * BLOCK)] * 3,
        [SMEM] + [VMEM] * 4,
        place,
        *exchange(pieces),
        dtype=jnp.float32,
        scratch=[(NY, *piece)],
    )

    arrived = lax.all_to_all(partial, ("y", "x"), split_axis=0, concat_axis=0, tiled=True)
    total = arrived.astype(jnp.float32).sum(axis=0).astype(jnp.bfloat16)
    lower, upper = total[:, :256], total[:, 256:]
    keep, give = jnp.where(core == 0, lower, upper), jnp.where(core == 0, upper, lower)
    take = lax.ppermute(give, "core", SWAP)
    grad_inputs = jnp.concatenate(
        [jnp.where(core == 0, keep, take), jnp.where(core == 0, take, keep)], axis=0
    )
    return grad_inputs, grad_gate, grad_up, grad_down.T


def solution(mesh):
    finer = Mesh(mesh.devices.reshape(NZ, NY, NX, 2), ("z", "y", "x", "core"))
    fs, tp = ("z", "y"), ("x", "core")

    return jax.shard_map(
        per_device,
        mesh=finer,
        in_specs=(P(fs, tp), P(fs, tp), P(fs, tp), P(fs, tp), P(tp, fs)),
        out_specs=(P(fs, tp), P(fs, tp), P(fs, tp), P(tp, fs)),
        check_vma=False,
    )
```

time: 355 us -> 174 us (0.49)
  waiting for transfers between devices: 271 us -> 46.8 us
  Pallas kernels: 0 us -> 31.9 us
  matrix products: 27.3 us -> 0 us
  blocking collectives: 14.8 us -> 33.6 us
  starting transfers between devices: 12.2 us -> 30.4 us
    all_gather x3 -> x1, waiting for transfers between devices: 142 us -> 13.1 us  [per_device(): w_own = lax.all_gather(rows, 'z', axis=0, tiled=False)]
    reduce_scatter x2 -> x1, waiting for transfers between devices: 118 us -> 1.65 us  [per_device(): summed = lax.psum_scatter(grads, 'z', scatter_dimension=0, tiled=False)]
    all_to_all x0 -> x1, blocking collectives: none -> 33.6 us  [per_device(): lax.all_to_all(partial, ('y', 'x'), split_axis=0, concat_axis=0, tiled=True)]
    ppermute x0 -> x24, waiting for transfers between devices: none -> 32.1 us  [the longest x20 30 us: shift(): lax.ppermute(array, axis, [(i, (i + by) % RING) for i in range(RING)])]
    pallas_call x0 -> x8, Pallas kernels: none -> 31.9 us  [call(): pl.pallas_call(kernel, out_shape=[jax.ShapeDtypeStruct(s, dtype) for s in...]
    ppermute x0 -> x24, starting transfers between devices: none -> 30.3 us  [the longest x20 30 us: shift(): lax.ppermute(array, axis, [(i, (i + by) % RING) for i in range(RING)])]
    dot_general x7 -> x0, matrix products: 27.3 us -> none  [the longest x3 10.3 us: contract_cols(): lax.dot_general(left, right, (((1,), (1,)), ((), ())), preferred_element_...]
    all_gather x1 -> x0, blocking collectives: 14.8 us -> none  [gather_axes(): result = lax.all_gather(result, axes[number], axis=dim, tiled=True)]
  transfers between devices with their start and end apart: 7 -> 26, of which waited for: 7 -> 18; matrix products, arithmetic and copies ran while one was open for 8% -> 5% of each run, Pallas kernels for 0% -> 4%
where the time goes in v1:
time: 174 us
  waiting for transfers between devices  46.8 us (27%)
  blocking collectives  33.6 us (19%)
  Pallas kernels  31.9 us (18%)
  starting transfers between devices  30.4 us (17%)
  between operations  14.2 us (8%)
  local copies, waits for them, and re-layouts  10.8 us (6%)
  other arithmetic  6.07 us (3%)
    all_to_all x1, blocking collectives, per_device(): lax.all_to_all(partial, ('y', 'x'), split_axis=0, concat_axis=0, tiled=True)  33.6 us
    pallas_call x8, Pallas kernels, call(): pl.pallas_call(kernel, out_shape=[jax.ShapeDtypeStruct(s, dtype) for s in...  31.9 us
    ppermute x20, waiting for transfers between devices, shift(): lax.ppermute(array, axis, [(i, (i + by) % RING) for i in range(RING)])  30 us
    ppermute x20, starting transfers between devices, shift(): lax.ppermute(array, axis, [(i, (i + by) % RING) for i in range(RING)])  30 us
    all_gather x1, waiting for transfers between devices, per_device(): w_own = lax.all_gather(rows, 'z', axis=0, tiled=False)  13.1 us
    unnamed x40, local copies, waits for them, and re-layouts  6.94 us
  transfers between devices with their start and end apart: 26, of which 18 were waited for; matrix products, arithmetic and copies ran while one was open for 5% of the time, Pallas kernels for 4%

profile of v1, /device:TPU:2, one launch (start us, length us, event | category | flops | bytes accessed | tf_op | source)
XLA Modules:
  0.0 173.7 jit_solution(18164734175983218335)
XLA Ops:
  7.2 1.0 fusion.2
  8.2 0.1 collective-permute-start
  8.3 0.6 pad_add_fusion.place
  8.8 0.8 collective-permute-done.came
  9.6 0.7 copy-done.13
  10.3 2.2 %shard_map.84 = (bf16[64,528]{1,0:T(8,128)(2,1)}, bf16[64,528]{1,0:T(8,128)(2,1)}, bf16[64,528]{1,0:T(8,128)(2,1)}, bf16[64,528]{1,0:T(8,128)(2,1)}, bf16[128,512]{1,0:T(8,128)(2,1)}, /*index=5*/bf16[128,512]{1,0:T(8,128)(2,1)}) custom-call(s32[3]{0:T(128)} %pad_add_fusion.place, bf16[64,704]{1,0:T(8,128)(2,1)} %gate.1, bf16[64,704]{1,0:T(8,128)(2,1)} %up.1, ...), custom_call_target="tpu_custom_call" | custom-call | tf_op jit(solution)/shard_map/pallas_call | solution.py:30
  12.5 1.6 collective-permute-start.15
  14.1 1.7 collective-permute-start.16
  15.7 2.0 %collective-permute-start.17 = (bf16[64,528]{1,0:T(8,128)(2,1)}, bf16[64,528]{1,0:T(8,128)(2,1)S(1)}, u32[]{:S(2)}, u32[]{:S(2)}) collective-permute-start(bf16[64,528]{1,0:T(8,128)(2,1)} %get-tuple-element.27), channel_id=1, source_target_pairs={{0,16},{8,24},{16,0},{24,8},{1,17},{9,25},{17,1},{25,9},{2,18},{10... | collective-permute-start | bytes 202760 | tf_op jit(solution)/shard_map/ppermute | solution.py:42
  17.7 0.8 collective-permute-done.15.from_prev
  18.5 0.2 collective-permute-done.16.from_next
  18.7 3.2 %collective-permute-done.17.from_far = bf16[64,528]{1,0:T(8,128)(2,1)S(1)} collective-permute-done((bf16[64,528]{1,0:T(8,128)(2,1)}, bf16[64,528]{1,0:T(8,128)(2,1)S(1)}, u32[]{:S(2)}, u32[]{:S(2)}) %collective-permute-start.17) | collective-permute-done | bytes 67616 | tf_op jit(solution)/shard_map/ppermute | solution.py:42
  21.9 0.6 copy-done.19
  22.5 1.9 %shard_map.85 = bf16[528,256]{1,0:T(8,128)(2,1)} custom-call(s32[3]{0:T(128)} %pad_add_fusion.place, bf16[64,528]{1,0:T(8,128)(2,1)} %get-tuple-element.24.kept, bf16[64,528]{1,0:T(8,128)(2,1)} %copy-done.17, bf16[64,528]{1,0:T(8,128)(2,1)} %copy-done.18, bf16[64,528]{1,0:T(8,128)(2,1)} %copy-done.19), custom_call_target="tpu_custom_call" | custom-call | tf_op jit(solution)/shard_map/pallas_call | solution.py:30
  24.5 2.1 %collective-permute-start.10 = (bf16[128,512]{1,0:T(8,128)(2,1)}, bf16[128,512]{1,0:T(8,128)(2,1)S(1)}, u32[]{:S(2)}, u32[]{:S(2)}) collective-permute-start(bf16[128,512]{1,0:T(8,128)(2,1)} %get-tuple-element.23), channel_id=1, source_target_pairs={{0,16},{8,24},{16,0},{24,8},{1,17},{9,25},{17,1},{25,9},{2,18},{10... | collective-permute-start | bytes 393224 | tf_op jit(solution)/shard_map/ppermute | solution.py:42
  26.5 1.4 collective-permute-start.9
  28.0 0.6 collective-permute-start.8
  28.6 2.1 %collective-permute-start.3 = (bf16[128,512]{1,0:T(8,128)(2,1)}, bf16[128,512]{1,0:T(8,128)(2,1)S(1)}, u32[]{:S(2)}, u32[]{:S(2)}) collective-permute-start(bf16[128,512]{1,0:T(8,128)(2,1)} %get-tuple-element.22), channel_id=1, source_target_pairs={{0,4},{2,6},{4,0},{6,2},{1,5},{3,7},{5,1},{7,3},{8,12},{10,14},{12... | collective-permute-start | bytes 393224 | tf_op jit(solution)/shard_map/ppermute | solution.py:42
  30.7 1.4 collective-permute-start.2
  32.1 1.2 collective-permute-start.1
  33.3 1.1 collective-permute-done.8
  34.3 1.0 pad_maximum_fusion.1.refs_5_
  35.3 1.6 collective-permute-start.12
  36.9 0.5 collective-permute-start.11
  37.4 1.0 pad_maximum_fusion.refs_0_
  38.4 3.4 %collective-permute-start.5 = (bf16[4,128,512]{2,1,0:T(8,128)(2,1)S(1)}, bf16[4,128,512]{2,1,0:T(8,128)(2,1)S(1)}, u32[]{:S(2)}, u32[]{:S(2)}) collective-permute-start(bf16[4,128,512]{2,1,0:T(8,128)(2,1)S(1)} %pad_maximum_fusion.refs_0_), channel_id=1, source_target_pairs={{0,24},{8,0},{16,8},{24,16},{1,25},{9,1},{17,9},{25,17},{2,26},{10... | collective-permute-start | bytes 1572872 | tf_op jit(solution)/shard_map/ppermute | solution.py:42
  41.8 6.0 %collective-permute-done.12.refs_4_.refs_7_ = bf16[4,128,512]{2,1,0:T(8,128)(2,1)S(1)} collective-permute-done((bf16[4,128,512]{2,1,0:T(8,128)(2,1)S(1)}, bf16[4,128,512]{2,1,0:T(8,128)(2,1)S(1)}, u32[]{:S(2)}, u32[]{:S(2)}) %collective-permute-start.12) | collective-permute-done | bytes 524320 | tf_op jit(solution)/shard_map/ppermute | solution.py:42
  47.9 1.7 collective-permute-done.11.refs_3_.refs_6_
  49.5 1.1 collective-permute-done.5.refs_2_
  50.7 3.4 %collective-permute-done.4.refs_1_ = bf16[4,128,512]{2,1,0:T(8,128)(2,1)S(1)} collective-permute-done((bf16[4,128,512]{2,1,0:T(8,128)(2,1)S(1)}, bf16[4,128,512]{2,1,0:T(8,128)(2,1)S(1)}, u32[]{:S(2)}, u32[]{:S(2)}) %collective-permute-start.4) | collective-permute-done | bytes 524320 | tf_op jit(solution)/shard_map/ppermute | solution.py:42
  54.1 13.1 %all-gather.3.cloned.1.call-done = bf16[4224,256]{1,0:T(8,128)(2,1)} async-done(((bf16[528,256]{1,0:T(8,128)(2,1)}), bf16[4224,256]{1,0:T(8,128)(2,1)}) %all-gather.3.cloned.1.call-update) | async-done | bytes 2162704 | tf_op jit(solution)/shard_map/all_gather | solution.py:207
  67.2 0.1 collective-permute-start.18
  67.3 1.0 slice.37
  68.3 0.6 collective-permute-start.14
  68.9 1.0 slice.36
  69.9 1.7 collective-permute-start.13
  71.6 1.0 slice.35
  72.6 2.8 %collective-permute-start.7 = (bf16[2,128,512]{2,1,0:T(8,128)(2,1)S(1)}, bf16[2,128,512]{2,1,0:T(8,128)(2,1)S(1)}, u32[]{:S(2)}, u32[]{:S(2)}) collective-permute-start(bf16[2,128,512]{2,1,0:T(8,128)(2,1)S(1)} %slice.35), channel_id=1, source_target_pairs={{0,24},{8,0},{16,8},{24,16},{1,25},{9,1},{17,9},{25,17},{2,26},{10... | collective-permute-start | bytes 786440 | tf_op jit(solution)/shard_map/ppermute | solution.py:42
  75.4 1.0 slice.34
  76.4 0.6 collective-permute-done.14.refs_9_
  77.0 2.6 %collective-permute-done.13.refs_8_ = bf16[2,128,512]{2,1,0:T(8,128)(2,1)S(1)} collective-permute-done((bf16[2,128,512]{2,1,0:T(8,128)(2,1)S(1)}, bf16[2,128,512]{2,1,0:T(8,128)(2,1)S(1)}, u32[]{:S(2)}, u32[]{:S(2)}) %collective-permute-start.13) | collective-permute-done | bytes 262176 | tf_op jit(solution)/shard_map/ppermute | solution.py:42
  79.6 1.4 collective-permute-done.7.refs_4_
  81.0 4.5 %collective-permute-done.6.refs_3_ = bf16[2,128,512]{2,1,0:T(8,128)(2,1)S(1)} collective-permute-done((bf16[2,128,512]{2,1,0:T(8,128)(2,1)S(1)}, bf16[2,128,512]{2,1,0:T(8,128)(2,1)S(1)}, u32[]{:S(2)}, u32[]{:S(2)}) %collective-permute-start.6) | collective-permute-done | bytes 262176 | tf_op jit(solution)/shard_map/ppermute | solution.py:42
  85.5 0.7 copy-done.12
  86.2 1.4 copy-done.1
  87.6 13.5 %shard_map.87 = (bf16[2,3,512,176]{3,2,1,0:T(8,128)(2,1)}, bf16[8,528,256]{2,1,0:T(8,128)(2,1)}, bf16[8,528,256]{2,1,0:T(8,128)(2,1)}) custom-call(s32[3]{0:T(128)} %pad_add_fusion.place, bf16[4,128,512]{2,1,0:T(8,128)(2,1)} %copy-done.8, bf16[4,128,512]{2,1,0:T(8,128)(2,1)} %copy-done.5, bf16[4,128,512]{2,1,0:T(8,128)(2,1)} %copy-done.4, ...), custom_call_target="tpu_custom_call" | custom-call | tf_op jit(solution)/shard_map/pallas_call | solution.py:30
  101.0 6.4 %shard_map.88.partial = bf16[16,128,512]{2,1,0:T(8,128)(2,1)} custom-call(bf16[2,3,512,176]{3,2,1,0:T(8,128)(2,1)} %get-tuple-element.30.hid, bf16[8,528,256]{2,1,0:T(8,128)(2,1)} %copy-done.1, bf16[8,528,256]{2,1,0:T(8,128)(2,1)} %shard_map.86.refs_11_.weights_b), custom_call_target="tpu_custom_call" | custom-call | tf_op jit(solution)/shard_map/pallas_call | solution.py:30
  107.4 1.4 copy-done.6
  108.8 4.1 %shard_map.89 = (bf16[8,528,256]{2,1,0:T(8,128)(2,1)}, bf16[16,128,512]{2,1,0:T(8,128)(2,1)}) custom-call(bf16[8,528,256]{2,1,0:T(8,128)(2,1)} %get-tuple-element.28.own, bf16[8,528,256]{2,1,0:T(8,128)(2,1)} %copy-done.6, bf16[16,128,512]{2,1,0:T(8,128)(2,1)} %shard_map.88.partial), custom_call_target="tpu_custom_call", output_to_operand_aliasing={{1}: (2, {})} | custom-call | tf_op jit(solution)/shard_map/pallas_call | solution.py:30
  113.0 1.6 copy-done
  114.5 33.6 %all_to_all.5 = bf16[16,128,512]{2,1,0:T(8,128)(2,1)} all-to-all(bf16[16,128,512]{2,1,0:T(8,128)(2,1)S(1)} %copy-done), channel_id=1, replica_groups=mesh['z'=8,'y'=4,'x'=4,'core'=2] {'y','x'}, dimensions={0} | all-to-all | bytes 4194304 | tf_op jit(solution)/shard_map/all_to_all | solution.py:266
  148.1 1.9 %reduce_sum.12 = bf16[128,512]{1,0:T(8,128)(2,1)S(1)} reduce(bf16[16,128,512]{2,1,0:T(8,128)(2,1)} %all_to_all.5, bf16[]{:T(256)} %constant.15.clone.1), dimensions={0}, to_apply=%region_0.1 | reduce | flops 983040 | bytes 2228226 | tf_op jit(solution)/shard_map/reduce_sum | solution.py:267
  150.1 0.1 collective-permute-start.20
  150.2 1.2 collective-permute-done.20
  151.4 1.6 reduce-scatter.2.cloned.1.call-done
  153.1 1.8 %shard_map.90 = (bf16[64,528]{1,0:T(8,128)(2,1)}, bf16[64,528]{1,0:T(8,128)(2,1)}, bf16[64,528]{1,0:T(8,128)(2,1)}, bf16[64,528]{1,0:T(8,128)(2,1)}) custom-call(s32[3]{0:T(128)} %pad_add_fusion.place, bf16[528,256]{1,0:T(8,128)(2,1)} %bitcast.22), custom_call_target="tpu_custom_call" | custom-call | tf_op jit(solution)/shard_map/pallas_call | solution.py:30
  154.9 1.7 collective-permute-start.21
  156.6 1.6 collective-permute-start.22
  158.1 2.0 %collective-permute-start.23 = (bf16[64,528]{1,0:T(8,128)(2,1)}, bf16[64,528]{1,0:T(8,128)(2,1)S(1)}, u32[]{:S(2)}, u32[]{:S(2)}) collective-permute-start(bf16[64,528]{1,0:T(8,128)(2,1)} %get-tuple-element.36), channel_id=1, source_target_pairs={{0,16},{8,24},{16,0},{24,8},{1,17},{9,25},{17,1},{25,9},{2,18},{10... | collective-permute-start | bytes 202760 | tf_op jit(solution)/shard_map/ppermute | solution.py:42
  160.1 0.7 pad_maximum_fusion.3
  160.8 0.8 collective-permute-done.21.from_prev
  161.6 2.7 %collective-permute-done.23.from_far = bf16[64,528]{1,0:T(8,128)(2,1)S(1)} collective-permute-done((bf16[64,528]{1,0:T(8,128)(2,1)}, bf16[64,528]{1,0:T(8,128)(2,1)S(1)}, u32[]{:S(2)}, u32[]{:S(2)}) %collective-permute-start.23) | collective-permute-done | bytes 67616 | tf_op jit(solution)/shard_map/ppermute | solution.py:42
  164.3 0.6 copy-done.16
  164.9 2.0 %shard_map.91 = (f32[64,704]{1,0:T(8,128)}, f32[64,704]{1,0:T(8,128)}, f32[64,704]{1,0:T(8,128)}) custom-call(s32[3]{0:T(128)} %pad_add_fusion.place, bf16[64,528]{1,0:T(8,128)(2,1)} %get-tuple-element.33.kept, bf16[64,528]{1,0:T(8,128)(2,1)} %copy-done.14, bf16[64,528]{1,0:T(8,128)(2,1)} %copy-done.15, bf16[64,528]{1,0:T(8,128)(2,1)} %copy-done.16), custom_call_target="tpu_custom_call" | custom-call | tf_op jit(solution)/shard_map/pallas_call | solution.py:30
  (51 shorter events, 0.3 us)
Async XLA Ops:
  7.2 60.0 %all-gather.3.cloned.1.call-start = ((), (), s32[]{:S(2)}) async-start(), calls=%async_computation.3 | async-start | bytes 2433024 | tf_op jit(solution)/shard_map/all_gather | solution.py:207
  8.2 1.4 collective-permute-start
  9.6 0.7 copy-start.13
  12.5 6.0 %collective-permute-start.15 = (bf16[64,528]{1,0:T(8,128)(2,1)}, bf16[64,528]{1,0:T(8,128)(2,1)S(1)}, u32[]{:S(2)}, u32[]{:S(2)}) collective-permute-start(bf16[64,528]{1,0:T(8,128)(2,1)} %get-tuple-element.25), channel_id=1, source_target_pairs={{0,8},{8,16},{16,24},{24,0},{1,9},{9,17},{17,25},{25,1},{2,10},{10... | collective-permute-start | bytes 202760 | tf_op jit(solution)/shard_map/ppermute | solution.py:42
  14.1 4.7 %collective-permute-start.16 = (bf16[64,528]{1,0:T(8,128)(2,1)}, bf16[64,528]{1,0:T(8,128)(2,1)S(1)}, u32[]{:S(2)}, u32[]{:S(2)}) collective-permute-start(bf16[64,528]{1,0:T(8,128)(2,1)} %get-tuple-element.26), channel_id=1, source_target_pairs={{0,24},{8,0},{16,8},{24,16},{1,25},{9,1},{17,9},{25,17},{2,26},{10... | collective-permute-start | bytes 202760 | tf_op jit(solution)/shard_map/ppermute | solution.py:42
  15.7 6.2 %collective-permute-start.17 = (bf16[64,528]{1,0:T(8,128)(2,1)}, bf16[64,528]{1,0:T(8,128)(2,1)S(1)}, u32[]{:S(2)}, u32[]{:S(2)}) collective-permute-start(bf16[64,528]{1,0:T(8,128)(2,1)} %get-tuple-element.27), channel_id=1, source_target_pairs={{0,16},{8,24},{16,0},{24,8},{1,17},{9,25},{17,1},{25,9},{2,18},{10... | collective-permute-start | bytes 202760 | tf_op jit(solution)/shard_map/ppermute | solution.py:42
  18.5 3.4 %copy-start.17 = (bf16[64,528]{1,0:T(8,128)(2,1)}, bf16[64,528]{1,0:T(8,128)(2,1)S(1)}, u32[]{:S(2)}) copy-start(bf16[64,528]{1,0:T(8,128)(2,1)S(1)} %collective-permute-done.15.from_prev) | copy-start | bytes 202756
  18.7 3.2 %copy-start.18 = (bf16[64,528]{1,0:T(8,128)(2,1)}, bf16[64,528]{1,0:T(8,128)(2,1)S(1)}, u32[]{:S(2)}) copy-start(bf16[64,528]{1,0:T(8,128)(2,1)S(1)} %collective-permute-done.16.from_next) | copy-start | bytes 202756
  21.9 0.6 copy-start.19
  24.4 128.7 %reduce-scatter.2.cloned.1.call-start = ((), (), s32[]{:S(2)}) async-start(), calls=%async_computation.2 | async-start | bytes 2433024 | tf_op jit(solution)/shard_map/reduce_scatter | solution.py:252
  24.5 7.7 %collective-permute-start.10 = (bf16[128,512]{1,0:T(8,128)(2,1)}, bf16[128,512]{1,0:T(8,128)(2,1)S(1)}, u32[]{:S(2)}, u32[]{:S(2)}) collective-permute-start(bf16[128,512]{1,0:T(8,128)(2,1)} %get-tuple-element.23), channel_id=1, source_target_pairs={{0,16},{8,24},{16,0},{24,8},{1,17},{9,25},{17,1},{25,9},{2,18},{10... | collective-permute-start | bytes 393224 | tf_op jit(solution)/shard_map/ppermute | solution.py:42
  26.5 6.8 %collective-permute-start.9 = (bf16[128,512]{1,0:T(8,128)(2,1)}, bf16[128,512]{1,0:T(8,128)(2,1)S(1)}, u32[]{:S(2)}, u32[]{:S(2)}) collective-permute-start(bf16[128,512]{1,0:T(8,128)(2,1)} %get-tuple-element.23), channel_id=1, source_target_pairs={{0,24},{8,0},{16,8},{24,16},{1,25},{9,1},{17,9},{25,17},{2,26},{10... | collective-permute-start | bytes 393224 | tf_op jit(solution)/shard_map/ppermute | solution.py:42
  28.0 6.4 %collective-permute-start.8 = (bf16[128,512]{1,0:T(8,128)(2,1)}, bf16[128,512]{1,0:T(8,128)(2,1)S(1)}, u32[]{:S(2)}, u32[]{:S(2)}) collective-permute-start(bf16[128,512]{1,0:T(8,128)(2,1)} %get-tuple-element.23), channel_id=1, source_target_pairs={{0,8},{8,16},{16,24},{24,0},{1,9},{9,17},{17,25},{25,1},{2,10},{10... | collective-permute-start | bytes 393224 | tf_op jit(solution)/shard_map/ppermute | solution.py:42
  28.6 8.9 %collective-permute-start.3 = (bf16[128,512]{1,0:T(8,128)(2,1)}, bf16[128,512]{1,0:T(8,128)(2,1)S(1)}, u32[]{:S(2)}, u32[]{:S(2)}) collective-permute-start(bf16[128,512]{1,0:T(8,128)(2,1)} %get-tuple-element.22), channel_id=1, source_target_pairs={{0,4},{2,6},{4,0},{6,2},{1,5},{3,7},{5,1},{7,3},{8,12},{10,14},{12... | collective-permute-start | bytes 393224 | tf_op jit(solution)/shard_map/ppermute | solution.py:42
  30.7 6.8 %collective-permute-start.2 = (bf16[128,512]{1,0:T(8,128)(2,1)}, bf16[128,512]{1,0:T(8,128)(2,1)S(1)}, u32[]{:S(2)}, u32[]{:S(2)}) collective-permute-start(bf16[128,512]{1,0:T(8,128)(2,1)} %get-tuple-element.22), channel_id=1, source_target_pairs={{0,6},{2,0},{4,2},{6,4},{1,7},{3,1},{5,3},{7,5},{8,14},{10,8},{12,... | collective-permute-start | bytes 393224 | tf_op jit(solution)/shard_map/ppermute | solution.py:42
  32.1 5.3 %collective-permute-start.1 = (bf16[128,512]{1,0:T(8,128)(2,1)}, bf16[128,512]{1,0:T(8,128)(2,1)S(1)}, u32[]{:S(2)}, u32[]{:S(2)}) collective-permute-start(bf16[128,512]{1,0:T(8,128)(2,1)} %get-tuple-element.22), channel_id=1, source_target_pairs={{0,2},{2,4},{4,6},{6,0},{1,3},{3,5},{5,7},{7,1},{8,10},{10,12},{12... | collective-permute-start | bytes 393224 | tf_op jit(solution)/shard_map/ppermute | solution.py:42
  35.3 31.9 %copy-start.7 = (bf16[4,128,512]{2,1,0:T(8,128)(2,1)}, bf16[4,128,512]{2,1,0:T(8,128)(2,1)S(1)}, u32[]{:S(2)}) copy-start(bf16[4,128,512]{2,1,0:T(8,128)(2,1)S(1)} %pad_maximum_fusion.1.refs_5_) | copy-start | bytes 1572868
  35.3 12.6 %collective-permute-start.12 = (bf16[4,128,512]{2,1,0:T(8,128)(2,1)S(1)}, bf16[4,128,512]{2,1,0:T(8,128)(2,1)S(1)}, u32[]{:S(2)}, u32[]{:S(2)}) collective-permute-start(bf16[4,128,512]{2,1,0:T(8,128)(2,1)S(1)} %pad_maximum_fusion.1.refs_5_), channel_id=1, source_target_pairs={{0,6},{2,0},{4,2},{6,4},{1,7},{3,1},{5,3},{7,5},{8,14},{10,8},{12,... | collective-permute-start | bytes 1572872 | tf_op jit(solution)/shard_map/ppermute | solution.py:42
  36.9 12.6 %collective-permute-start.11 = (bf16[4,128,512]{2,1,0:T(8,128)(2,1)S(1)}, bf16[4,128,512]{2,1,0:T(8,128)(2,1)S(1)}, u32[]{:S(2)}, u32[]{:S(2)}) collective-permute-start(bf16[4,128,512]{2,1,0:T(8,128)(2,1)S(1)} %pad_maximum_fusion.1.refs_5_), channel_id=1, source_target_pairs={{0,2},{2,4},{4,6},{6,0},{1,3},{3,5},{5,7},{7,1},{8,10},{10,12},{12... | collective-permute-start | bytes 1572872 | tf_op jit(solution)/shard_map/ppermute | solution.py:42
  38.4 47.1 %copy-start.8 = (bf16[4,128,512]{2,1,0:T(8,128)(2,1)}, bf16[4,128,512]{2,1,0:T(8,128)(2,1)S(1)}, u32[]{:S(2)}) copy-start(bf16[4,128,512]{2,1,0:T(8,128)(2,1)S(1)} %pad_maximum_fusion.refs_0_) | copy-start | bytes 1572868
  38.4 12.2 %collective-permute-start.5 = (bf16[4,128,512]{2,1,0:T(8,128)(2,1)S(1)}, bf16[4,128,512]{2,1,0:T(8,128)(2,1)S(1)}, u32[]{:S(2)}, u32[]{:S(2)}) collective-permute-start(bf16[4,128,512]{2,1,0:T(8,128)(2,1)S(1)} %pad_maximum_fusion.refs_0_), channel_id=1, source_target_pairs={{0,24},{8,0},{16,8},{24,16},{1,25},{9,1},{17,9},{25,17},{2,26},{10... | collective-permute-start | bytes 1572872 | tf_op jit(solution)/shard_map/ppermute | solution.py:42
  41.8 12.2 %collective-permute-start.4 = (bf16[4,128,512]{2,1,0:T(8,128)(2,1)S(1)}, bf16[4,128,512]{2,1,0:T(8,128)(2,1)S(1)}, u32[]{:S(2)}, u32[]{:S(2)}) collective-permute-start(bf16[4,128,512]{2,1,0:T(8,128)(2,1)S(1)} %pad_maximum_fusion.refs_0_), channel_id=1, source_target_pairs={{0,8},{8,16},{16,24},{24,0},{1,9},{9,17},{17,25},{25,1},{2,10},{10... | collective-permute-start | bytes 1572872 | tf_op jit(solution)/shard_map/ppermute | solution.py:42
  47.9 19.3 %copy-start.2 = (bf16[4,128,512]{2,1,0:T(8,128)(2,1)}, bf16[4,128,512]{2,1,0:T(8,128)(2,1)S(1)}, u32[]{:S(2)}) copy-start(bf16[4,128,512]{2,1,0:T(8,128)(2,1)S(1)} %collective-permute-done.12.refs_4_.refs_7_) | copy-start | bytes 1572868
  49.5 17.6 %copy-start.3 = (bf16[4,128,512]{2,1,0:T(8,128)(2,1)}, bf16[4,128,512]{2,1,0:T(8,128)(2,1)S(1)}, u32[]{:S(2)}) copy-start(bf16[4,128,512]{2,1,0:T(8,128)(2,1)S(1)} %collective-permute-done.11.refs_3_.refs_6_) | copy-start | bytes 1572868
  50.7 16.5 %copy-start.4 = (bf16[4,128,512]{2,1,0:T(8,128)(2,1)}, bf16[4,128,512]{2,1,0:T(8,128)(2,1)S(1)}, u32[]{:S(2)}) copy-start(bf16[4,128,512]{2,1,0:T(8,128)(2,1)S(1)} %collective-permute-done.5.refs_2_) | copy-start | bytes 1572868
  54.1 13.1 %copy-start.5 = (bf16[4,128,512]{2,1,0:T(8,128)(2,1)}, bf16[4,128,512]{2,1,0:T(8,128)(2,1)S(1)}, u32[]{:S(2)}) copy-start(bf16[4,128,512]{2,1,0:T(8,128)(2,1)S(1)} %collective-permute-done.4.refs_1_) | copy-start | bytes 1572868
  67.2 18.3 %collective-permute-start.18 = (bf16[8,528,256]{2,1,0:T(8,128)(2,1)}, bf16[8,528,256]{2,1,0:T(8,128)(2,1)S(1)}, u32[]{:S(2)}, u32[]{:S(2)}) collective-permute-start(bf16[8,528,256]{2,1,0:T(8,128)(2,1)} %shard_map.86.refs_11_.weights_b), channel_id=1, source_target_pairs={{0,1},{1,0},{2,3},{3,2},{4,5},{5,4},{6,7},{7,6},{8,9},{9,8},{10,11... | collective-permute-start | bytes 6488072 | tf_op jit(solution)/shard_map/ppermute | solution.py:224
  68.3 8.8 %collective-permute-start.14 = (bf16[2,128,512]{2,1,0:T(8,128)(2,1)S(1)}, bf16[2,128,512]{2,1,0:T(8,128)(2,1)S(1)}, u32[]{:S(2)}, u32[]{:S(2)}) collective-permute-start(bf16[2,128,512]{2,1,0:T(8,128)(2,1)S(1)} %slice.37), channel_id=1, source_target_pairs={{0,6},{2,0},{4,2},{6,4},{1,7},{3,1},{5,3},{7,5},{8,14},{10,8},{12,... | collective-permute-start | bytes 786440 | tf_op jit(solution)/shard_map/ppermute | solution.py:42
  69.9 9.7 %collective-permute-start.13 = (bf16[2,128,512]{2,1,0:T(8,128)(2,1)S(1)}, bf16[2,128,512]{2,1,0:T(8,128)(2,1)S(1)}, u32[]{:S(2)}, u32[]{:S(2)}) collective-permute-start(bf16[2,128,512]{2,1,0:T(8,128)(2,1)S(1)} %slice.36), channel_id=1, source_target_pairs={{0,2},{2,4},{4,6},{6,0},{1,3},{3,5},{5,7},{7,1},{8,10},{10,12},{12... | collective-permute-start | bytes 786440 | tf_op jit(solution)/shard_map/ppermute | solution.py:42
  72.6 8.5 %collective-permute-start.7 = (bf16[2,128,512]{2,1,0:T(8,128)(2,1)S(1)}, bf16[2,128,512]{2,1,0:T(8,128)(2,1)S(1)}, u32[]{:S(2)}, u32[]{:S(2)}) collective-permute-start(bf16[2,128,512]{2,1,0:T(8,128)(2,1)S(1)} %slice.35), channel_id=1, source_target_pairs={{0,24},{8,0},{16,8},{24,16},{1,25},{9,1},{17,9},{25,17},{2,26},{10... | collective-permute-start | bytes 786440 | tf_op jit(solution)/shard_map/ppermute | solution.py:42
  76.3 9.2 %collective-permute-start.6 = (bf16[2,128,512]{2,1,0:T(8,128)(2,1)S(1)}, bf16[2,128,512]{2,1,0:T(8,128)(2,1)S(1)}, u32[]{:S(2)}, u32[]{:S(2)}) collective-permute-start(bf16[2,128,512]{2,1,0:T(8,128)(2,1)S(1)} %slice.34), channel_id=1, source_target_pairs={{0,8},{8,16},{16,24},{24,0},{1,9},{9,17},{17,25},{25,1},{2,10},{10... | collective-permute-start | bytes 786440 | tf_op jit(solution)/shard_map/ppermute | solution.py:42
  77.0 8.5 %copy-start.9 = (bf16[2,128,512]{2,1,0:T(8,128)(2,1)}, bf16[2,128,512]{2,1,0:T(8,128)(2,1)S(1)}, u32[]{:S(2)}) copy-start(bf16[2,128,512]{2,1,0:T(8,128)(2,1)S(1)} %collective-permute-done.14.refs_9_) | copy-start | bytes 786436
  79.6 5.9 %copy-start.10 = (bf16[2,128,512]{2,1,0:T(8,128)(2,1)}, bf16[2,128,512]{2,1,0:T(8,128)(2,1)S(1)}, u32[]{:S(2)}) copy-start(bf16[2,128,512]{2,1,0:T(8,128)(2,1)S(1)} %collective-permute-done.13.refs_8_) | copy-start | bytes 786436
  81.0 4.5 %copy-start.11 = (bf16[2,128,512]{2,1,0:T(8,128)(2,1)}, bf16[2,128,512]{2,1,0:T(8,128)(2,1)S(1)}, u32[]{:S(2)}) copy-start(bf16[2,128,512]{2,1,0:T(8,128)(2,1)S(1)} %collective-permute-done.7.refs_4_) | copy-start | bytes 786436
  85.5 0.7 copy-start.12
  86.2 1.4 copy-start.1
  101.0 6.4 %collective-permute-start.19 = (bf16[8,528,256]{2,1,0:T(8,128)(2,1)}, bf16[8,528,256]{2,1,0:T(8,128)(2,1)S(1)}, u32[]{:S(2)}, u32[]{:S(2)}) collective-permute-start(bf16[8,528,256]{2,1,0:T(8,128)(2,1)} %get-tuple-element.29), channel_id=1, source_target_pairs={{0,1},{1,0},{2,3},{3,2},{4,5},{5,4},{6,7},{7,6},{8,9},{9,8},{10,11... | collective-permute-start | bytes 6488072 | tf_op jit(solution)/shard_map/ppermute | solution.py:237
  107.4 1.4 copy-start.6
  112.9 1.6 copy-start
  150.1 1.3 collective-permute-start.20
  154.9 6.7 %collective-permute-start.21 = (bf16[64,528]{1,0:T(8,128)(2,1)}, bf16[64,528]{1,0:T(8,128)(2,1)S(1)}, u32[]{:S(2)}, u32[]{:S(2)}) collective-permute-start(bf16[64,528]{1,0:T(8,128)(2,1)} %get-tuple-element.34), channel_id=1, source_target_pairs={{0,8},{8,16},{16,24},{24,0},{1,9},{9,17},{17,25},{25,1},{2,10},{10... | collective-permute-start | bytes 202760 | tf_op jit(solution)/shard_map/ppermute | solution.py:42
  156.6 5.0 %collective-permute-start.22 = (bf16[64,528]{1,0:T(8,128)(2,1)}, bf16[64,528]{1,0:T(8,128)(2,1)S(1)}, u32[]{:S(2)}, u32[]{:S(2)}) collective-permute-start(bf16[64,528]{1,0:T(8,128)(2,1)} %get-tuple-element.35), channel_id=1, source_target_pairs={{0,24},{8,0},{16,8},{24,16},{1,25},{9,1},{17,9},{25,17},{2,26},{10... | collective-permute-start | bytes 202760 | tf_op jit(solution)/shard_map/ppermute | solution.py:42
  158.1 6.2 %collective-permute-start.23 = (bf16[64,528]{1,0:T(8,128)(2,1)}, bf16[64,528]{1,0:T(8,128)(2,1)S(1)}, u32[]{:S(2)}, u32[]{:S(2)}) collective-permute-start(bf16[64,528]{1,0:T(8,128)(2,1)} %get-tuple-element.36), channel_id=1, source_target_pairs={{0,16},{8,24},{16,0},{24,8},{1,17},{9,25},{17,1},{25,9},{2,18},{10... | collective-permute-start | bytes 202760 | tf_op jit(solution)/shard_map/ppermute | solution.py:42
  161.6 2.7 %copy-start.14 = (bf16[64,528]{1,0:T(8,128)(2,1)}, bf16[64,528]{1,0:T(8,128)(2,1)S(1)}, u32[]{:S(2)}) copy-start(bf16[64,528]{1,0:T(8,128)(2,1)S(1)} %collective-permute-done.21.from_prev) | copy-start | bytes 202756
  161.6 2.7 %copy-start.15 = (bf16[64,528]{1,0:T(8,128)(2,1)}, bf16[64,528]{1,0:T(8,128)(2,1)S(1)}, u32[]{:S(2)}) copy-start(bf16[64,528]{1,0:T(8,128)(2,1)S(1)} %collective-permute-done.22.from_next) | copy-start | bytes 202756
  164.3 0.6 copy-start.16
Sparse Core Ops, SparseCore 0:
  24.5 42.5 all-gather.2
  113.1 39.9 reduce-scatter.1

commit v2 on v1

--- a/solution.py
+++ b/solution.py
@@ -26,13 +26,14 @@
     )
 
 
-def call(kernel, outs, specs, *args, dtype=jnp.bfloat16, scratch=(), aliases={}, out_specs=None):
+def call(kernel, outs, specs, *args, dtype=jnp.bfloat16, scratch=(), sems=(), aliases={}, out_specs=None):
     return pl.pallas_call(
         kernel,
         out_shape=[jax.ShapeDtypeStruct(s, dtype) for s in outs],
         in_specs=specs,
         out_specs=out_specs or [VMEM] * len(outs),
-        scratch_shapes=[pltpu.VMEM(s, jnp.bfloat16) for s in scratch],
+        scratch_shapes=[pltpu.VMEM(s, jnp.bfloat16) for s in scratch]
+        + [pltpu.SemaphoreType.DMA(s) for s in sems],
         input_output_aliases=aliases,
         compiler_params=pltpu.CompilerParams(vmem_limit_bytes=56 * 1024 * 1024),
     )(*args)
@@ -53,9 +54,7 @@
     return own, low, high, far_first, far_last
 
 
-def front_kernel(
-    place, gate, up, down, inputs, cotangent, came, keep, to_next, to_prev, to_far, inp, cot, pieces
-):
+def cut_kernel(place, gate, up, down, keep, to_next, to_prev, to_far, pieces):
     for y in range(NY):
         for part, array in enumerate((gate, up, down)):
             pieces[y, :, part * BLOCK : (part + 1) * BLOCK] = array[
@@ -63,6 +62,9 @@
             ]
     for out, by in ((keep, 0), (to_next, 1), (to_prev, NY - 1), (to_far, 2)):
         out[...] = pieces[(place[0] + by) % NY]
+
+
+def pair_kernel(place, inputs, cotangent, came, inp, cot):
     for core in range(2):
 
         @pl.when(place[2] == core)
@@ -107,44 +109,73 @@
 def main_kernel(place, *refs):
     inp, cot = refs[0:5], refs[5:10]
     weights = refs[10:12]
-    hid, grads_other, grads_own, acts, whole, flipped = refs[12:18]
+    hid, grads_other, grads_own = refs[12:15]
+    acts, whole, flipped, hid_at, out_at, acts_sems, weight_sems, out_sems = refs[15:]
+
+    loads = []
     spots = ((0, 0, 4), (3, 0, 4), (1, 0, 4), (2, 0, 2), (2, 2, 4))
     for which, arrays in enumerate((inp, cot)):
+        count = 0
         for array, (by, first, last) in zip(arrays, spots):
             for slot in range(first, last):
                 near, far = place[1 - which] + ORDER[slot] + RING, place[which] + by
                 x, y = (near, far) if which == 0 else (far, near)
-                acts[
+                spot = acts.at[
                     which,
                     pl.ds(pl.multiple_of((y % NY) * HALF, HALF), HALF),
                     pl.ds(pl.multiple_of((x % NX) * 512, 512), 512),
-                ] = array[slot - first]
-    for block, array in enumerate(weights):
-        for z in range(NZ):
-            whole[:, z * 256 : (z + 1) * 256] = array[z]
-        gate_pre = dot(acts[0], whole[0:BLOCK, :], ((1,), (1,)))
-        up_pre = dot(acts[0], whole[BLOCK : 2 * BLOCK, :], ((1,), (1,)))
-        grad_hidden = dot(acts[1], whole[2 * BLOCK :, :], ((1,), (1,)))
+                ]
+                sem = acts_sems.at[which, count]
+                loads.append(pltpu.make_async_copy(array.at[slot - first], spot, sem))
+                count += 1
+    fetches = [
+        [
+            pltpu.make_async_copy(
+                array.at[z], whole.at[block, :, z * 256 : (z + 1) * 256], weight_sems.at[block, z]
+            )
+            for z in range(NZ)
+        ]
+        for block, array in enumerate(weights)
+    ]
+    for copy in loads + fetches[1] + fetches[0]:
+        copy.start()
+    for copy in loads:
+        copy.wait()
+    stores = []
+    for block in (1, 0):
+        for copy in fetches[block]:
+            copy.wait()
+        gate_pre = dot(acts[0], whole[block, 0:BLOCK, :], ((1,), (1,)))
+        up_pre = dot(acts[0], whole[block, BLOCK : 2 * BLOCK, :], ((1,), (1,)))
+        grad_hidden = dot(acts[1], whole[block, 2 * BLOCK :, :], ((1,), (1,)))
         gate_sig = jax.nn.sigmoid(gate_pre)
         gate_act = gate_pre * gate_sig
-        hid[block, 0] = (
+        hid_at[block, 0] = (
             grad_hidden * up_pre * gate_sig * (1.0 + gate_pre * (1.0 - gate_sig))
         ).astype(jnp.bfloat16)
-        hid[block, 1] = (grad_hidden * gate_act).astype(jnp.bfloat16)
-        hid[block, 2] = (gate_act * up_pre).astype(jnp.bfloat16)
+        hid_at[block, 1] = (grad_hidden * gate_act).astype(jnp.bfloat16)
+        hid_at[block, 2] = (gate_act * up_pre).astype(jnp.bfloat16)
+        store = pltpu.make_async_copy(hid_at.at[block], hid.at[block], out_sems.at[block])
+        store.start()
+        stores.append(store)
         for part in range(3):
-            flipped[block, part] = hid[block, part].T
-
-    def step(z, carry):
-        lanes = pl.ds(pl.multiple_of(z * 256, 256), 256)
-        for block, out in enumerate((grads_other, grads_own)):
+            flipped[block, part] = hid_at[block, part].T
+    for block, out in ((1, grads_own), (0, grads_other)):
+
+        def step(z, carry):
+            lanes = pl.ds(pl.multiple_of(z * 256, 256), 256)
             for part, which in ((0, 0), (1, 0), (2, 1)):
-                out[z, part * BLOCK : (part + 1) * BLOCK, :] = dot(
+                out_at[block, z, part * BLOCK : (part + 1) * BLOCK, :] = dot(
                     flipped[block, part], acts[which, :, lanes], ((1,), (0,))
                 ).astype(jnp.bfloat16)
-        return carry
-
-    lax.fori_loop(0, NZ, step, 0)
+            return carry
+
+        lax.fori_loop(0, NZ, step, 0)
+        store = pltpu.make_async_copy(out_at.at[block], out, out_sems.at[2 + block])
+        store.start()
+        stores.append(store)
+    for store in stores:
+        store.wait()
 
 
 def inputs_kernel(hid, weights_a, weights_b, out):
@@ -163,11 +194,6 @@
             ].astype(jnp.bfloat16)
 
 
-def add_kernel(own, other, partial, out, partial_out):
-    del partial, partial_out
-    out[...] = (own[...].astype(jnp.float32) + other[...].astype(jnp.float32)).astype(jnp.bfloat16)
-
-
 def hold_kernel(*refs):
     del refs
 
@@ -181,20 +207,16 @@
     came = lax.ppermute(sent, "core", SWAP)
 
     piece = (64, COLS)
-    *pieces, inp, cot = call(
-        front_kernel,
-        [piece] * 4 + [(HALF, 512)] * 2,
-        [SMEM] + [VMEM] * 6,
+    pieces = call(
+        cut_kernel,
+        [piece] * 4,
+        [SMEM] + [VMEM] * 3,
         place,
         gate_weight,
         up_weight,
         down_weight.T,
-        inputs,
-        cotangent,
-        came,
         scratch=[(NY, *piece)],
     )
-
     moved = exchange(pieces)
     (rows,) = call(
         join_kernel,
@@ -206,11 +228,15 @@
     )
     w_own = lax.all_gather(rows, "z", axis=0, tiled=False)
 
-    inp_near, cot_near = around(inp, "x"), around(cot, "y")
+    inp, cot = call(
+        pair_kernel, [(HALF, 512)] * 2, [SMEM] + [VMEM] * 3, place, inputs, cotangent, came
+    )
+    inp_near = around(inp, "x")
+    cot_near = around(cot, "y")
     inp_blocks = around_in_halves(jnp.stack(inp_near), "y")
     cot_blocks = around_in_halves(jnp.stack(cot_near), "x")
 
-    held = call(
+    (w_own,) = call(
         hold_kernel,
         [(NZ, COLS, 256)],
         [ANY] * 5,
@@ -220,33 +246,42 @@
         aliases={0: 0},
         out_specs=[ANY],
     )
-    w_own = held[0]
     w_other = lax.ppermute(w_own, "core", SWAP)
 
+    grads_shape = (NZ, COLS, 256)
+    hid_shape = (2, 3, ROWS, BLOCK)
     hid, grads_other, grads_own = call(
         main_kernel,
-        [(2, 3, ROWS, BLOCK), (NZ, COLS, 256), (NZ, COLS, 256)],
-        [SMEM] + [VMEM] * 12,
+        [hid_shape, grads_shape, grads_shape],
+        [SMEM] + [ANY] * 12,
         place,
         *inp_blocks,
         *cot_blocks,
         w_other,
         w_own,
-        scratch=[(2, ROWS, 2048), (COLS, 2048), (2, 3, BLOCK, ROWS)],
+        scratch=[
+            (2, ROWS, 2048),
+            (2, COLS, 2048),
+            (2, 3, BLOCK, ROWS),
+            hid_shape,
+            (2, *grads_shape),
+        ],
+        sems=[(2, 16), (2, NZ), (4,)],
+        out_specs=[ANY] * 3,
     )
     grads_came = lax.ppermute(grads_other, "core", SWAP)
     (partial,) = call(
         inputs_kernel, [(NY * NX, HALF, 512)], [VMEM] * 3, hid, w_other, w_own
     )
-    grads, partial = call(
-        add_kernel,
-        [(NZ, COLS, 256), (NY * NX, HALF, 512)],
-        [VMEM, VMEM, ANY],
-        grads_own,
-        grads_came,
+    grads = (grads_own.astype(jnp.float32) + grads_came.astype(jnp.float32)).astype(jnp.bfloat16)
+    (partial,) = call(
+        hold_kernel,
+        [(NY * NX, HALF, 512)],
+        [ANY] * 2,
         partial,
-        aliases={2: 1},
-        out_specs=[VMEM, ANY],
+        grads,
+        aliases={0: 0},
+        out_specs=[ANY],
     )
 
     summed = lax.psum_scatter(grads, "z", scatter_dimension=0, tiled=False)

time: 174 us -> 172 us (0.989)
  local copies, waits for them, and re-layouts: 10.8 us -> 7.87 us
  other arithmetic: 6.07 us -> 8.09 us
  starting transfers between devices: 30.4 us -> 28.6 us
    all_gather x1, waiting for transfers between devices: 13.1 us -> 6.91 us  [per_device(): w_own = lax.all_gather(rows, 'z', axis=0, tiled=False)]
    ppermute x1, waiting for transfers between devices: 0.01 us -> 4.45 us  [per_device(): grads_came = lax.ppermute(grads_other, 'core', SWAP)]
    convert_element_type x0 -> x1, other arithmetic: none -> 3.54 us  [per_device(): (grads_own.astype(jnp.float32) + grads_came.astype(jnp.float32)).astype(j...]
    ppermute x20, waiting for transfers between devices: 30 us -> 33.2 us  [shift(): lax.ppermute(array, axis, [(i, (i + by) % RING) for i in range(RING)])]
    unnamed x40 -> x36, local copies, waits for them, and re-layouts: 6.94 us -> 4 us
    ppermute x20, starting transfers between devices: 30 us -> 28.2 us  [shift(): lax.ppermute(array, axis, [(i, (i + by) % RING) for i in range(RING)])]
    pallas_call x8 -> x9, Pallas kernels: 31.9 us -> 32.1 us  [call(): pl.pallas_call(kernel, out_shape=[jax.ShapeDtypeStruct(s, dtype) for s in...]
  transfers between devices with their start and end apart: 26 -> 26, of which waited for: 18 -> 21; matrix products, arithmetic and copies ran while one was open for 5% -> 5% of each run, Pallas kernels for 4% -> 5%
where the time goes in v2:
time: 172 us; the launch traced here: 171 us
  waiting for transfers between devices  47.2 us (27%)
  blocking collectives  33.1 us (19%)
  Pallas kernels  32.1 us (19%)
  starting transfers between devices  28.6 us (17%)
  between operations  14.2 us (8%)
  other arithmetic  8.09 us (5%)
  local copies, waits for them, and re-layouts  7.87 us (5%)
    ppermute x20, waiting for transfers between devices, shift(): lax.ppermute(array, axis, [(i, (i + by) % RING) for i in range(RING)])  33.2 us
    all_to_all x1, blocking collectives, per_device(): lax.all_to_all(partial, ('y', 'x'), split_axis=0, concat_axis=0, tiled=True)  33.1 us
    pallas_call x9, Pallas kernels, call(): pl.pallas_call(kernel, out_shape=[jax.ShapeDtypeStruct(s, dtype) for s in...  32.1 us
    ppermute x20, starting transfers between devices, shift(): lax.ppermute(array, axis, [(i, (i + by) % RING) for i in range(RING)])  28.2 us
    all_gather x1, waiting for transfers between devices, per_device(): w_own = lax.all_gather(rows, 'z', axis=0, tiled=False)  6.91 us
    ppermute x1, waiting for transfers between devices, per_device(): grads_came = lax.ppermute(grads_other, 'core', SWAP)  4.45 us
    unnamed x36, local copies, waits for them, and re-layouts  4 us
    convert_element_type x1, other arithmetic, per_device(): (grads_own.astype(jnp.float32) + grads_came.astype(jnp.float32)).astype(j...  3.54 us
  transfers between devices with their start and end apart: 26, of which 21 were waited for; matrix products, arithmetic and copies ran while one was open for 5% of the time, Pallas kernels for 5%

profile of v2, /device:TPU:2, one launch (start us, length us, event | category | flops | bytes accessed | tf_op | source)
XLA Modules:
  0.0 171.2 jit_solution(912360588055574714)
XLA Ops:
  7.2 0.7 pad_add_fusion.place
  7.9 1.9 %shard_map.85 = (bf16[64,528]{1,0:T(8,128)(2,1)}, bf16[64,528]{1,0:T(8,128)(2,1)}, bf16[64,528]{1,0:T(8,128)(2,1)}, bf16[64,528]{1,0:T(8,128)(2,1)}) custom-call(s32[3]{0:T(128)} %pad_add_fusion.place, bf16[64,704]{1,0:T(8,128)(2,1)} %gate.1, bf16[64,704]{1,0:T(8,128)(2,1)} %up.1, bf16[64,704]{1,0:T(8,128)(2,1)} %bitcast.31), custom_call_target="tpu_custom_call" | custom-call | tf_op jit(solution)/shard_map/pallas_call | solution.py:30
  9.8 1.6 collective-permute-start.15
  11.3 1.7 collective-permute-start.16
  13.0 2.0 %collective-permute-start.17 = (bf16[64,528]{1,0:T(8,128)(2,1)}, bf16[64,528]{1,0:T(8,128)(2,1)S(1)}, u32[]{:S(2)}, u32[]{:S(2)}) collective-permute-start(bf16[64,528]{1,0:T(8,128)(2,1)} %get-tuple-element.25), channel_id=1, source_target_pairs={{0,16},{8,24},{16,0},{24,8},{1,17},{9,25},{17,1},{25,9},{2,18},{10... | collective-permute-start | bytes 202760 | tf_op jit(solution)/shard_map/ppermute | solution.py:43
  15.0 0.6 collective-permute-done.15.from_prev
  15.6 0.6 collective-permute-done.16.from_next
  16.3 2.9 %collective-permute-done.17.from_far = bf16[64,528]{1,0:T(8,128)(2,1)S(1)} collective-permute-done((bf16[64,528]{1,0:T(8,128)(2,1)}, bf16[64,528]{1,0:T(8,128)(2,1)S(1)}, u32[]{:S(2)}, u32[]{:S(2)}) %collective-permute-start.17) | collective-permute-done | bytes 67616 | tf_op jit(solution)/shard_map/ppermute | solution.py:43
  19.2 0.6 copy-done.17
  19.8 1.9 %shard_map.86 = bf16[528,256]{1,0:T(8,128)(2,1)} custom-call(s32[3]{0:T(128)} %pad_add_fusion.place, bf16[64,528]{1,0:T(8,128)(2,1)} %get-tuple-element.22.kept, bf16[64,528]{1,0:T(8,128)(2,1)} %copy-done.15, bf16[64,528]{1,0:T(8,128)(2,1)} %copy-done.16, bf16[64,528]{1,0:T(8,128)(2,1)} %copy-done.17), custom_call_target="tpu_custom_call" | custom-call | tf_op jit(solution)/shard_map/pallas_call | solution.py:30
  21.8 1.0 fusion.2
  22.7 0.1 collective-permute-start
  22.8 1.3 collective-permute-done.came
  24.2 0.7 copy-done.11
  24.8 1.8 %shard_map.84 = (bf16[128,512]{1,0:T(8,128)(2,1)}, bf16[128,512]{1,0:T(8,128)(2,1)}) custom-call(s32[3]{0:T(128)} %pad_add_fusion.place, bf16[256,256]{1,0:T(8,128)(2,1)} %inputs.1, bf16[256,256]{1,0:T(8,128)(2,1)} %cotangent.1, bf16[2,128,256]{2,1,0:T(8,128)(2,1)} %copy-done.11), custom_call_target="tpu_custom_call" | custom-call | tf_op jit(solution)/shard_map/pallas_call | solution.py:30
  26.6 2.0 %collective-permute-start.10 = (bf16[128,512]{1,0:T(8,128)(2,1)}, bf16[128,512]{1,0:T(8,128)(2,1)S(1)}, u32[]{:S(2)}, u32[]{:S(2)}) collective-permute-start(bf16[128,512]{1,0:T(8,128)(2,1)} %get-tuple-element.21), channel_id=1, source_target_pairs={{0,16},{8,24},{16,0},{24,8},{1,17},{9,25},{17,1},{25,9},{2,18},{10... | collective-permute-start | bytes 393224 | tf_op jit(solution)/shard_map/ppermute | solution.py:43
  28.6 1.1 collective-permute-start.9
  29.7 0.9 collective-permute-start.8
  30.6 2.1 %collective-permute-start.3 = (bf16[128,512]{1,0:T(8,128)(2,1)}, bf16[128,512]{1,0:T(8,128)(2,1)S(1)}, u32[]{:S(2)}, u32[]{:S(2)}) collective-permute-start(bf16[128,512]{1,0:T(8,128)(2,1)} %get-tuple-element.20), channel_id=1, source_target_pairs={{0,4},{2,6},{4,0},{6,2},{1,5},{3,7},{5,1},{7,3},{8,12},{10,14},{12... | collective-permute-start | bytes 393224 | tf_op jit(solution)/shard_map/ppermute | solution.py:43
  32.7 1.4 collective-permute-start.2
  34.2 0.5 collective-permute-done.10
  34.7 1.5 collective-permute-start.1
  36.2 0.6 collective-permute-done.8
  36.8 1.0 pad_maximum_fusion.1.refs_5_
  37.8 2.2 %collective-permute-start.12 = (bf16[4,128,512]{2,1,0:T(8,128)(2,1)S(1)}, bf16[4,128,512]{2,1,0:T(8,128)(2,1)S(1)}, u32[]{:S(2)}, u32[]{:S(2)}) collective-permute-start(bf16[4,128,512]{2,1,0:T(8,128)(2,1)S(1)} %pad_maximum_fusion.1.refs_5_), channel_id=1, source_target_pairs={{0,6},{2,0},{4,2},{6,4},{1,7},{3,1},{5,3},{7,5},{8,14},{10,8},{12,... | collective-permute-start | bytes 1572872 | tf_op jit(solution)/shard_map/ppermute | solution.py:43
  40.0 0.1 collective-permute-done.1
  40.1 1.0 pad_maximum_fusion.refs_0_
  41.1 2.2 %collective-permute-start.5 = (bf16[4,128,512]{2,1,0:T(8,128)(2,1)S(1)}, bf16[4,128,512]{2,1,0:T(8,128)(2,1)S(1)}, u32[]{:S(2)}, u32[]{:S(2)}) collective-permute-start(bf16[4,128,512]{2,1,0:T(8,128)(2,1)S(1)} %pad_maximum_fusion.refs_0_), channel_id=1, source_target_pairs={{0,24},{8,0},{16,8},{24,16},{1,25},{9,1},{17,9},{25,17},{2,26},{10... | collective-permute-start | bytes 1572872 | tf_op jit(solution)/shard_map/ppermute | solution.py:43
  43.3 8.0 %collective-permute-done.12.refs_4_.refs_7_ = bf16[4,128,512]{2,1,0:T(8,128)(2,1)S(1)} collective-permute-done((bf16[4,128,512]{2,1,0:T(8,128)(2,1)S(1)}, bf16[4,128,512]{2,1,0:T(8,128)(2,1)S(1)}, u32[]{:S(2)}, u32[]{:S(2)}) %collective-permute-start.12) | collective-permute-done | bytes 524320 | tf_op jit(solution)/shard_map/ppermute | solution.py:43
  51.3 2.2 %collective-permute-done.11.refs_3_.refs_6_ = bf16[4,128,512]{2,1,0:T(8,128)(2,1)S(1)} collective-permute-done((bf16[4,128,512]{2,1,0:T(8,128)(2,1)S(1)}, bf16[4,128,512]{2,1,0:T(8,128)(2,1)S(1)}, u32[]{:S(2)}, u32[]{:S(2)}) %collective-permute-start.11) | collective-permute-done | bytes 524320 | tf_op jit(solution)/shard_map/ppermute | solution.py:43
  53.5 1.1 collective-permute-done.5.refs_2_
  54.6 3.0 %collective-permute-done.4.refs_1_ = bf16[4,128,512]{2,1,0:T(8,128)(2,1)S(1)} collective-permute-done((bf16[4,128,512]{2,1,0:T(8,128)(2,1)S(1)}, bf16[4,128,512]{2,1,0:T(8,128)(2,1)S(1)}, u32[]{:S(2)}, u32[]{:S(2)}) %collective-permute-start.4) | collective-permute-done | bytes 524320 | tf_op jit(solution)/shard_map/ppermute | solution.py:43
  57.6 6.9 %all-gather.3.cloned.1.call-done = bf16[4224,256]{1,0:T(8,128)(2,1)} async-done(((bf16[528,256]{1,0:T(8,128)(2,1)}), bf16[4224,256]{1,0:T(8,128)(2,1)}) %all-gather.3.cloned.1.call-update) | async-done | bytes 2162704 | tf_op jit(solution)/shard_map/all_gather | solution.py:229
  64.7 1.0 slice.37
  65.7 0.6 collective-permute-start.14
  66.2 1.0 slice.36
  67.2 1.8 %collective-permute-start.13 = (bf16[2,128,512]{2,1,0:T(8,128)(2,1)S(1)}, bf16[2,128,512]{2,1,0:T(8,128)(2,1)S(1)}, u32[]{:S(2)}, u32[]{:S(2)}) collective-permute-start(bf16[2,128,512]{2,1,0:T(8,128)(2,1)S(1)} %slice.36), channel_id=1, source_target_pairs={{0,2},{2,4},{4,6},{6,0},{1,3},{3,5},{5,7},{7,1},{8,10},{10,12},{12... | collective-permute-start | bytes 786440 | tf_op jit(solution)/shard_map/ppermute | solution.py:43
  69.0 1.0 slice.35
  70.0 2.7 %collective-permute-start.7 = (bf16[2,128,512]{2,1,0:T(8,128)(2,1)S(1)}, bf16[2,128,512]{2,1,0:T(8,128)(2,1)S(1)}, u32[]{:S(2)}, u32[]{:S(2)}) collective-permute-start(bf16[2,128,512]{2,1,0:T(8,128)(2,1)S(1)} %slice.35), channel_id=1, source_target_pairs={{0,24},{8,0},{16,8},{24,16},{1,25},{9,1},{17,9},{25,17},{2,26},{10... | collective-permute-start | bytes 786440 | tf_op jit(solution)/shard_map/ppermute | solution.py:43
  72.7 1.0 slice.34
  73.7 0.7 collective-permute-done.14.refs_9_
  74.5 2.4 %collective-permute-done.13.refs_8_ = bf16[2,128,512]{2,1,0:T(8,128)(2,1)S(1)} collective-permute-done((bf16[2,128,512]{2,1,0:T(8,128)(2,1)S(1)}, bf16[2,128,512]{2,1,0:T(8,128)(2,1)S(1)}, u32[]{:S(2)}, u32[]{:S(2)}) %collective-permute-start.13) | collective-permute-done | bytes 262176 | tf_op jit(solution)/shard_map/ppermute | solution.py:43
  76.9 1.5 collective-permute-done.7.refs_4_
  78.3 4.5 %collective-permute-done.6.refs_3_ = bf16[2,128,512]{2,1,0:T(8,128)(2,1)S(1)} collective-permute-done((bf16[2,128,512]{2,1,0:T(8,128)(2,1)S(1)}, bf16[2,128,512]{2,1,0:T(8,128)(2,1)S(1)}, u32[]{:S(2)}, u32[]{:S(2)}) %collective-permute-start.6) | collective-permute-done | bytes 262176 | tf_op jit(solution)/shard_map/ppermute | solution.py:43
  82.8 0.7 copy-done.10
  83.5 1.4 copy-done
  84.9 16.3 %shard_map.88 = (bf16[2,3,512,176]{3,2,1,0:T(8,128)(2,1)}, bf16[8,528,256]{2,1,0:T(8,128)(2,1)}, bf16[8,528,256]{2,1,0:T(8,128)(2,1)}) custom-call(s32[3]{0:T(128)} %pad_add_fusion.place, bf16[4,128,512]{2,1,0:T(8,128)(2,1)} %copy-done.6, bf16[4,128,512]{2,1,0:T(8,128)(2,1)} %copy-done.4, bf16[4,128,512]{2,1,0:T(8,128)(2,1)} %copy-done.3, ...), custom_call_target="tpu_custom_call" | custom-call | tf_op jit(solution)/shard_map/pallas_call | solution.py:30
  101.3 4.5 %collective-permute-done.19 = bf16[8,528,256]{2,1,0:T(8,128)(2,1)S(1)} collective-permute-done((bf16[8,528,256]{2,1,0:T(8,128)(2,1)}, bf16[8,528,256]{2,1,0:T(8,128)(2,1)S(1)}, u32[]{:S(2)}, u32[]{:S(2)}) %collective-permute-start.19) | collective-permute-done | bytes 2162720 | tf_op jit(solution)/shard_map/ppermute | solution.py:272
  105.7 3.5 %add_convert_fusion.refs_1_ = bf16[8,528,256]{2,1,0:T(8,128)(2,1)} fusion(bf16[8,528,256]{2,1,0:T(8,128)(2,1)S(1)} %collective-permute-done.19, bf16[8,528,256]{2,1,0:T(8,128)(2,1)} %get-tuple-element.27), kind=kLoop, calls=%fused_computation | loop fusion | flops 4325376 | bytes 6488064 | tf_op jit(solution)/shard_map/convert_element_type | solution.py:276
  109.3 6.4 %shard_map.89.refs_0_ = bf16[16,128,512]{2,1,0:T(8,128)(2,1)} custom-call(bf16[2,3,512,176]{3,2,1,0:T(8,128)(2,1)} %get-tuple-element.26.hid, bf16[8,528,256]{2,1,0:T(8,128)(2,1)} %copy-done, bf16[8,528,256]{2,1,0:T(8,128)(2,1)} %shard_map.87.refs_11_.weights_b), custom_call_target="tpu_custom_call" | custom-call | tf_op jit(solution)/shard_map/pallas_call | solution.py:30
  115.7 33.1 %all_to_all.5 = bf16[16,128,512]{2,1,0:T(8,128)(2,1)S(1)} all-to-all(bf16[16,128,512]{2,1,0:T(8,128)(2,1)} %shard_map.90), channel_id=1, replica_groups=mesh['z'=8,'y'=4,'x'=4,'core'=2] {'y','x'}, dimensions={0} | all-to-all | bytes 4194304 | tf_op jit(solution)/shard_map/all_to_all | solution.py:301
  148.8 0.3 reduce_sum.12
  149.1 0.1 collective-permute-start.20
  149.2 1.2 collective-permute-done.20
  150.5 1.8 %shard_map.91 = (bf16[64,528]{1,0:T(8,128)(2,1)}, bf16[64,528]{1,0:T(8,128)(2,1)}, bf16[64,528]{1,0:T(8,128)(2,1)}, bf16[64,528]{1,0:T(8,128)(2,1)}) custom-call(s32[3]{0:T(128)} %pad_add_fusion.place, bf16[528,256]{1,0:T(8,128)(2,1)} %bitcast.22), custom_call_target="tpu_custom_call" | custom-call | tf_op jit(solution)/shard_map/pallas_call | solution.py:30
  152.3 0.8 collective-permute-start.21
  153.1 2.4 %collective-permute-start.22 = (bf16[64,528]{1,0:T(8,128)(2,1)}, bf16[64,528]{1,0:T(8,128)(2,1)S(1)}, u32[]{:S(2)}, u32[]{:S(2)}) collective-permute-start(bf16[64,528]{1,0:T(8,128)(2,1)} %get-tuple-element.31), channel_id=1, source_target_pairs={{0,24},{8,0},{16,8},{24,16},{1,25},{9,1},{17,9},{25,17},{2,26},{10... | collective-permute-start | bytes 202760 | tf_op jit(solution)/shard_map/ppermute | solution.py:43
  155.6 1.1 collective-permute-start.23
  156.6 0.7 pad_maximum_fusion.3
  157.3 0.9 collective-permute-done.21.from_prev
  158.3 1.2 collective-permute-done.22.from_next
  159.4 2.3 %collective-permute-done.23.from_far = bf16[64,528]{1,0:T(8,128)(2,1)S(1)} collective-permute-done((bf16[64,528]{1,0:T(8,128)(2,1)}, bf16[64,528]{1,0:T(8,128)(2,1)S(1)}, u32[]{:S(2)}, u32[]{:S(2)}) %collective-permute-start.23) | collective-permute-done | bytes 67616 | tf_op jit(solution)/shard_map/ppermute | solution.py:43
  161.7 0.6 copy-done.14
  162.4 2.0 %shard_map.92 = (f32[64,704]{1,0:T(8,128)}, f32[64,704]{1,0:T(8,128)}, f32[64,704]{1,0:T(8,128)}) custom-call(s32[3]{0:T(128)} %pad_add_fusion.place, bf16[64,528]{1,0:T(8,128)(2,1)} %get-tuple-element.29.kept, bf16[64,528]{1,0:T(8,128)(2,1)} %copy-done.12, bf16[64,528]{1,0:T(8,128)(2,1)} %copy-done.13, bf16[64,528]{1,0:T(8,128)(2,1)} %copy-done.14), custom_call_target="tpu_custom_call" | custom-call | tf_op jit(solution)/shard_map/pallas_call | solution.py:30
  (49 shorter events, 0.5 us)
Async XLA Ops:
  7.2 57.4 %all-gather.3.cloned.1.call-start = ((), (), s32[]{:S(2)}) async-start(), calls=%async_computation.3 | async-start | bytes 2433024 | tf_op jit(solution)/shard_map/all_gather | solution.py:229
  9.8 5.9 %collective-permute-start.15 = (bf16[64,528]{1,0:T(8,128)(2,1)}, bf16[64,528]{1,0:T(8,128)(2,1)S(1)}, u32[]{:S(2)}, u32[]{:S(2)}) collective-permute-start(bf16[64,528]{1,0:T(8,128)(2,1)} %get-tuple-element.23), channel_id=1, source_target_pairs={{0,8},{8,16},{16,24},{24,0},{1,9},{9,17},{17,25},{25,1},{2,10},{10... | collective-permute-start | bytes 202760 | tf_op jit(solution)/shard_map/ppermute | solution.py:43
  11.3 4.9 %collective-permute-start.16 = (bf16[64,528]{1,0:T(8,128)(2,1)}, bf16[64,528]{1,0:T(8,128)(2,1)S(1)}, u32[]{:S(2)}, u32[]{:S(2)}) collective-permute-start(bf16[64,528]{1,0:T(8,128)(2,1)} %get-tuple-element.24), channel_id=1, source_target_pairs={{0,24},{8,0},{16,8},{24,16},{1,25},{9,1},{17,9},{25,17},{2,26},{10... | collective-permute-start | bytes 202760 | tf_op jit(solution)/shard_map/ppermute | solution.py:43
  13.0 6.2 %collective-permute-start.17 = (bf16[64,528]{1,0:T(8,128)(2,1)}, bf16[64,528]{1,0:T(8,128)(2,1)S(1)}, u32[]{:S(2)}, u32[]{:S(2)}) collective-permute-start(bf16[64,528]{1,0:T(8,128)(2,1)} %get-tuple-element.25), channel_id=1, source_target_pairs={{0,16},{8,24},{16,0},{24,8},{1,17},{9,25},{17,1},{25,9},{2,18},{10... | collective-permute-start | bytes 202760 | tf_op jit(solution)/shard_map/ppermute | solution.py:43
  15.6 3.5 %copy-start.15 = (bf16[64,528]{1,0:T(8,128)(2,1)}, bf16[64,528]{1,0:T(8,128)(2,1)S(1)}, u32[]{:S(2)}) copy-start(bf16[64,528]{1,0:T(8,128)(2,1)S(1)} %collective-permute-done.15.from_prev) | copy-start | bytes 202756
  16.3 2.9 %copy-start.16 = (bf16[64,528]{1,0:T(8,128)(2,1)}, bf16[64,528]{1,0:T(8,128)(2,1)S(1)}, u32[]{:S(2)}) copy-start(bf16[64,528]{1,0:T(8,128)(2,1)S(1)} %collective-permute-done.16.from_next) | copy-start | bytes 202756
  19.1 0.6 copy-start.17
  21.7 128.8 %reduce-scatter.2.cloned.1.call-start = ((), (), s32[]{:S(2)}) async-start(), calls=%async_computation.2 | async-start | bytes 2433024 | tf_op jit(solution)/shard_map/reduce_scatter | solution.py:287
  22.7 1.4 collective-permute-start
  24.2 0.7 copy-start.11
  26.6 8.1 %collective-permute-start.10 = (bf16[128,512]{1,0:T(8,128)(2,1)}, bf16[128,512]{1,0:T(8,128)(2,1)S(1)}, u32[]{:S(2)}, u32[]{:S(2)}) collective-permute-start(bf16[128,512]{1,0:T(8,128)(2,1)} %get-tuple-element.21), channel_id=1, source_target_pairs={{0,16},{8,24},{16,0},{24,8},{1,17},{9,25},{17,1},{25,9},{2,18},{10... | collective-permute-start | bytes 393224 | tf_op jit(solution)/shard_map/ppermute | solution.py:43
  28.6 7.6 %collective-permute-start.9 = (bf16[128,512]{1,0:T(8,128)(2,1)}, bf16[128,512]{1,0:T(8,128)(2,1)S(1)}, u32[]{:S(2)}, u32[]{:S(2)}) collective-permute-start(bf16[128,512]{1,0:T(8,128)(2,1)} %get-tuple-element.21), channel_id=1, source_target_pairs={{0,24},{8,0},{16,8},{24,16},{1,25},{9,1},{17,9},{25,17},{2,26},{10... | collective-permute-start | bytes 393224 | tf_op jit(solution)/shard_map/ppermute | solution.py:43
  29.7 7.1 %collective-permute-start.8 = (bf16[128,512]{1,0:T(8,128)(2,1)}, bf16[128,512]{1,0:T(8,128)(2,1)S(1)}, u32[]{:S(2)}, u32[]{:S(2)}) collective-permute-start(bf16[128,512]{1,0:T(8,128)(2,1)} %get-tuple-element.21), channel_id=1, source_target_pairs={{0,8},{8,16},{16,24},{24,0},{1,9},{9,17},{17,25},{25,1},{2,10},{10... | collective-permute-start | bytes 393224 | tf_op jit(solution)/shard_map/ppermute | solution.py:43
  30.6 9.4 %collective-permute-start.3 = (bf16[128,512]{1,0:T(8,128)(2,1)}, bf16[128,512]{1,0:T(8,128)(2,1)S(1)}, u32[]{:S(2)}, u32[]{:S(2)}) collective-permute-start(bf16[128,512]{1,0:T(8,128)(2,1)} %get-tuple-element.20), channel_id=1, source_target_pairs={{0,4},{2,6},{4,0},{6,2},{1,5},{3,7},{5,1},{7,3},{8,12},{10,14},{12... | collective-permute-start | bytes 393224 | tf_op jit(solution)/shard_map/ppermute | solution.py:43
  32.7 7.2 %collective-permute-start.2 = (bf16[128,512]{1,0:T(8,128)(2,1)}, bf16[128,512]{1,0:T(8,128)(2,1)S(1)}, u32[]{:S(2)}, u32[]{:S(2)}) collective-permute-start(bf16[128,512]{1,0:T(8,128)(2,1)} %get-tuple-element.20), channel_id=1, source_target_pairs={{0,6},{2,0},{4,2},{6,4},{1,7},{3,1},{5,3},{7,5},{8,14},{10,8},{12,... | collective-permute-start | bytes 393224 | tf_op jit(solution)/shard_map/ppermute | solution.py:43
  34.7 5.4 %collective-permute-start.1 = (bf16[128,512]{1,0:T(8,128)(2,1)}, bf16[128,512]{1,0:T(8,128)(2,1)S(1)}, u32[]{:S(2)}, u32[]{:S(2)}) collective-permute-start(bf16[128,512]{1,0:T(8,128)(2,1)} %get-tuple-element.20), channel_id=1, source_target_pairs={{0,2},{2,4},{4,6},{6,0},{1,3},{3,5},{5,7},{7,1},{8,10},{10,12},{12... | collective-permute-start | bytes 393224 | tf_op jit(solution)/shard_map/ppermute | solution.py:43
  37.8 26.8 %copy-start.5 = (bf16[4,128,512]{2,1,0:T(8,128)(2,1)}, bf16[4,128,512]{2,1,0:T(8,128)(2,1)S(1)}, u32[]{:S(2)}) copy-start(bf16[4,128,512]{2,1,0:T(8,128)(2,1)S(1)} %pad_maximum_fusion.1.refs_5_) | copy-start | bytes 1572868
  37.8 13.6 %collective-permute-start.12 = (bf16[4,128,512]{2,1,0:T(8,128)(2,1)S(1)}, bf16[4,128,512]{2,1,0:T(8,128)(2,1)S(1)}, u32[]{:S(2)}, u32[]{:S(2)}) collective-permute-start(bf16[4,128,512]{2,1,0:T(8,128)(2,1)S(1)} %pad_maximum_fusion.1.refs_5_), channel_id=1, source_target_pairs={{0,6},{2,0},{4,2},{6,4},{1,7},{3,1},{5,3},{7,5},{8,14},{10,8},{12,... | collective-permute-start | bytes 1572872 | tf_op jit(solution)/shard_map/ppermute | solution.py:43
  40.0 13.6 %collective-permute-start.11 = (bf16[4,128,512]{2,1,0:T(8,128)(2,1)S(1)}, bf16[4,128,512]{2,1,0:T(8,128)(2,1)S(1)}, u32[]{:S(2)}, u32[]{:S(2)}) collective-permute-start(bf16[4,128,512]{2,1,0:T(8,128)(2,1)S(1)} %pad_maximum_fusion.1.refs_5_), channel_id=1, source_target_pairs={{0,2},{2,4},{4,6},{6,0},{1,3},{3,5},{5,7},{7,1},{8,10},{10,12},{12... | collective-permute-start | bytes 1572872 | tf_op jit(solution)/shard_map/ppermute | solution.py:43
  41.1 23.5 %copy-start.6 = (bf16[4,128,512]{2,1,0:T(8,128)(2,1)}, bf16[4,128,512]{2,1,0:T(8,128)(2,1)S(1)}, u32[]{:S(2)}) copy-start(bf16[4,128,512]{2,1,0:T(8,128)(2,1)S(1)} %pad_maximum_fusion.refs_0_) | copy-start | bytes 1572868
  41.1 13.5 %collective-permute-start.5 = (bf16[4,128,512]{2,1,0:T(8,128)(2,1)S(1)}, bf16[4,128,512]{2,1,0:T(8,128)(2,1)S(1)}, u32[]{:S(2)}, u32[]{:S(2)}) collective-permute-start(bf16[4,128,512]{2,1,0:T(8,128)(2,1)S(1)} %pad_maximum_fusion.refs_0_), channel_id=1, source_target_pairs={{0,24},{8,0},{16,8},{24,16},{1,25},{9,1},{17,9},{25,17},{2,26},{10... | collective-permute-start | bytes 1572872 | tf_op jit(solution)/shard_map/ppermute | solution.py:43
  43.3 14.3 %collective-permute-start.4 = (bf16[4,128,512]{2,1,0:T(8,128)(2,1)S(1)}, bf16[4,128,512]{2,1,0:T(8,128)(2,1)S(1)}, u32[]{:S(2)}, u32[]{:S(2)}) collective-permute-start(bf16[4,128,512]{2,1,0:T(8,128)(2,1)S(1)} %pad_maximum_fusion.refs_0_), channel_id=1, source_target_pairs={{0,8},{8,16},{16,24},{24,0},{1,9},{9,17},{17,25},{25,1},{2,10},{10... | collective-permute-start | bytes 1572872 | tf_op jit(solution)/shard_map/ppermute | solution.py:43
  51.3 13.2 %copy-start.1 = (bf16[4,128,512]{2,1,0:T(8,128)(2,1)}, bf16[4,128,512]{2,1,0:T(8,128)(2,1)S(1)}, u32[]{:S(2)}) copy-start(bf16[4,128,512]{2,1,0:T(8,128)(2,1)S(1)} %collective-permute-done.12.refs_4_.refs_7_) | copy-start | bytes 1572868
  53.5 11.0 %copy-start.2 = (bf16[4,128,512]{2,1,0:T(8,128)(2,1)}, bf16[4,128,512]{2,1,0:T(8,128)(2,1)S(1)}, u32[]{:S(2)}) copy-start(bf16[4,128,512]{2,1,0:T(8,128)(2,1)S(1)} %collective-permute-done.11.refs_3_.refs_6_) | copy-start | bytes 1572868
  54.6 9.9 %copy-start.3 = (bf16[4,128,512]{2,1,0:T(8,128)(2,1)}, bf16[4,128,512]{2,1,0:T(8,128)(2,1)S(1)}, u32[]{:S(2)}) copy-start(bf16[4,128,512]{2,1,0:T(8,128)(2,1)S(1)} %collective-permute-done.5.refs_2_) | copy-start | bytes 1572868
  57.6 6.9 %copy-start.4 = (bf16[4,128,512]{2,1,0:T(8,128)(2,1)}, bf16[4,128,512]{2,1,0:T(8,128)(2,1)S(1)}, u32[]{:S(2)}) copy-start(bf16[4,128,512]{2,1,0:T(8,128)(2,1)S(1)} %collective-permute-done.4.refs_1_) | copy-start | bytes 1572868
  64.6 18.2 %collective-permute-start.18 = (bf16[8,528,256]{2,1,0:T(8,128)(2,1)}, bf16[8,528,256]{2,1,0:T(8,128)(2,1)S(1)}, u32[]{:S(2)}, u32[]{:S(2)}) collective-permute-start(bf16[8,528,256]{2,1,0:T(8,128)(2,1)} %shard_map.87.refs_11_.weights_b), channel_id=1, source_target_pairs={{0,1},{1,0},{2,3},{3,2},{4,5},{5,4},{6,7},{7,6},{8,9},{9,8},{10,11... | collective-permute-start | bytes 6488072 | tf_op jit(solution)/shard_map/ppermute | solution.py:249
  65.7 8.8 %collective-permute-start.14 = (bf16[2,128,512]{2,1,0:T(8,128)(2,1)S(1)}, bf16[2,128,512]{2,1,0:T(8,128)(2,1)S(1)}, u32[]{:S(2)}, u32[]{:S(2)}) collective-permute-start(bf16[2,128,512]{2,1,0:T(8,128)(2,1)S(1)} %slice.37), channel_id=1, source_target_pairs={{0,6},{2,0},{4,2},{6,4},{1,7},{3,1},{5,3},{7,5},{8,14},{10,8},{12,... | collective-permute-start | bytes 786440 | tf_op jit(solution)/shard_map/ppermute | solution.py:43
  67.2 9.7 %collective-permute-start.13 = (bf16[2,128,512]{2,1,0:T(8,128)(2,1)S(1)}, bf16[2,128,512]{2,1,0:T(8,128)(2,1)S(1)}, u32[]{:S(2)}, u32[]{:S(2)}) collective-permute-start(bf16[2,128,512]{2,1,0:T(8,128)(2,1)S(1)} %slice.36), channel_id=1, source_target_pairs={{0,2},{2,4},{4,6},{6,0},{1,3},{3,5},{5,7},{7,1},{8,10},{10,12},{12... | collective-permute-start | bytes 786440 | tf_op jit(solution)/shard_map/ppermute | solution.py:43
  70.0 8.4 %collective-permute-start.7 = (bf16[2,128,512]{2,1,0:T(8,128)(2,1)S(1)}, bf16[2,128,512]{2,1,0:T(8,128)(2,1)S(1)}, u32[]{:S(2)}, u32[]{:S(2)}) collective-permute-start(bf16[2,128,512]{2,1,0:T(8,128)(2,1)S(1)} %slice.35), channel_id=1, source_target_pairs={{0,24},{8,0},{16,8},{24,16},{1,25},{9,1},{17,9},{25,17},{2,26},{10... | collective-permute-start | bytes 786440 | tf_op jit(solution)/shard_map/ppermute | solution.py:43
  73.7 9.2 %collective-permute-start.6 = (bf16[2,128,512]{2,1,0:T(8,128)(2,1)S(1)}, bf16[2,128,512]{2,1,0:T(8,128)(2,1)S(1)}, u32[]{:S(2)}, u32[]{:S(2)}) collective-permute-start(bf16[2,128,512]{2,1,0:T(8,128)(2,1)S(1)} %slice.34), channel_id=1, source_target_pairs={{0,8},{8,16},{16,24},{24,0},{1,9},{9,17},{17,25},{25,1},{2,10},{10... | collective-permute-start | bytes 786440 | tf_op jit(solution)/shard_map/ppermute | solution.py:43
  74.5 8.4 %copy-start.7 = (bf16[2,128,512]{2,1,0:T(8,128)(2,1)}, bf16[2,128,512]{2,1,0:T(8,128)(2,1)S(1)}, u32[]{:S(2)}) copy-start(bf16[2,128,512]{2,1,0:T(8,128)(2,1)S(1)} %collective-permute-done.14.refs_9_) | copy-start | bytes 786436
  76.9 5.9 %copy-start.8 = (bf16[2,128,512]{2,1,0:T(8,128)(2,1)}, bf16[2,128,512]{2,1,0:T(8,128)(2,1)S(1)}, u32[]{:S(2)}) copy-start(bf16[2,128,512]{2,1,0:T(8,128)(2,1)S(1)} %collective-permute-done.13.refs_8_) | copy-start | bytes 786436
  78.3 4.5 %copy-start.9 = (bf16[2,128,512]{2,1,0:T(8,128)(2,1)}, bf16[2,128,512]{2,1,0:T(8,128)(2,1)S(1)}, u32[]{:S(2)}) copy-start(bf16[2,128,512]{2,1,0:T(8,128)(2,1)S(1)} %collective-permute-done.7.refs_4_) | copy-start | bytes 786436
  82.8 0.7 copy-start.10
  83.5 1.4 copy-start
  101.2 4.6 %collective-permute-start.19 = (bf16[8,528,256]{2,1,0:T(8,128)(2,1)}, bf16[8,528,256]{2,1,0:T(8,128)(2,1)S(1)}, u32[]{:S(2)}, u32[]{:S(2)}) collective-permute-start(bf16[8,528,256]{2,1,0:T(8,128)(2,1)} %get-tuple-element.28), channel_id=1, source_target_pairs={{0,1},{1,0},{2,3},{3,2},{4,5},{5,4},{6,7},{7,6},{8,9},{9,8},{10,11... | collective-permute-start | bytes 6488072 | tf_op jit(solution)/shard_map/ppermute | solution.py:272
  149.1 1.3 collective-permute-start.20
  152.3 5.9 %collective-permute-start.21 = (bf16[64,528]{1,0:T(8,128)(2,1)}, bf16[64,528]{1,0:T(8,128)(2,1)S(1)}, u32[]{:S(2)}, u32[]{:S(2)}) collective-permute-start(bf16[64,528]{1,0:T(8,128)(2,1)} %get-tuple-element.30), channel_id=1, source_target_pairs={{0,8},{8,16},{16,24},{24,0},{1,9},{9,17},{17,25},{25,1},{2,10},{10... | collective-permute-start | bytes 202760 | tf_op jit(solution)/shard_map/ppermute | solution.py:43
  153.1 6.3 %collective-permute-start.22 = (bf16[64,528]{1,0:T(8,128)(2,1)}, bf16[64,528]{1,0:T(8,128)(2,1)S(1)}, u32[]{:S(2)}, u32[]{:S(2)}) collective-permute-start(bf16[64,528]{1,0:T(8,128)(2,1)} %get-tuple-element.31), channel_id=1, source_target_pairs={{0,24},{8,0},{16,8},{24,16},{1,25},{9,1},{17,9},{25,17},{2,26},{10... | collective-permute-start | bytes 202760 | tf_op jit(solution)/shard_map/ppermute | solution.py:43
  155.6 6.2 %collective-permute-start.23 = (bf16[64,528]{1,0:T(8,128)(2,1)}, bf16[64,528]{1,0:T(8,128)(2,1)S(1)}, u32[]{:S(2)}, u32[]{:S(2)}) collective-permute-start(bf16[64,528]{1,0:T(8,128)(2,1)} %get-tuple-element.32), channel_id=1, source_target_pairs={{0,16},{8,24},{16,0},{24,8},{1,17},{9,25},{17,1},{25,9},{2,18},{10... | collective-permute-start | bytes 202760 | tf_op jit(solution)/shard_map/ppermute | solution.py:43
  158.2 3.5 %copy-start.12 = (bf16[64,528]{1,0:T(8,128)(2,1)}, bf16[64,528]{1,0:T(8,128)(2,1)S(1)}, u32[]{:S(2)}) copy-start(bf16[64,528]{1,0:T(8,128)(2,1)S(1)} %collective-permute-done.21.from_prev) | copy-start | bytes 202756
  159.4 2.3 %copy-start.13 = (bf16[64,528]{1,0:T(8,128)(2,1)}, bf16[64,528]{1,0:T(8,128)(2,1)S(1)}, u32[]{:S(2)}) copy-start(bf16[64,528]{1,0:T(8,128)(2,1)S(1)} %collective-permute-done.22.from_next) | copy-start | bytes 202756
  161.7 0.6 copy-start.14
Sparse Core Ops, SparseCore 0:
  21.8 42.6 all-gather.2
  109.4 40.4 reduce-scatter.1

commit v3 on v1

v3 whole, which is shorter than its diff:
```python
import jax
import jax.numpy as jnp
from jax import lax
from jax.experimental import pallas as pl
from jax.experimental.pallas import tpu as pltpu
from jax.sharding import Mesh
from jax.sharding import PartitionSpec as P


NZ, NY, NX = 8, 4, 4
RING = 4
BLOCK = 176
COLS = 3 * BLOCK
HALF = 128
ROWS = NY * HALF
SWAP = [(0, 1), (1, 0)]
ORDER = (0, -1, 1, 2)
VMEM = pl.BlockSpec(memory_space=pltpu.VMEM)
SMEM = pl.BlockSpec(memory_space=pltpu.SMEM)


def dot(left, right, dims):
    return lax.dot_general(
        left, right, (dims, ((), ())), preferred_element_type=jnp.float32
    )


def call(kernel, outs, specs, *args, dtype=jnp.bfloat16, scratch=()):
    return pl.pallas_call(
        kernel,
        out_shape=[jax.ShapeDtypeStruct(s, dtype) for s in outs],
        in_specs=specs,
        out_specs=[VMEM] * len(outs),
        scratch_shapes=[pltpu.VMEM(s, jnp.bfloat16) for s in scratch],
        compiler_params=pltpu.CompilerParams(vmem_limit_bytes=24 * 1024 * 1024),
    )(*args)


def shift(array, axis, by):
    return lax.ppermute(array, axis, [(i, (i + by) % RING) for i in range(RING)])


def around(own, axis):
    return own, shift(own, axis, 1), shift(own, axis, -1), shift(own, axis, 2)


def around_in_halves(own, axis):
    low, high = shift(own, axis, 1), shift(own, axis, -1)
    far_first = shift(low[:2], axis, 1)
    far_last = shift(high[2:], axis, -1)
    return own, low, high, far_first, far_last


def cut_kernel(place, gate, up, down, keep, to_next, to_prev, to_far, pieces):
    for y in range(NY):
        for part, array in enumerate((gate, up, down)):
            pieces[y, :, part * BLOCK : (part + 1) * BLOCK] = array[
                :, y * BLOCK : (y + 1) * BLOCK
            ]
    for out, by in ((keep, 0), (to_next, 1), (to_prev, NY - 1), (to_far, 2)):
        out[...] = pieces[(place[0] + by) % NY]


def pair_kernel(place, inputs, cotangent, came, inp, cot):
    for core in range(2):

        @pl.when(place[2] == core)
        def _():
            own = slice(core * 256, (core + 1) * 256)
            other = slice((1 - core) * 256, (2 - core) * 256)
            for which, (array, out) in enumerate(((inputs, inp), (cotangent, cot))):
                out[:, own] = array[core * HALF : (core + 1) * HALF, :]
                out[:, other] = came[which]


def join_kernel(place, kept, from_prev, from_next, from_far, out, pieces):
    for array, by in ((kept, 0), (from_prev, NY - 1), (from_next, 1), (from_far, 2)):
        pieces[(place[0] + by) % NY] = array[...]
    rows = jnp.concatenate([pieces[y] for y in range(NY)], axis=0)
    out[...] = rows.T


def split_kernel(place, grads, keep, to_next, to_prev, to_far, pieces):
    rows = grads[...].T
    for y in range(NY):
        pieces[y] = rows[y * 64 : (y + 1) * 64]
    for out, by in ((keep, 0), (to_next, 1), (to_prev, NY - 1), (to_far, 2)):
        out[...] = pieces[(place[0] + by) % NY]


def finish_kernel(place, kept, from_prev, from_next, from_far, gate, up, down, pieces):
    for array, by in ((kept, 0), (from_prev, NY - 1), (from_next, 1), (from_far, 2)):
        pieces[(place[0] + by) % NY] = array[...]
    for y in range(NY):
        for part, out in enumerate((gate, up, down)):
            out[:, y * BLOCK : (y + 1) * BLOCK] = pieces[
                y, :, part * BLOCK : (part + 1) * BLOCK
            ].astype(jnp.float32)


def exchange(pieces):
    keep, to_next, to_prev, to_far = pieces
    return keep, shift(to_next, "y", 1), shift(to_prev, "y", -1), shift(to_far, "y", 2)


def main_kernel(place, *refs):
    inp, cot = refs[0:5], refs[5:10]
    weights = refs[10:12]
    hid, grads = refs[12], refs[13:15]
    columns = [(place[1] + by + NX) % NX for by in ORDER]

    def tile(which, y, x, lanes=slice(None)):
        arrays, near, far = (inp, x, y) if which == 0 else (cot, y, x)
        if far == 3:
            return arrays[3 + near // 2][near % 2, :, lanes]
        return arrays[far][near, :, lanes]

    def tall(first, last):
        return jnp.concatenate(
            [
                jnp.concatenate(
                    [array[2 * x + side, first:last, :] for x in columns for side in range(2)],
                    axis=1,
                )
                for array in weights
            ],
            axis=0,
        )

    for half in range(2):
        rows = slice(half * 256, (half + 1) * 256)

        def tokens(which):
            return jnp.concatenate(
                [
                    jnp.concatenate([tile(which, y, x) for x in range(NX)], axis=1)
                    for y in (2 * half, 2 * half + 1)
                ],
                axis=0,
            )

        pre = dot(tall(0, 2 * BLOCK), tokens(0), ((1,), (1,)))
        back = dot(tall(2 * BLOCK, COLS), tokens(1), ((1,), (1,)))
        for block in range(2):
            at = block * 2 * BLOCK
            gate_pre, up_pre = pre[at : at + BLOCK], pre[at + BLOCK : at + 2 * BLOCK]
            grad_hidden = back[block * BLOCK : (block + 1) * BLOCK]
            gate_sig = jax.nn.sigmoid(gate_pre)
            gate_act = gate_pre * gate_sig
            hid[at : at + BLOCK, rows] = (
                grad_hidden * up_pre * gate_sig * (1.0 + gate_pre * (1.0 - gate_sig))
            ).astype(jnp.bfloat16)
            hid[at + BLOCK : at + 2 * BLOCK, rows] = (grad_hidden * gate_act).astype(jnp.bfloat16)
            hid[4 * BLOCK + block * BLOCK : 4 * BLOCK + (block + 1) * BLOCK, rows] = (
                gate_act * up_pre
            ).astype(jnp.bfloat16)
    for slot, x in enumerate(columns):
        for side in range(2):
            lanes = slice(side * 256, (side + 1) * 256)
            for which, rows, first, size in ((0, 0, 0, 2 * BLOCK), (1, 4 * BLOCK, 2 * BLOCK, BLOCK)):
                acts = jnp.concatenate([tile(which, y, slot, lanes) for y in range(NY)], axis=0)
                grad = dot(hid[rows : rows + 2 * size], acts, ((1,), (0,))).astype(jnp.bfloat16)
                for block in range(2):
                    grads[block][2 * x + side, first : first + size, :] = grad[
                        block * size : (block + 1) * size
                    ]


def inputs_kernel(place, hid, weights_a, weights_b, out, flipped):
    flipped[...] = hid[0 : 4 * BLOCK, :].T
    for z in range(NZ):
        rows = jnp.concatenate([weights_a[z, : 2 * BLOCK], weights_b[z, : 2 * BLOCK]], axis=0)
        total = dot(flipped[...], rows, ((1,), (0,))).astype(jnp.bfloat16)
        lanes = slice((z % 2) * 256, (z % 2 + 1) * 256)
        for slot in range(NY):
            y = (place[0] + ORDER[slot] + NY) % NY
            out[y * NX + z // 2, :, lanes] = total[slot * HALF : (slot + 1) * HALF]


def per_device(inputs, cotangent, gate_weight, up_weight, down_weight):
    core = lax.axis_index("core")
    place = jnp.stack([lax.axis_index("y"), lax.axis_index("x"), core]).astype(jnp.int32)

    both = jnp.stack([inputs, cotangent]).reshape(2, 2, HALF, 256)
    sent = jnp.where(core == 0, both[:, 1], both[:, 0])
    came = lax.ppermute(sent, "core", SWAP)

    piece = (64, COLS)
    pieces = call(
        cut_kernel,
        [piece] * 4,
        [SMEM] + [VMEM] * 3,
        place,
        gate_weight,
        up_weight,
        down_weight.T,
        scratch=[(NY, *piece)],
    )
    moved = exchange(pieces)
    (rows,) = call(
        join_kernel,
        [(COLS, 256)],
        [SMEM] + [VMEM] * 4,
        place,
        *moved,
        scratch=[(NY, *piece)],
    )
    w_own = lax.all_gather(rows, "z", axis=0, tiled=False)

    inp, cot = call(
        pair_kernel, [(HALF, 512)] * 2, [SMEM] + [VMEM] * 3, place, inputs, cotangent, came
    )
    inp_near, cot_near = around(inp, "x"), around(cot, "y")
    inp_blocks = around_in_halves(jnp.stack(inp_near), "y")
    cot_blocks = around_in_halves(jnp.stack(cot_near), "x")

    w_other = lax.ppermute(w_own, "core", SWAP)

    grads_shape = (NZ, COLS, 256)
    hid_shape = (2 * COLS, ROWS)
    hid, grads_other, grads_own = call(
        main_kernel,
        [hid_shape, grads_shape, grads_shape],
        [SMEM] + [VMEM] * 12,
        place,
        *inp_blocks,
        *cot_blocks,
        w_other,
        w_own,
    )
    grads_came = lax.ppermute(grads_other, "core", SWAP)
    (partial,) = call(
        inputs_kernel,
        [(NY * NX, HALF, 512)],
        [SMEM] + [VMEM] * 3,
        place,
        hid,
        w_other,
        w_own,
        scratch=[(ROWS, 4 * BLOCK)],
    )
    grads = grads_own.astype(jnp.float32) + grads_came.astype(jnp.float32)
    grads = grads.astype(jnp.bfloat16)

    summed = lax.psum_scatter(grads, "z", scatter_dimension=0, tiled=False)
    pieces = call(
        split_kernel, [piece] * 4, [SMEM, VMEM], place, summed, scratch=[(NY, *piece)]
    )
    grad_gate, grad_up, grad_down = call(
        finish_kernel,
        [(64, NY * BLOCK)] * 3,
        [SMEM] + [VMEM] * 4,
        place,
        *exchange(pieces),
        dtype=jnp.float32,
        scratch=[(NY, *piece)],
    )

    arrived = lax.all_to_all(partial, ("y", "x"), split_axis=0, concat_axis=0, tiled=True)
    total = arrived.astype(jnp.float32).sum(axis=0).astype(jnp.bfloat16)
    lower, upper = total[:, :256], total[:, 256:]
    keep, give = jnp.where(core == 0, lower, upper), jnp.where(core == 0, upper, lower)
    take = lax.ppermute(give, "core", SWAP)
    grad_inputs = jnp.concatenate(
        [jnp.where(core == 0, keep, take), jnp.where(core == 0, take, keep)], axis=0
    )
    return grad_inputs, grad_gate, grad_up, grad_down.T


def solution(mesh):
    finer = Mesh(mesh.devices.reshape(NZ, NY, NX, 2), ("z", "y", "x", "core"))
    fs, tp = ("z", "y"), ("x", "core")

    return jax.shard_map(
        per_device,
        mesh=finer,
        in_specs=(P(fs, tp), P(fs, tp), P(fs, tp), P(fs, tp), P(tp, fs)),
        out_specs=(P(fs, tp), P(fs, tp), P(fs, tp), P(tp, fs)),
        check_vma=False,
    )
```

time: 174 us -> 183 us (1.052)
  waiting for transfers between devices: 46.8 us -> 80.8 us
  Pallas kernels: 31.9 us -> 14.9 us
  local copies, waits for them, and re-layouts: 10.8 us -> 5.51 us
  other arithmetic: 6.07 us -> 4.17 us
    all_gather x1, waiting for transfers between devices: 13.1 us -> 42.7 us  [per_device(): w_own = lax.all_gather(rows, 'z', axis=0, tiled=False)]
    pallas_call x8 -> x7, Pallas kernels: 31.9 us -> 14.9 us  [call(): pl.pallas_call(kernel, out_shape=[jax.ShapeDtypeStruct(s, dtype) for s in...]
    ppermute x1, waiting for transfers between devices: 0.01 us -> 4.24 us  [per_device(): grads_came = lax.ppermute(grads_other, 'core', SWAP)]
    ppermute x20, waiting for transfers between devices: 30 us -> 27.5 us  [shift(): lax.ppermute(array, axis, [(i, (i + by) % RING) for i in range(RING)])]
    ppermute x1, waiting for transfers between devices: 0.77 us -> 3.09 us  [per_device(): came = lax.ppermute(sent, 'core', SWAP)]
    convert_element_type x0 -> x1, other arithmetic: none -> 2.01 us  [per_device(): grads = grads.astype(jnp.bfloat16)]
    slice x2, local copies, waits for them, and re-layouts: 1.94 us -> 0.04 us  [around_in_halves(): far_last = shift(high[2:], axis, -1)]
    slice x2, local copies, waits for them, and re-layouts: 1.93 us -> 0.04 us  [around_in_halves(): far_first = shift(low[:2], axis, 1)]
  transfers between devices with their start and end apart: 26 -> 26, of which waited for: 18 -> 22; matrix products, arithmetic and copies ran while one was open for 5% -> 1% of each run, Pallas kernels for 4% -> 2%
where the time goes in v3:
time: 183 us
  waiting for transfers between devices  80.8 us (44%)
  blocking collectives  31.9 us (17%)
  starting transfers between devices  31.1 us (17%)
  Pallas kernels  14.9 us (8%)
  between operations  14.2 us (8%)
  local copies, waits for them, and re-layouts  5.51 us (3%)
  other arithmetic  4.17 us (2%)
    all_gather x1, waiting for transfers between devices, per_device(): w_own = lax.all_gather(rows, 'z', axis=0, tiled=False)  42.7 us
    all_to_all x1, blocking collectives, per_device(): lax.all_to_all(partial, ('y', 'x'), split_axis=0, concat_axis=0, tiled=True)  31.9 us
    ppermute x20, starting transfers between devices, shift(): lax.ppermute(array, axis, [(i, (i + by) % RING) for i in range(RING)])  30.3 us
    ppermute x20, waiting for transfers between devices, shift(): lax.ppermute(array, axis, [(i, (i + by) % RING) for i in range(RING)])  27.5 us
    pallas_call x7, Pallas kernels, call(): pl.pallas_call(kernel, out_shape=[jax.ShapeDtypeStruct(s, dtype) for s in...  14.9 us
    unnamed x14, local copies, waits for them, and re-layouts  5.44 us
    ppermute x1, waiting for transfers between devices, per_device(): grads_came = lax.ppermute(grads_other, 'core', SWAP)  4.24 us
  transfers between devices with their start and end apart: 26, of which 22 were waited for; matrix products, arithmetic and copies ran while one was open for 1% of the time, Pallas kernels for 2%

profile of v3, /device:TPU:2, one launch (start us, length us, event | category | flops | bytes accessed | tf_op | source)
XLA Modules:
  0.0 182.7 jit_solution(4944060842320073264)
XLA Ops:
  7.2 0.1 pad_add_fusion.place
  7.3 0.9 copy-done.4
  8.2 0.9 copy-done.5
  9.1 0.9 copy-done.6
  10.0 0.7 shard_map.85
  10.7 1.7 collective-permute-start.15
  12.4 1.7 collective-permute-start.16
  14.0 2.0 %collective-permute-start.17 = (bf16[64,528]{1,0:T(8,128)(2,1)S(1)}, bf16[64,528]{1,0:T(8,128)(2,1)S(1)}, u32[]{:S(2)}, u32[]{:S(2)}) collective-permute-start(bf16[64,528]{1,0:T(8,128)(2,1)S(1)} %get-tuple-element.25), channel_id=1, source_target_pairs={{0,16},{8,24},{16,0},{24,8},{1,17},{9,25},{17,1},{25,9},{2,18},{10... | collective-permute-start | bytes 202760 | tf_op jit(solution)/shard_map/ppermute | solution.py:40
  16.0 0.4 collective-permute-done.15.from_prev
  16.4 0.6 collective-permute-done.16.from_next
  17.1 2.9 %collective-permute-done.17.from_far = bf16[64,528]{1,0:T(8,128)(2,1)S(1)} collective-permute-done((bf16[64,528]{1,0:T(8,128)(2,1)S(1)}, bf16[64,528]{1,0:T(8,128)(2,1)S(1)}, u32[]{:S(2)}, u32[]{:S(2)}) %collective-permute-start.17) | collective-permute-done | bytes 67616 | tf_op jit(solution)/shard_map/ppermute | solution.py:40
  20.0 1.4 shard_map.86
  21.5 42.7 %all-gather.3.cloned.1.call-done = bf16[4224,256]{1,0:T(8,128)(2,1)} async-done(((bf16[528,256]{1,0:T(8,128)(2,1)}), bf16[4224,256]{1,0:T(8,128)(2,1)}) %all-gather.3.cloned.1.call-update) | async-done | bytes 2162704 | tf_op jit(solution)/shard_map/all_gather | solution.py:208
  64.2 1.0 fusion.2
  65.1 0.6 collective-permute-start
  65.7 3.1 %collective-permute-done.came = bf16[2,128,256]{2,1,0:T(8,128)(2,1)S(1)} collective-permute-done((bf16[2,128,256]{2,1,0:T(8,128)(2,1)S(1)}, bf16[2,128,256]{2,1,0:T(8,128)(2,1)S(1)}, u32[]{:S(2)}, u32[]{:S(2)}) %collective-permute-start) | collective-permute-done | bytes 131104 | tf_op jit(solution)/shard_map/ppermute | solution.py:186
  68.8 0.9 copy-done.1
  69.7 0.9 copy-done.2
  70.6 0.6 shard_map.84
  71.2 3.1 %collective-permute-start.10 = (bf16[128,512]{1,0:T(8,128)(2,1)S(1)}, bf16[128,512]{1,0:T(8,128)(2,1)S(1)}, u32[]{:S(2)}, u32[]{:S(2)}) collective-permute-start(bf16[128,512]{1,0:T(8,128)(2,1)S(1)} %get-tuple-element.21), channel_id=1, source_target_pairs={{0,16},{8,24},{16,0},{24,8},{1,17},{9,25},{17,1},{25,9},{2,18},{10... | collective-permute-start | bytes 393224 | tf_op jit(solution)/shard_map/ppermute | solution.py:40
  74.3 1.1 collective-permute-start.9
  75.5 0.9 collective-permute-start.8
  76.3 2.1 %collective-permute-start.3 = (bf16[128,512]{1,0:T(8,128)(2,1)S(1)}, bf16[128,512]{1,0:T(8,128)(2,1)S(1)}, u32[]{:S(2)}, u32[]{:S(2)}) collective-permute-start(bf16[128,512]{1,0:T(8,128)(2,1)S(1)} %get-tuple-element.20), channel_id=1, source_target_pairs={{0,4},{2,6},{4,0},{6,2},{1,5},{3,7},{5,1},{7,3},{8,12},{10,14},{12... | collective-permute-start | bytes 393224 | tf_op jit(solution)/shard_map/ppermute | solution.py:40
  78.4 0.8 collective-permute-done.10
  79.2 0.7 collective-permute-start.2
  79.9 1.3 collective-permute-done.9
  81.2 1.5 collective-permute-start.1
  82.7 0.1 pad_maximum_fusion.1.refs_5_
  82.8 0.6 collective-permute-start.12
  83.4 0.5 collective-permute-done.3
  84.0 0.9 collective-permute-start.11
  84.9 1.4 collective-permute-done.2
  86.3 1.3 collective-permute-done.1
  87.7 2.7 %collective-permute-start.5 = (bf16[4,128,512]{2,1,0:T(8,128)(2,1)S(1)}, bf16[4,128,512]{2,1,0:T(8,128)(2,1)S(1)}, u32[]{:S(2)}, u32[]{:S(2)}) collective-permute-start(bf16[4,128,512]{2,1,0:T(8,128)(2,1)S(1)} %pad_maximum_fusion.refs_0_), channel_id=1, source_target_pairs={{0,24},{8,0},{16,8},{24,16},{1,25},{9,1},{17,9},{25,17},{2,26},{10... | collective-permute-start | bytes 1572872 | tf_op jit(solution)/shard_map/ppermute | solution.py:40
  90.4 6.2 %collective-permute-done.12.refs_7_ = bf16[4,128,512]{2,1,0:T(8,128)(2,1)S(1)} collective-permute-done((bf16[4,128,512]{2,1,0:T(8,128)(2,1)S(1)}, bf16[4,128,512]{2,1,0:T(8,128)(2,1)S(1)}, u32[]{:S(2)}, u32[]{:S(2)}) %collective-permute-start.12) | collective-permute-done | bytes 524320 | tf_op jit(solution)/shard_map/ppermute | solution.py:40
  96.6 0.7 collective-permute-start.14
  97.3 0.1 collective-permute-done.11.refs_6_
  97.4 1.7 collective-permute-start.13
  99.1 0.9 collective-permute-done.5.refs_2_
  100.0 3.8 %collective-permute-start.7 = (bf16[2,128,512]{2,1,0:T(8,128)(2,1)S(1)}, bf16[2,128,512]{2,1,0:T(8,128)(2,1)S(1)}, u32[]{:S(2)}, u32[]{:S(2)}) collective-permute-start(bf16[2,128,512]{2,1,0:T(8,128)(2,1)S(1)} %slice.35), channel_id=1, source_target_pairs={{0,24},{8,0},{16,8},{24,16},{1,25},{9,1},{17,9},{25,17},{2,26},{10... | collective-permute-start | bytes 786440 | tf_op jit(solution)/shard_map/ppermute | solution.py:40
  103.8 0.1 collective-permute-start.6
  103.9 0.1 collective-permute-done.14.refs_9_
  104.0 1.1 collective-permute-done.13.refs_8_
  105.1 2.6 %collective-permute-done.7.refs_4_ = bf16[2,128,512]{2,1,0:T(8,128)(2,1)S(1)} collective-permute-done((bf16[2,128,512]{2,1,0:T(8,128)(2,1)S(1)}, bf16[2,128,512]{2,1,0:T(8,128)(2,1)S(1)}, u32[]{:S(2)}, u32[]{:S(2)}) %collective-permute-start.7) | collective-permute-done | bytes 262176 | tf_op jit(solution)/shard_map/ppermute | solution.py:40
  107.7 3.8 %collective-permute-done.6.refs_3_ = bf16[2,128,512]{2,1,0:T(8,128)(2,1)S(1)} collective-permute-done((bf16[2,128,512]{2,1,0:T(8,128)(2,1)S(1)}, bf16[2,128,512]{2,1,0:T(8,128)(2,1)S(1)}, u32[]{:S(2)}, u32[]{:S(2)}) %collective-permute-start.6) | collective-permute-done | bytes 262176 | tf_op jit(solution)/shard_map/ppermute | solution.py:40
  111.5 6.4 %shard_map.87 = (bf16[1056,512]{1,0:T(8,128)(2,1)S(1)}, bf16[8,528,256]{2,1,0:T(8,128)(2,1)S(1)}, bf16[8,528,256]{2,1,0:T(8,128)(2,1)S(1)}) custom-call(s32[3]{0:T(128)S(1)} %pad_add_fusion.place, bf16[4,128,512]{2,1,0:T(8,128)(2,1)S(1)} %pad_maximum_fusion.refs_0_, bf16[4,128,512]{2,1,0:T(8,128)(2,1)S(1)} %collective-permute-done.4.refs_1_, ...), custom_call_target="tpu_custom_call" | custom-call | tf_op jit(solution)/shard_map/pallas_call | solution.py:29
  117.9 0.1 collective-permute-start.20
  118.0 4.2 %collective-permute-done.20 = bf16[8,528,256]{2,1,0:T(8,128)(2,1)S(1)} collective-permute-done((bf16[8,528,256]{2,1,0:T(8,128)(2,1)S(1)}, bf16[8,528,256]{2,1,0:T(8,128)(2,1)S(1)}, u32[]{:S(2)}, u32[]{:S(2)}) %collective-permute-start.20) | collective-permute-done | bytes 2162720 | tf_op jit(solution)/shard_map/ppermute | solution.py:231
  122.2 2.0 %add_convert_fusion = bf16[8,528,256]{2,1,0:T(8,128)(2,1)} fusion(bf16[8,528,256]{2,1,0:T(8,128)(2,1)S(1)} %collective-permute-done.20, bf16[8,528,256]{2,1,0:T(8,128)(2,1)S(1)} %get-tuple-element.27), kind=kLoop, calls=%fused_computation | loop fusion | flops 4325376 | bytes 6488064 | tf_op jit(solution)/shard_map/convert_element_type | solution.py:243
  124.2 3.6 %shard_map.88 = bf16[16,128,512]{2,1,0:T(8,128)(2,1)S(1)} custom-call(s32[3]{0:T(128)S(1)} %pad_add_fusion.place, bf16[1056,512]{1,0:T(8,128)(2,1)S(1)} %get-tuple-element.26.hid, bf16[8,528,256]{2,1,0:T(8,128)(2,1)} %collective-permute-done.18.refs_10_.weights_a, bf16[8,528,256]{2,1,0:T(8,128)(2,1)S(1)} %bitcast.21), custom_call_target="tpu_custom_call" | custom-call | tf_op jit(solution)/shard_map/pallas_call | solution.py:29
  127.8 31.9 %all_to_all.5 = bf16[16,128,512]{2,1,0:T(8,128)(2,1)S(1)} all-to-all(bf16[16,128,512]{2,1,0:T(8,128)(2,1)S(1)} %shard_map.88), channel_id=1, replica_groups=mesh['z'=8,'y'=4,'x'=4,'core'=2] {'y','x'}, dimensions={0} | all-to-all | bytes 4194304 | tf_op jit(solution)/shard_map/all_to_all | solution.py:259
  159.7 0.3 reduce_sum.12
  160.1 0.1 collective-permute-start.19
  160.2 1.2 collective-permute-done.19
  161.4 2.0 %reduce-scatter.2.cloned.1.call-done = bf16[1,528,256]{2,1,0:T(8,128)(2,1)} async-done(((bf16[8,528,256]{2,1,0:T(8,128)(2,1)}), bf16[1,528,256]{2,1,0:T(8,128)(2,1)}) %reduce-scatter.2.cloned.1.call-update) | async-done | bytes 270352 | tf_op jit(solution)/shard_map/reduce_scatter | solution.py:245
  163.4 1.0 copy-done.3
  164.3 0.7 shard_map.89
  165.0 1.5 collective-permute-start.21
  166.6 1.8 collective-permute-start.22
  168.4 1.8 collective-permute-start.23
  170.1 0.7 pad_maximum_fusion.3
  170.8 0.8 collective-permute-done.21.from_prev
  171.7 2.6 %collective-permute-done.23.from_far = bf16[64,528]{1,0:T(8,128)(2,1)S(1)} collective-permute-done((bf16[64,528]{1,0:T(8,128)(2,1)S(1)}, bf16[64,528]{1,0:T(8,128)(2,1)S(1)}, u32[]{:S(2)}, u32[]{:S(2)}) %collective-permute-start.23) | collective-permute-done | bytes 67616 | tf_op jit(solution)/shard_map/ppermute | solution.py:40
  174.3 1.5 shard_map.90
  (25 shorter events, 0.3 us)
Async XLA Ops:
  7.2 57.0 %all-gather.3.cloned.1.call-start = ((), (), s32[]{:S(2)}) async-start(), calls=%async_computation.3 | async-start | bytes 2433024 | tf_op jit(solution)/shard_map/all_gather | solution.py:208
  7.3 0.9 copy-start.4
  8.2 0.9 copy-start.5
  9.1 0.9 copy-start.6
  10.7 5.7 %collective-permute-start.15 = (bf16[64,528]{1,0:T(8,128)(2,1)S(1)}, bf16[64,528]{1,0:T(8,128)(2,1)S(1)}, u32[]{:S(2)}, u32[]{:S(2)}) collective-permute-start(bf16[64,528]{1,0:T(8,128)(2,1)S(1)} %get-tuple-element.23), channel_id=1, source_target_pairs={{0,8},{8,16},{16,24},{24,0},{1,9},{9,17},{17,25},{25,1},{2,10},{10... | collective-permute-start | bytes 202760 | tf_op jit(solution)/shard_map/ppermute | solution.py:40
  12.4 4.7 %collective-permute-start.16 = (bf16[64,528]{1,0:T(8,128)(2,1)S(1)}, bf16[64,528]{1,0:T(8,128)(2,1)S(1)}, u32[]{:S(2)}, u32[]{:S(2)}) collective-permute-start(bf16[64,528]{1,0:T(8,128)(2,1)S(1)} %get-tuple-element.24), channel_id=1, source_target_pairs={{0,24},{8,0},{16,8},{24,16},{1,25},{9,1},{17,9},{25,17},{2,26},{10... | collective-permute-start | bytes 202760 | tf_op jit(solution)/shard_map/ppermute | solution.py:40
  14.0 5.9 %collective-permute-start.17 = (bf16[64,528]{1,0:T(8,128)(2,1)S(1)}, bf16[64,528]{1,0:T(8,128)(2,1)S(1)}, u32[]{:S(2)}, u32[]{:S(2)}) collective-permute-start(bf16[64,528]{1,0:T(8,128)(2,1)S(1)} %get-tuple-element.25), channel_id=1, source_target_pairs={{0,16},{8,24},{16,0},{24,8},{1,17},{9,25},{17,1},{25,9},{2,18},{10... | collective-permute-start | bytes 202760 | tf_op jit(solution)/shard_map/ppermute | solution.py:40
  21.4 142.0 %reduce-scatter.2.cloned.1.call-start = ((), (), s32[]{:S(2)}) async-start(), calls=%async_computation.2 | async-start | bytes 2433024 | tf_op jit(solution)/shard_map/reduce_scatter | solution.py:245
  64.2 47.3 %collective-permute-start.18 = (bf16[8,528,256]{2,1,0:T(8,128)(2,1)}, bf16[8,528,256]{2,1,0:T(8,128)(2,1)}, u32[]{:S(2)}, u32[]{:S(2)}) collective-permute-start(bf16[8,528,256]{2,1,0:T(8,128)(2,1)} %bitcast.19), channel_id=1, source_target_pairs={{0,1},{1,0},{2,3},{3,2},{4,5},{5,4},{6,7},{7,6},{8,9},{9,8},{10,11... | collective-permute-start | bytes 6488072 | tf_op jit(solution)/shard_map/ppermute | solution.py:217
  65.1 3.7 %collective-permute-start = (bf16[2,128,256]{2,1,0:T(8,128)(2,1)S(1)}, bf16[2,128,256]{2,1,0:T(8,128)(2,1)S(1)}, u32[]{:S(2)}, u32[]{:S(2)}) collective-permute-start(bf16[2,128,256]{2,1,0:T(8,128)(2,1)S(1)} %fusion.2), channel_id=1, source_target_pairs={{0,1},{1,0},{2,3},{3,2},{4,5},{5,4},{6,7},{7,6},{8,9},{9,8},{10,11... | collective-permute-start | bytes 393224 | tf_op jit(solution)/shard_map/ppermute | solution.py:186
  68.8 0.9 copy-start.1
  69.7 0.9 copy-start.2
  71.2 40.3 %copy-start = (bf16[4224,256]{1,0:T(8,128)(2,1)S(1)}, bf16[4224,256]{1,0:T(8,128)(2,1)}, u32[]{:S(2)}) copy-start(bf16[4224,256]{1,0:T(8,128)(2,1)} %all-gather.3.cloned.1.call-done) | copy-start | bytes 6488068
  71.2 8.0 %collective-permute-start.10 = (bf16[128,512]{1,0:T(8,128)(2,1)S(1)}, bf16[128,512]{1,0:T(8,128)(2,1)S(1)}, u32[]{:S(2)}, u32[]{:S(2)}) collective-permute-start(bf16[128,512]{1,0:T(8,128)(2,1)S(1)} %get-tuple-element.21), channel_id=1, source_target_pairs={{0,16},{8,24},{16,0},{24,8},{1,17},{9,25},{17,1},{25,9},{2,18},{10... | collective-permute-start | bytes 393224 | tf_op jit(solution)/shard_map/ppermute | solution.py:40
  74.3 6.9 %collective-permute-start.9 = (bf16[128,512]{1,0:T(8,128)(2,1)S(1)}, bf16[128,512]{1,0:T(8,128)(2,1)S(1)}, u32[]{:S(2)}, u32[]{:S(2)}) collective-permute-start(bf16[128,512]{1,0:T(8,128)(2,1)S(1)} %get-tuple-element.21), channel_id=1, source_target_pairs={{0,24},{8,0},{16,8},{24,16},{1,25},{9,1},{17,9},{25,17},{2,26},{10... | collective-permute-start | bytes 393224 | tf_op jit(solution)/shard_map/ppermute | solution.py:40
  75.5 7.2 %collective-permute-start.8 = (bf16[128,512]{1,0:T(8,128)(2,1)S(1)}, bf16[128,512]{1,0:T(8,128)(2,1)S(1)}, u32[]{:S(2)}, u32[]{:S(2)}) collective-permute-start(bf16[128,512]{1,0:T(8,128)(2,1)S(1)} %get-tuple-element.21), channel_id=1, source_target_pairs={{0,8},{8,16},{16,24},{24,0},{1,9},{9,17},{17,25},{25,1},{2,10},{10... | collective-permute-start | bytes 393224 | tf_op jit(solution)/shard_map/ppermute | solution.py:40
  76.3 7.6 %collective-permute-start.3 = (bf16[128,512]{1,0:T(8,128)(2,1)S(1)}, bf16[128,512]{1,0:T(8,128)(2,1)S(1)}, u32[]{:S(2)}, u32[]{:S(2)}) collective-permute-start(bf16[128,512]{1,0:T(8,128)(2,1)S(1)} %get-tuple-element.20), channel_id=1, source_target_pairs={{0,4},{2,6},{4,0},{6,2},{1,5},{3,7},{5,1},{7,3},{8,12},{10,14},{12... | collective-permute-start | bytes 393224 | tf_op jit(solution)/shard_map/ppermute | solution.py:40
  79.2 7.1 %collective-permute-start.2 = (bf16[128,512]{1,0:T(8,128)(2,1)S(1)}, bf16[128,512]{1,0:T(8,128)(2,1)S(1)}, u32[]{:S(2)}, u32[]{:S(2)}) collective-permute-start(bf16[128,512]{1,0:T(8,128)(2,1)S(1)} %get-tuple-element.20), channel_id=1, source_target_pairs={{0,6},{2,0},{4,2},{6,4},{1,7},{3,1},{5,3},{7,5},{8,14},{10,8},{12,... | collective-permute-start | bytes 393224 | tf_op jit(solution)/shard_map/ppermute | solution.py:40
  81.2 6.4 %collective-permute-start.1 = (bf16[128,512]{1,0:T(8,128)(2,1)S(1)}, bf16[128,512]{1,0:T(8,128)(2,1)S(1)}, u32[]{:S(2)}, u32[]{:S(2)}) collective-permute-start(bf16[128,512]{1,0:T(8,128)(2,1)S(1)} %get-tuple-element.20), channel_id=1, source_target_pairs={{0,2},{2,4},{4,6},{6,0},{1,3},{3,5},{5,7},{7,1},{8,10},{10,12},{12... | collective-permute-start | bytes 393224 | tf_op jit(solution)/shard_map/ppermute | solution.py:40
  82.8 13.8 %collective-permute-start.12 = (bf16[4,128,512]{2,1,0:T(8,128)(2,1)S(1)}, bf16[4,128,512]{2,1,0:T(8,128)(2,1)S(1)}, u32[]{:S(2)}, u32[]{:S(2)}) collective-permute-start(bf16[4,128,512]{2,1,0:T(8,128)(2,1)S(1)} %pad_maximum_fusion.1.refs_5_), channel_id=1, source_target_pairs={{0,6},{2,0},{4,2},{6,4},{1,7},{3,1},{5,3},{7,5},{8,14},{10,8},{12,... | collective-permute-start | bytes 1572872 | tf_op jit(solution)/shard_map/ppermute | solution.py:40
  84.0 13.4 %collective-permute-start.11 = (bf16[4,128,512]{2,1,0:T(8,128)(2,1)S(1)}, bf16[4,128,512]{2,1,0:T(8,128)(2,1)S(1)}, u32[]{:S(2)}, u32[]{:S(2)}) collective-permute-start(bf16[4,128,512]{2,1,0:T(8,128)(2,1)S(1)} %pad_maximum_fusion.1.refs_5_), channel_id=1, source_target_pairs={{0,2},{2,4},{4,6},{6,0},{1,3},{3,5},{5,7},{7,1},{8,10},{10,12},{12... | collective-permute-start | bytes 1572872 | tf_op jit(solution)/shard_map/ppermute | solution.py:40
  87.7 12.3 %collective-permute-start.5 = (bf16[4,128,512]{2,1,0:T(8,128)(2,1)S(1)}, bf16[4,128,512]{2,1,0:T(8,128)(2,1)S(1)}, u32[]{:S(2)}, u32[]{:S(2)}) collective-permute-start(bf16[4,128,512]{2,1,0:T(8,128)(2,1)S(1)} %pad_maximum_fusion.refs_0_), channel_id=1, source_target_pairs={{0,24},{8,0},{16,8},{24,16},{1,25},{9,1},{17,9},{25,17},{2,26},{10... | collective-permute-start | bytes 1572872 | tf_op jit(solution)/shard_map/ppermute | solution.py:40
  90.4 13.4 %collective-permute-start.4 = (bf16[4,128,512]{2,1,0:T(8,128)(2,1)S(1)}, bf16[4,128,512]{2,1,0:T(8,128)(2,1)S(1)}, u32[]{:S(2)}, u32[]{:S(2)}) collective-permute-start(bf16[4,128,512]{2,1,0:T(8,128)(2,1)S(1)} %pad_maximum_fusion.refs_0_), channel_id=1, source_target_pairs={{0,8},{8,16},{16,24},{24,0},{1,9},{9,17},{17,25},{25,1},{2,10},{10... | collective-permute-start | bytes 1572872 | tf_op jit(solution)/shard_map/ppermute | solution.py:40
  96.6 7.3 %collective-permute-start.14 = (bf16[2,128,512]{2,1,0:T(8,128)(2,1)S(1)}, bf16[2,128,512]{2,1,0:T(8,128)(2,1)S(1)}, u32[]{:S(2)}, u32[]{:S(2)}) collective-permute-start(bf16[2,128,512]{2,1,0:T(8,128)(2,1)S(1)} %slice.37), channel_id=1, source_target_pairs={{0,6},{2,0},{4,2},{6,4},{1,7},{3,1},{5,3},{7,5},{8,14},{10,8},{12,... | collective-permute-start | bytes 786440 | tf_op jit(solution)/shard_map/ppermute | solution.py:40
  97.4 7.7 %collective-permute-start.13 = (bf16[2,128,512]{2,1,0:T(8,128)(2,1)S(1)}, bf16[2,128,512]{2,1,0:T(8,128)(2,1)S(1)}, u32[]{:S(2)}, u32[]{:S(2)}) collective-permute-start(bf16[2,128,512]{2,1,0:T(8,128)(2,1)S(1)} %slice.36), channel_id=1, source_target_pairs={{0,2},{2,4},{4,6},{6,0},{1,3},{3,5},{5,7},{7,1},{8,10},{10,12},{12... | collective-permute-start | bytes 786440 | tf_op jit(solution)/shard_map/ppermute | solution.py:40
  100.0 7.7 %collective-permute-start.7 = (bf16[2,128,512]{2,1,0:T(8,128)(2,1)S(1)}, bf16[2,128,512]{2,1,0:T(8,128)(2,1)S(1)}, u32[]{:S(2)}, u32[]{:S(2)}) collective-permute-start(bf16[2,128,512]{2,1,0:T(8,128)(2,1)S(1)} %slice.35), channel_id=1, source_target_pairs={{0,24},{8,0},{16,8},{24,16},{1,25},{9,1},{17,9},{25,17},{2,26},{10... | collective-permute-start | bytes 786440 | tf_op jit(solution)/shard_map/ppermute | solution.py:40
  103.8 7.7 %collective-permute-start.6 = (bf16[2,128,512]{2,1,0:T(8,128)(2,1)S(1)}, bf16[2,128,512]{2,1,0:T(8,128)(2,1)S(1)}, u32[]{:S(2)}, u32[]{:S(2)}) collective-permute-start(bf16[2,128,512]{2,1,0:T(8,128)(2,1)S(1)} %slice.34), channel_id=1, source_target_pairs={{0,8},{8,16},{16,24},{24,0},{1,9},{9,17},{17,25},{25,1},{2,10},{10... | collective-permute-start | bytes 786440 | tf_op jit(solution)/shard_map/ppermute | solution.py:40
  117.9 4.3 %collective-permute-start.20 = (bf16[8,528,256]{2,1,0:T(8,128)(2,1)S(1)}, bf16[8,528,256]{2,1,0:T(8,128)(2,1)S(1)}, u32[]{:S(2)}, u32[]{:S(2)}) collective-permute-start(bf16[8,528,256]{2,1,0:T(8,128)(2,1)S(1)} %get-tuple-element.28), channel_id=1, source_target_pairs={{0,1},{1,0},{2,3},{3,2},{4,5},{5,4},{6,7},{7,6},{8,9},{9,8},{10,11... | collective-permute-start | bytes 6488072 | tf_op jit(solution)/shard_map/ppermute | solution.py:231
  160.1 1.3 collective-permute-start.19
  163.4 1.0 copy-start.3
  165.0 6.6 %collective-permute-start.21 = (bf16[64,528]{1,0:T(8,128)(2,1)S(1)}, bf16[64,528]{1,0:T(8,128)(2,1)S(1)}, u32[]{:S(2)}, u32[]{:S(2)}) collective-permute-start(bf16[64,528]{1,0:T(8,128)(2,1)S(1)} %get-tuple-element.30), channel_id=1, source_target_pairs={{0,8},{8,16},{16,24},{24,0},{1,9},{9,17},{17,25},{25,1},{2,10},{10... | collective-permute-start | bytes 202760 | tf_op jit(solution)/shard_map/ppermute | solution.py:40
  166.6 5.1 %collective-permute-start.22 = (bf16[64,528]{1,0:T(8,128)(2,1)S(1)}, bf16[64,528]{1,0:T(8,128)(2,1)S(1)}, u32[]{:S(2)}, u32[]{:S(2)}) collective-permute-start(bf16[64,528]{1,0:T(8,128)(2,1)S(1)} %get-tuple-element.31), channel_id=1, source_target_pairs={{0,24},{8,0},{16,8},{24,16},{1,25},{9,1},{17,9},{25,17},{2,26},{10... | collective-permute-start | bytes 202760 | tf_op jit(solution)/shard_map/ppermute | solution.py:40
  168.4 5.9 %collective-permute-start.23 = (bf16[64,528]{1,0:T(8,128)(2,1)S(1)}, bf16[64,528]{1,0:T(8,128)(2,1)S(1)}, u32[]{:S(2)}, u32[]{:S(2)}) collective-permute-start(bf16[64,528]{1,0:T(8,128)(2,1)S(1)} %get-tuple-element.32), channel_id=1, source_target_pairs={{0,16},{8,24},{16,0},{24,8},{1,17},{9,25},{17,1},{25,9},{2,18},{10... | collective-permute-start | bytes 202760 | tf_op jit(solution)/shard_map/ppermute | solution.py:40
Sparse Core Ops, SparseCore 0:
  21.5 42.5 all-gather.2
  124.4 38.9 reduce-scatter.1

commit v4 on v3

--- a/solution.py
+++ b/solution.py
@@ -103,10 +103,9 @@
     return keep, shift(to_next, "y", 1), shift(to_prev, "y", -1), shift(to_far, "y", 2)
 
 
-def main_kernel(place, *refs):
+def block_kernel(place, *refs):
     inp, cot = refs[0:5], refs[5:10]
-    weights = refs[10:12]
-    hid, grads = refs[12], refs[13:15]
+    weights, hid, grads = refs[10:13]
     columns = [(place[1] + by + NX) % NX for by in ORDER]
 
     def tile(which, y, x, lanes=slice(None)):
@@ -115,16 +114,9 @@
             return arrays[3 + near // 2][near % 2, :, lanes]
         return arrays[far][near, :, lanes]
 
-    def tall(first, last):
+    def wide(first, last):
         return jnp.concatenate(
-            [
-                jnp.concatenate(
-                    [array[2 * x + side, first:last, :] for x in columns for side in range(2)],
-                    axis=1,
-                )
-                for array in weights
-            ],
-            axis=0,
+            [weights[2 * x + side, first:last, :] for x in columns for side in range(2)], axis=1
         )
 
     for half in range(2):
@@ -139,35 +131,29 @@
                 axis=0,
             )
 
-        pre = dot(tall(0, 2 * BLOCK), tokens(0), ((1,), (1,)))
-        back = dot(tall(2 * BLOCK, COLS), tokens(1), ((1,), (1,)))
-        for block in range(2):
-            at = block * 2 * BLOCK
-            gate_pre, up_pre = pre[at : at + BLOCK], pre[at + BLOCK : at + 2 * BLOCK]
-            grad_hidden = back[block * BLOCK : (block + 1) * BLOCK]
-            gate_sig = jax.nn.sigmoid(gate_pre)
-            gate_act = gate_pre * gate_sig
-            hid[at : at + BLOCK, rows] = (
-                grad_hidden * up_pre * gate_sig * (1.0 + gate_pre * (1.0 - gate_sig))
-            ).astype(jnp.bfloat16)
-            hid[at + BLOCK : at + 2 * BLOCK, rows] = (grad_hidden * gate_act).astype(jnp.bfloat16)
-            hid[4 * BLOCK + block * BLOCK : 4 * BLOCK + (block + 1) * BLOCK, rows] = (
-                gate_act * up_pre
-            ).astype(jnp.bfloat16)
+        pre = dot(wide(0, 2 * BLOCK), tokens(0), ((1,), (1,)))
+        grad_hidden = dot(wide(2 * BLOCK, COLS), tokens(1), ((1,), (1,)))
+        gate_pre, up_pre = pre[:BLOCK], pre[BLOCK:]
+        gate_sig = jax.nn.sigmoid(gate_pre)
+        gate_act = gate_pre * gate_sig
+        hid[0:BLOCK, rows] = (
+            grad_hidden * up_pre * gate_sig * (1.0 + gate_pre * (1.0 - gate_sig))
+        ).astype(jnp.bfloat16)
+        hid[BLOCK : 2 * BLOCK, rows] = (grad_hidden * gate_act).astype(jnp.bfloat16)
+        hid[2 * BLOCK : COLS, rows] = (gate_act * up_pre).astype(jnp.bfloat16)
     for slot, x in enumerate(columns):
         for side in range(2):
             lanes = slice(side * 256, (side + 1) * 256)
-            for which, rows, first, size in ((0, 0, 0, 2 * BLOCK), (1, 4 * BLOCK, 2 * BLOCK, BLOCK)):
+            for which, rows in ((0, slice(0, 2 * BLOCK)), (1, slice(2 * BLOCK, COLS))):
                 acts = jnp.concatenate([tile(which, y, slot, lanes) for y in range(NY)], axis=0)
-                grad = dot(hid[rows : rows + 2 * size], acts, ((1,), (0,))).astype(jnp.bfloat16)
-                for block in range(2):
-                    grads[block][2 * x + side, first : first + size, :] = grad[
-                        block * size : (block + 1) * size
-                    ]
-
-
-def inputs_kernel(place, hid, weights_a, weights_b, out, flipped):
-    flipped[...] = hid[0 : 4 * BLOCK, :].T
+                grads[2 * x + side, rows, :] = dot(hid[rows], acts, ((1,), (0,))).astype(
+                    jnp.bfloat16
+                )
+
+
+def inputs_kernel(place, hid_a, hid_b, weights_a, weights_b, out, flipped):
+    both = jnp.concatenate([hid_a[: 2 * BLOCK], hid_b[: 2 * BLOCK]], axis=0)
+    flipped[...] = both.T
     for z in range(NZ):
         rows = jnp.concatenate([weights_a[z, : 2 * BLOCK], weights_b[z, : 2 * BLOCK]], axis=0)
         total = dot(flipped[...], rows, ((1,), (0,))).astype(jnp.bfloat16)
@@ -216,25 +202,27 @@
 
     w_other = lax.ppermute(w_own, "core", SWAP)
 
-    grads_shape = (NZ, COLS, 256)
-    hid_shape = (2 * COLS, ROWS)
-    hid, grads_other, grads_own = call(
-        main_kernel,
-        [hid_shape, grads_shape, grads_shape],
-        [SMEM] + [VMEM] * 12,
-        place,
-        *inp_blocks,
-        *cot_blocks,
-        w_other,
-        w_own,
-    )
+    def block(weights):
+        return call(
+            block_kernel,
+            [(COLS, ROWS), (NZ, COLS, 256)],
+            [SMEM] + [VMEM] * 11,
+            place,
+            *inp_blocks,
+            *cot_blocks,
+            weights,
+        )
+
+    hid_own, grads_own = block(w_own)
+    hid_other, grads_other = block(w_other)
     grads_came = lax.ppermute(grads_other, "core", SWAP)
     (partial,) = call(
         inputs_kernel,
         [(NY * NX, HALF, 512)],
-        [SMEM] + [VMEM] * 3,
-        place,
-        hid,
+        [SMEM] + [VMEM] * 4,
+        place,
+        hid_other,
+        hid_own,
         w_other,
         w_own,
         scratch=[(ROWS, 4 * BLOCK)],

time: 183 us -> 181 us (0.989)
  waiting for transfers between devices: 80.8 us -> 77.5 us
    ppermute x1, waiting for transfers between devices: 4.24 us -> 0.92 us  [per_device(): grads_came = lax.ppermute(grads_other, 'core', SWAP)]
    pallas_call x7 -> x8, Pallas kernels: 14.9 us -> 16.2 us  [call(): pl.pallas_call(kernel, out_shape=[jax.ShapeDtypeStruct(s, dtype) for s in...]
  transfers between devices with their start and end apart: 26 -> 26, of which waited for: 22 -> 22; matrix products, arithmetic and copies ran while one was open for 1% -> 1% of each run, Pallas kernels for 2% -> 4%
where the time goes in v4:
time: 181 us
  waiting for transfers between devices  77.5 us (43%)
  blocking collectives  31.9 us (18%)
  starting transfers between devices  31.1 us (17%)
  Pallas kernels  16.2 us (9%)
  between operations  14.2 us (8%)
  local copies, waits for them, and re-layouts  5.51 us (3%)
  other arithmetic  4.15 us (2%)
    all_gather x1, waiting for transfers between devices, per_device(): w_own = lax.all_gather(rows, 'z', axis=0, tiled=False)  42.7 us
    all_to_all x1, blocking collectives, per_device(): lax.all_to_all(partial, ('y', 'x'), split_axis=0, concat_axis=0, tiled=True)  31.9 us
    ppermute x20, starting transfers between devices, shift(): lax.ppermute(array, axis, [(i, (i + by) % RING) for i in range(RING)])  30.3 us
    ppermute x20, waiting for transfers between devices, shift(): lax.ppermute(array, axis, [(i, (i + by) % RING) for i in range(RING)])  27.5 us
    pallas_call x8, Pallas kernels, call(): pl.pallas_call(kernel, out_shape=[jax.ShapeDtypeStruct(s, dtype) for s in...  16.2 us
    unnamed x14, local copies, waits for them, and re-layouts  5.44 us
  transfers between devices with their start and end apart: 26, of which 22 were waited for; matrix products, arithmetic and copies ran while one was open for 1% of the time, Pallas kernels for 4%

profile of v4, /device:TPU:2, one launch (start us, length us, event | category | flops | bytes accessed | tf_op | source)
XLA Modules:
  0.0 180.6 jit_solution(13958702777967180651)
XLA Ops:
  7.2 0.1 pad_add_fusion.place
  7.3 0.9 copy-done.4
  8.2 0.9 copy-done.5
  9.1 0.9 copy-done.6
  10.0 0.7 shard_map.85
  10.7 1.7 collective-permute-start.15
  12.4 1.7 collective-permute-start.16
  14.0 2.0 %collective-permute-start.17 = (bf16[64,528]{1,0:T(8,128)(2,1)S(1)}, bf16[64,528]{1,0:T(8,128)(2,1)S(1)}, u32[]{:S(2)}, u32[]{:S(2)}) collective-permute-start(bf16[64,528]{1,0:T(8,128)(2,1)S(1)} %get-tuple-element.26), channel_id=1, source_target_pairs={{0,16},{8,24},{16,0},{24,8},{1,17},{9,25},{17,1},{25,9},{2,18},{10... | collective-permute-start | bytes 202760 | tf_op jit(solution)/shard_map/ppermute | solution.py:40
  16.0 0.4 collective-permute-done.15.from_prev
  16.4 0.6 collective-permute-done.16.from_next
  17.1 2.9 %collective-permute-done.17.from_far = bf16[64,528]{1,0:T(8,128)(2,1)S(1)} collective-permute-done((bf16[64,528]{1,0:T(8,128)(2,1)S(1)}, bf16[64,528]{1,0:T(8,128)(2,1)S(1)}, u32[]{:S(2)}, u32[]{:S(2)}) %collective-permute-start.17) | collective-permute-done | bytes 67616 | tf_op jit(solution)/shard_map/ppermute | solution.py:40
  20.0 1.4 shard_map.86
  21.5 42.7 %all-gather.3.cloned.1.call-done = bf16[4224,256]{1,0:T(8,128)(2,1)} async-done(((bf16[528,256]{1,0:T(8,128)(2,1)}), bf16[4224,256]{1,0:T(8,128)(2,1)}) %all-gather.3.cloned.1.call-update) | async-done | bytes 2162704 | tf_op jit(solution)/shard_map/all_gather | solution.py:194
  64.2 1.0 fusion.2
  65.1 0.6 collective-permute-start
  65.7 3.1 %collective-permute-done.came = bf16[2,128,256]{2,1,0:T(8,128)(2,1)S(1)} collective-permute-done((bf16[2,128,256]{2,1,0:T(8,128)(2,1)S(1)}, bf16[2,128,256]{2,1,0:T(8,128)(2,1)S(1)}, u32[]{:S(2)}, u32[]{:S(2)}) %collective-permute-start) | collective-permute-done | bytes 131104 | tf_op jit(solution)/shard_map/ppermute | solution.py:172
  68.8 0.9 copy-done.1
  69.7 0.9 copy-done.2
  70.6 0.6 shard_map.84
  71.2 3.1 %collective-permute-start.10 = (bf16[128,512]{1,0:T(8,128)(2,1)S(1)}, bf16[128,512]{1,0:T(8,128)(2,1)S(1)}, u32[]{:S(2)}, u32[]{:S(2)}) collective-permute-start(bf16[128,512]{1,0:T(8,128)(2,1)S(1)} %get-tuple-element.22), channel_id=1, source_target_pairs={{0,16},{8,24},{16,0},{24,8},{1,17},{9,25},{17,1},{25,9},{2,18},{10... | collective-permute-start | bytes 393224 | tf_op jit(solution)/shard_map/ppermute | solution.py:40
  74.3 1.1 collective-permute-start.9
  75.4 0.9 collective-permute-start.8
  76.3 2.1 %collective-permute-start.3 = (bf16[128,512]{1,0:T(8,128)(2,1)S(1)}, bf16[128,512]{1,0:T(8,128)(2,1)S(1)}, u32[]{:S(2)}, u32[]{:S(2)}) collective-permute-start(bf16[128,512]{1,0:T(8,128)(2,1)S(1)} %get-tuple-element.21), channel_id=1, source_target_pairs={{0,4},{2,6},{4,0},{6,2},{1,5},{3,7},{5,1},{7,3},{8,12},{10,14},{12... | collective-permute-start | bytes 393224 | tf_op jit(solution)/shard_map/ppermute | solution.py:40
  78.4 0.8 collective-permute-done.10
  79.2 0.7 collective-permute-start.2
  79.9 1.3 collective-permute-done.9
  81.2 1.5 collective-permute-start.1
  82.7 0.1 pad_maximum_fusion.1.refs_5_
  82.8 0.6 collective-permute-start.12
  83.4 0.5 collective-permute-done.3
  83.9 0.9 collective-permute-start.11
  84.9 1.4 collective-permute-done.2
  86.3 1.3 collective-permute-done.1
  87.7 2.7 %collective-permute-start.5 = (bf16[4,128,512]{2,1,0:T(8,128)(2,1)S(1)}, bf16[4,128,512]{2,1,0:T(8,128)(2,1)S(1)}, u32[]{:S(2)}, u32[]{:S(2)}) collective-permute-start(bf16[4,128,512]{2,1,0:T(8,128)(2,1)S(1)} %pad_maximum_fusion.refs_0_), channel_id=1, source_target_pairs={{0,24},{8,0},{16,8},{24,16},{1,25},{9,1},{17,9},{25,17},{2,26},{10... | collective-permute-start | bytes 1572872 | tf_op jit(solution)/shard_map/ppermute | solution.py:40
  90.4 6.2 %collective-permute-done.12.refs_7_ = bf16[4,128,512]{2,1,0:T(8,128)(2,1)S(1)} collective-permute-done((bf16[4,128,512]{2,1,0:T(8,128)(2,1)S(1)}, bf16[4,128,512]{2,1,0:T(8,128)(2,1)S(1)}, u32[]{:S(2)}, u32[]{:S(2)}) %collective-permute-start.12) | collective-permute-done | bytes 524320 | tf_op jit(solution)/shard_map/ppermute | solution.py:40
  96.6 0.7 collective-permute-start.14
  97.3 0.1 collective-permute-done.11.refs_6_
  97.4 1.7 collective-permute-start.13
  99.1 0.9 collective-permute-done.5.refs_2_
  100.0 3.8 %collective-permute-start.7 = (bf16[2,128,512]{2,1,0:T(8,128)(2,1)S(1)}, bf16[2,128,512]{2,1,0:T(8,128)(2,1)S(1)}, u32[]{:S(2)}, u32[]{:S(2)}) collective-permute-start(bf16[2,128,512]{2,1,0:T(8,128)(2,1)S(1)} %slice.35), channel_id=1, source_target_pairs={{0,24},{8,0},{16,8},{24,16},{1,25},{9,1},{17,9},{25,17},{2,26},{10... | collective-permute-start | bytes 786440 | tf_op jit(solution)/shard_map/ppermute | solution.py:40
  103.8 0.1 collective-permute-start.6
  103.9 1.1 collective-permute-done.13.refs_8_
  105.1 2.6 %collective-permute-done.7.refs_4_ = bf16[2,128,512]{2,1,0:T(8,128)(2,1)S(1)} collective-permute-done((bf16[2,128,512]{2,1,0:T(8,128)(2,1)S(1)}, bf16[2,128,512]{2,1,0:T(8,128)(2,1)S(1)}, u32[]{:S(2)}, u32[]{:S(2)}) %collective-permute-start.7) | collective-permute-done | bytes 262176 | tf_op jit(solution)/shard_map/ppermute | solution.py:40
  107.6 3.8 %collective-permute-done.6.refs_3_ = bf16[2,128,512]{2,1,0:T(8,128)(2,1)S(1)} collective-permute-done((bf16[2,128,512]{2,1,0:T(8,128)(2,1)S(1)}, bf16[2,128,512]{2,1,0:T(8,128)(2,1)S(1)}, u32[]{:S(2)}, u32[]{:S(2)}) %collective-permute-start.6) | collective-permute-done | bytes 262176 | tf_op jit(solution)/shard_map/ppermute | solution.py:40
  111.5 4.4 %shard_map.87 = (bf16[528,512]{1,0:T(8,128)(2,1)S(1)}, bf16[8,528,256]{2,1,0:T(8,128)(2,1)S(1)}) custom-call(s32[3]{0:T(128)S(1)} %pad_add_fusion.place, bf16[4,128,512]{2,1,0:T(8,128)(2,1)S(1)} %pad_maximum_fusion.refs_0_, bf16[4,128,512]{2,1,0:T(8,128)(2,1)S(1)} %collective-permute-done.4.refs_1_, bf16[4,128,512]{2,1,0:T(8,128)(2,1)S(1)} %collective-permute-done.5.refs_2_, ...), custom_call_target="tpu_custom_call" | custom-call | tf_op jit(solution)/shard_map/pallas_call | solution.py:29
  115.8 0.1 collective-permute-start.20
  115.9 3.3 %shard_map.88 = (bf16[528,512]{1,0:T(8,128)(2,1)S(1)}, bf16[8,528,256]{2,1,0:T(8,128)(2,1)S(1)}) custom-call(s32[3]{0:T(128)S(1)} %pad_add_fusion.place, bf16[4,128,512]{2,1,0:T(8,128)(2,1)S(1)} %pad_maximum_fusion.refs_0_, bf16[4,128,512]{2,1,0:T(8,128)(2,1)S(1)} %collective-permute-done.4.refs_1_, bf16[4,128,512]{2,1,0:T(8,128)(2,1)S(1)} %collective-permute-done.5.refs_2_, ...), custom_call_target="tpu_custom_call" | custom-call | tf_op jit(solution)/shard_map/pallas_call | solution.py:29
  119.3 0.9 collective-permute-done.20
  120.2 2.0 %add_convert_fusion = bf16[8,528,256]{2,1,0:T(8,128)(2,1)} fusion(bf16[8,528,256]{2,1,0:T(8,128)(2,1)S(1)} %collective-permute-done.20, bf16[8,528,256]{2,1,0:T(8,128)(2,1)S(1)} %get-tuple-element.29), kind=kLoop, calls=%fused_computation | loop fusion | flops 4325376 | bytes 6488064 | tf_op jit(solution)/shard_map/convert_element_type | solution.py:231
  122.2 3.6 %shard_map.89 = bf16[16,128,512]{2,1,0:T(8,128)(2,1)S(1)} custom-call(s32[3]{0:T(128)S(1)} %pad_add_fusion.place, bf16[528,512]{1,0:T(8,128)(2,1)S(1)} %get-tuple-element.27.hid_a, bf16[528,512]{1,0:T(8,128)(2,1)S(1)} %get-tuple-element.28.hid_b, bf16[8,528,256]{2,1,0:T(8,128)(2,1)} %collective-permute-done.18.refs_10_.weights_a, ...), custom_call_target="tpu_custom_call" | custom-call | tf_op jit(solution)/shard_map/pallas_call | solution.py:29
  125.8 31.9 %all_to_all.5 = bf16[16,128,512]{2,1,0:T(8,128)(2,1)S(1)} all-to-all(bf16[16,128,512]{2,1,0:T(8,128)(2,1)S(1)} %shard_map.89), channel_id=1, replica_groups=mesh['z'=8,'y'=4,'x'=4,'core'=2] {'y','x'}, dimensions={0} | all-to-all | bytes 4194304 | tf_op jit(solution)/shard_map/all_to_all | solution.py:247
  157.7 0.3 reduce_sum.12
  158.0 0.1 collective-permute-start.19
  158.1 1.2 collective-permute-done.19
  159.4 2.0 %reduce-scatter.2.cloned.1.call-done = bf16[1,528,256]{2,1,0:T(8,128)(2,1)} async-done(((bf16[8,528,256]{2,1,0:T(8,128)(2,1)}), bf16[1,528,256]{2,1,0:T(8,128)(2,1)}) %reduce-scatter.2.cloned.1.call-update) | async-done | bytes 270352 | tf_op jit(solution)/shard_map/reduce_scatter | solution.py:233
  161.3 1.0 copy-done.3
  162.3 0.7 shard_map.90
  163.0 1.5 collective-permute-start.21
  164.5 1.8 collective-permute-start.22
  166.3 1.8 collective-permute-start.23
  168.1 0.7 pad_maximum_fusion.3
  168.8 0.8 collective-permute-done.21.from_prev
  169.6 2.6 %collective-permute-done.23.from_far = bf16[64,528]{1,0:T(8,128)(2,1)S(1)} collective-permute-done((bf16[64,528]{1,0:T(8,128)(2,1)S(1)}, bf16[64,528]{1,0:T(8,128)(2,1)S(1)}, u32[]{:S(2)}, u32[]{:S(2)}) %collective-permute-start.23) | collective-permute-done | bytes 67616 | tf_op jit(solution)/shard_map/ppermute | solution.py:40
  172.3 1.5 shard_map.91
  (26 shorter events, 0.4 us)
Async XLA Ops:
  7.2 57.0 %all-gather.3.cloned.1.call-start = ((), (), s32[]{:S(2)}) async-start(), calls=%async_computation.3 | async-start | bytes 2433024 | tf_op jit(solution)/shard_map/all_gather | solution.py:194
  7.3 0.9 copy-start.4
  8.2 0.9 copy-start.5
  9.1 0.9 copy-start.6
  10.7 5.7 %collective-permute-start.15 = (bf16[64,528]{1,0:T(8,128)(2,1)S(1)}, bf16[64,528]{1,0:T(8,128)(2,1)S(1)}, u32[]{:S(2)}, u32[]{:S(2)}) collective-permute-start(bf16[64,528]{1,0:T(8,128)(2,1)S(1)} %get-tuple-element.24), channel_id=1, source_target_pairs={{0,8},{8,16},{16,24},{24,0},{1,9},{9,17},{17,25},{25,1},{2,10},{10... | collective-permute-start | bytes 202760 | tf_op jit(solution)/shard_map/ppermute | solution.py:40
  12.4 4.7 %collective-permute-start.16 = (bf16[64,528]{1,0:T(8,128)(2,1)S(1)}, bf16[64,528]{1,0:T(8,128)(2,1)S(1)}, u32[]{:S(2)}, u32[]{:S(2)}) collective-permute-start(bf16[64,528]{1,0:T(8,128)(2,1)S(1)} %get-tuple-element.25), channel_id=1, source_target_pairs={{0,24},{8,0},{16,8},{24,16},{1,25},{9,1},{17,9},{25,17},{2,26},{10... | collective-permute-start | bytes 202760 | tf_op jit(solution)/shard_map/ppermute | solution.py:40
  14.0 5.9 %collective-permute-start.17 = (bf16[64,528]{1,0:T(8,128)(2,1)S(1)}, bf16[64,528]{1,0:T(8,128)(2,1)S(1)}, u32[]{:S(2)}, u32[]{:S(2)}) collective-permute-start(bf16[64,528]{1,0:T(8,128)(2,1)S(1)} %get-tuple-element.26), channel_id=1, source_target_pairs={{0,16},{8,24},{16,0},{24,8},{1,17},{9,25},{17,1},{25,9},{2,18},{10... | collective-permute-start | bytes 202760 | tf_op jit(solution)/shard_map/ppermute | solution.py:40
  21.4 139.9 %reduce-scatter.2.cloned.1.call-start = ((), (), s32[]{:S(2)}) async-start(), calls=%async_computation.2 | async-start | bytes 2433024 | tf_op jit(solution)/shard_map/reduce_scatter | solution.py:233
  64.2 47.3 %collective-permute-start.18 = (bf16[8,528,256]{2,1,0:T(8,128)(2,1)}, bf16[8,528,256]{2,1,0:T(8,128)(2,1)}, u32[]{:S(2)}, u32[]{:S(2)}) collective-permute-start(bf16[8,528,256]{2,1,0:T(8,128)(2,1)} %bitcast.19), channel_id=1, source_target_pairs={{0,1},{1,0},{2,3},{3,2},{4,5},{5,4},{6,7},{7,6},{8,9},{9,8},{10,11... | collective-permute-start | bytes 6488072 | tf_op jit(solution)/shard_map/ppermute | solution.py:203
  65.1 3.7 %collective-permute-start = (bf16[2,128,256]{2,1,0:T(8,128)(2,1)S(1)}, bf16[2,128,256]{2,1,0:T(8,128)(2,1)S(1)}, u32[]{:S(2)}, u32[]{:S(2)}) collective-permute-start(bf16[2,128,256]{2,1,0:T(8,128)(2,1)S(1)} %fusion.2), channel_id=1, source_target_pairs={{0,1},{1,0},{2,3},{3,2},{4,5},{5,4},{6,7},{7,6},{8,9},{9,8},{10,11... | collective-permute-start | bytes 393224 | tf_op jit(solution)/shard_map/ppermute | solution.py:172
  68.8 0.9 copy-start.1
  69.7 0.9 copy-start.2
  71.2 8.0 %collective-permute-start.10 = (bf16[128,512]{1,0:T(8,128)(2,1)S(1)}, bf16[128,512]{1,0:T(8,128)(2,1)S(1)}, u32[]{:S(2)}, u32[]{:S(2)}) collective-permute-start(bf16[128,512]{1,0:T(8,128)(2,1)S(1)} %get-tuple-element.22), channel_id=1, source_target_pairs={{0,16},{8,24},{16,0},{24,8},{1,17},{9,25},{17,1},{25,9},{2,18},{10... | collective-permute-start | bytes 393224 | tf_op jit(solution)/shard_map/ppermute | solution.py:40
  74.3 6.9 %collective-permute-start.9 = (bf16[128,512]{1,0:T(8,128)(2,1)S(1)}, bf16[128,512]{1,0:T(8,128)(2,1)S(1)}, u32[]{:S(2)}, u32[]{:S(2)}) collective-permute-start(bf16[128,512]{1,0:T(8,128)(2,1)S(1)} %get-tuple-element.22), channel_id=1, source_target_pairs={{0,24},{8,0},{16,8},{24,16},{1,25},{9,1},{17,9},{25,17},{2,26},{10... | collective-permute-start | bytes 393224 | tf_op jit(solution)/shard_map/ppermute | solution.py:40
  75.4 7.2 %collective-permute-start.8 = (bf16[128,512]{1,0:T(8,128)(2,1)S(1)}, bf16[128,512]{1,0:T(8,128)(2,1)S(1)}, u32[]{:S(2)}, u32[]{:S(2)}) collective-permute-start(bf16[128,512]{1,0:T(8,128)(2,1)S(1)} %get-tuple-element.22), channel_id=1, source_target_pairs={{0,8},{8,16},{16,24},{24,0},{1,9},{9,17},{17,25},{25,1},{2,10},{10... | collective-permute-start | bytes 393224 | tf_op jit(solution)/shard_map/ppermute | solution.py:40
  76.3 7.6 %collective-permute-start.3 = (bf16[128,512]{1,0:T(8,128)(2,1)S(1)}, bf16[128,512]{1,0:T(8,128)(2,1)S(1)}, u32[]{:S(2)}, u32[]{:S(2)}) collective-permute-start(bf16[128,512]{1,0:T(8,128)(2,1)S(1)} %get-tuple-element.21), channel_id=1, source_target_pairs={{0,4},{2,6},{4,0},{6,2},{1,5},{3,7},{5,1},{7,3},{8,12},{10,14},{12... | collective-permute-start | bytes 393224 | tf_op jit(solution)/shard_map/ppermute | solution.py:40
  79.2 7.1 %collective-permute-start.2 = (bf16[128,512]{1,0:T(8,128)(2,1)S(1)}, bf16[128,512]{1,0:T(8,128)(2,1)S(1)}, u32[]{:S(2)}, u32[]{:S(2)}) collective-permute-start(bf16[128,512]{1,0:T(8,128)(2,1)S(1)} %get-tuple-element.21), channel_id=1, source_target_pairs={{0,6},{2,0},{4,2},{6,4},{1,7},{3,1},{5,3},{7,5},{8,14},{10,8},{12,... | collective-permute-start | bytes 393224 | tf_op jit(solution)/shard_map/ppermute | solution.py:40
  81.2 6.4 %collective-permute-start.1 = (bf16[128,512]{1,0:T(8,128)(2,1)S(1)}, bf16[128,512]{1,0:T(8,128)(2,1)S(1)}, u32[]{:S(2)}, u32[]{:S(2)}) collective-permute-start(bf16[128,512]{1,0:T(8,128)(2,1)S(1)} %get-tuple-element.21), channel_id=1, source_target_pairs={{0,2},{2,4},{4,6},{6,0},{1,3},{3,5},{5,7},{7,1},{8,10},{10,12},{12... | collective-permute-start | bytes 393224 | tf_op jit(solution)/shard_map/ppermute | solution.py:40
  82.8 13.8 %collective-permute-start.12 = (bf16[4,128,512]{2,1,0:T(8,128)(2,1)S(1)}, bf16[4,128,512]{2,1,0:T(8,128)(2,1)S(1)}, u32[]{:S(2)}, u32[]{:S(2)}) collective-permute-start(bf16[4,128,512]{2,1,0:T(8,128)(2,1)S(1)} %pad_maximum_fusion.1.refs_5_), channel_id=1, source_target_pairs={{0,6},{2,0},{4,2},{6,4},{1,7},{3,1},{5,3},{7,5},{8,14},{10,8},{12,... | collective-permute-start | bytes 1572872 | tf_op jit(solution)/shard_map/ppermute | solution.py:40
  83.9 13.4 %collective-permute-start.11 = (bf16[4,128,512]{2,1,0:T(8,128)(2,1)S(1)}, bf16[4,128,512]{2,1,0:T(8,128)(2,1)S(1)}, u32[]{:S(2)}, u32[]{:S(2)}) collective-permute-start(bf16[4,128,512]{2,1,0:T(8,128)(2,1)S(1)} %pad_maximum_fusion.1.refs_5_), channel_id=1, source_target_pairs={{0,2},{2,4},{4,6},{6,0},{1,3},{3,5},{5,7},{7,1},{8,10},{10,12},{12... | collective-permute-start | bytes 1572872 | tf_op jit(solution)/shard_map/ppermute | solution.py:40
  87.7 12.3 %collective-permute-start.5 = (bf16[4,128,512]{2,1,0:T(8,128)(2,1)S(1)}, bf16[4,128,512]{2,1,0:T(8,128)(2,1)S(1)}, u32[]{:S(2)}, u32[]{:S(2)}) collective-permute-start(bf16[4,128,512]{2,1,0:T(8,128)(2,1)S(1)} %pad_maximum_fusion.refs_0_), channel_id=1, source_target_pairs={{0,24},{8,0},{16,8},{24,16},{1,25},{9,1},{17,9},{25,17},{2,26},{10... | collective-permute-start | bytes 1572872 | tf_op jit(solution)/shard_map/ppermute | solution.py:40
  90.4 13.4 %collective-permute-start.4 = (bf16[4,128,512]{2,1,0:T(8,128)(2,1)S(1)}, bf16[4,128,512]{2,1,0:T(8,128)(2,1)S(1)}, u32[]{:S(2)}, u32[]{:S(2)}) collective-permute-start(bf16[4,128,512]{2,1,0:T(8,128)(2,1)S(1)} %pad_maximum_fusion.refs_0_), channel_id=1, source_target_pairs={{0,8},{8,16},{16,24},{24,0},{1,9},{9,17},{17,25},{25,1},{2,10},{10... | collective-permute-start | bytes 1572872 | tf_op jit(solution)/shard_map/ppermute | solution.py:40
  96.6 7.3 %collective-permute-start.14 = (bf16[2,128,512]{2,1,0:T(8,128)(2,1)S(1)}, bf16[2,128,512]{2,1,0:T(8,128)(2,1)S(1)}, u32[]{:S(2)}, u32[]{:S(2)}) collective-permute-start(bf16[2,128,512]{2,1,0:T(8,128)(2,1)S(1)} %slice.37), channel_id=1, source_target_pairs={{0,6},{2,0},{4,2},{6,4},{1,7},{3,1},{5,3},{7,5},{8,14},{10,8},{12,... | collective-permute-start | bytes 786440 | tf_op jit(solution)/shard_map/ppermute | solution.py:40
  97.4 7.7 %collective-permute-start.13 = (bf16[2,128,512]{2,1,0:T(8,128)(2,1)S(1)}, bf16[2,128,512]{2,1,0:T(8,128)(2,1)S(1)}, u32[]{:S(2)}, u32[]{:S(2)}) collective-permute-start(bf16[2,128,512]{2,1,0:T(8,128)(2,1)S(1)} %slice.36), channel_id=1, source_target_pairs={{0,2},{2,4},{4,6},{6,0},{1,3},{3,5},{5,7},{7,1},{8,10},{10,12},{12... | collective-permute-start | bytes 786440 | tf_op jit(solution)/shard_map/ppermute | solution.py:40
  100.0 7.7 %collective-permute-start.7 = (bf16[2,128,512]{2,1,0:T(8,128)(2,1)S(1)}, bf16[2,128,512]{2,1,0:T(8,128)(2,1)S(1)}, u32[]{:S(2)}, u32[]{:S(2)}) collective-permute-start(bf16[2,128,512]{2,1,0:T(8,128)(2,1)S(1)} %slice.35), channel_id=1, source_target_pairs={{0,24},{8,0},{16,8},{24,16},{1,25},{9,1},{17,9},{25,17},{2,26},{10... | collective-permute-start | bytes 786440 | tf_op jit(solution)/shard_map/ppermute | solution.py:40
  103.8 12.2 %copy-start = (bf16[4224,256]{1,0:T(8,128)(2,1)S(1)}, bf16[4224,256]{1,0:T(8,128)(2,1)}, u32[]{:S(2)}) copy-start(bf16[4224,256]{1,0:T(8,128)(2,1)} %all-gather.3.cloned.1.call-done) | copy-start | bytes 6488068
  103.8 7.7 %collective-permute-start.6 = (bf16[2,128,512]{2,1,0:T(8,128)(2,1)S(1)}, bf16[2,128,512]{2,1,0:T(8,128)(2,1)S(1)}, u32[]{:S(2)}, u32[]{:S(2)}) collective-permute-start(bf16[2,128,512]{2,1,0:T(8,128)(2,1)S(1)} %slice.34), channel_id=1, source_target_pairs={{0,8},{8,16},{16,24},{24,0},{1,9},{9,17},{17,25},{25,1},{2,10},{10... | collective-permute-start | bytes 786440 | tf_op jit(solution)/shard_map/ppermute | solution.py:40
  115.8 4.3 %collective-permute-start.20 = (bf16[8,528,256]{2,1,0:T(8,128)(2,1)S(1)}, bf16[8,528,256]{2,1,0:T(8,128)(2,1)S(1)}, u32[]{:S(2)}, u32[]{:S(2)}) collective-permute-start(bf16[8,528,256]{2,1,0:T(8,128)(2,1)S(1)} %get-tuple-element.30), channel_id=1, source_target_pairs={{0,1},{1,0},{2,3},{3,2},{4,5},{5,4},{6,7},{7,6},{8,9},{9,8},{10,11... | collective-permute-start | bytes 6488072 | tf_op jit(solution)/shard_map/ppermute | solution.py:218
  158.0 1.3 collective-permute-start.19
  161.3 1.0 copy-start.3
  163.0 6.6 %collective-permute-start.21 = (bf16[64,528]{1,0:T(8,128)(2,1)S(1)}, bf16[64,528]{1,0:T(8,128)(2,1)S(1)}, u32[]{:S(2)}, u32[]{:S(2)}) collective-permute-start(bf16[64,528]{1,0:T(8,128)(2,1)S(1)} %get-tuple-element.32), channel_id=1, source_target_pairs={{0,8},{8,16},{16,24},{24,0},{1,9},{9,17},{17,25},{25,1},{2,10},{10... | collective-permute-start | bytes 202760 | tf_op jit(solution)/shard_map/ppermute | solution.py:40
  164.5 5.1 %collective-permute-start.22 = (bf16[64,528]{1,0:T(8,128)(2,1)S(1)}, bf16[64,528]{1,0:T(8,128)(2,1)S(1)}, u32[]{:S(2)}, u32[]{:S(2)}) collective-permute-start(bf16[64,528]{1,0:T(8,128)(2,1)S(1)} %get-tuple-element.33), channel_id=1, source_target_pairs={{0,24},{8,0},{16,8},{24,16},{1,25},{9,1},{17,9},{25,17},{2,26},{10... | collective-permute-start | bytes 202760 | tf_op jit(solution)/shard_map/ppermute | solution.py:40
  166.3 5.9 %collective-permute-start.23 = (bf16[64,528]{1,0:T(8,128)(2,1)S(1)}, bf16[64,528]{1,0:T(8,128)(2,1)S(1)}, u32[]{:S(2)}, u32[]{:S(2)}) collective-permute-start(bf16[64,528]{1,0:T(8,128)(2,1)S(1)} %get-tuple-element.34), channel_id=1, source_target_pairs={{0,16},{8,24},{16,0},{24,8},{1,17},{9,25},{17,1},{25,9},{2,18},{10... | collective-permute-start | bytes 202760 | tf_op jit(solution)/shard_map/ppermute | solution.py:40
Sparse Core Ops, SparseCore 0:
  21.5 42.5 all-gather.2
  122.3 38.9 reduce-scatter.1

commit v5 on v4

--- a/solution.py
+++ b/solution.py
@@ -16,6 +16,7 @@
 SWAP = [(0, 1), (1, 0)]
 ORDER = (0, -1, 1, 2)
 VMEM = pl.BlockSpec(memory_space=pltpu.VMEM)
+ANY = pl.BlockSpec(memory_space=pl.ANY)
 SMEM = pl.BlockSpec(memory_space=pltpu.SMEM)
 
 
@@ -163,6 +164,12 @@
             out[y * NX + z // 2, :, lanes] = total[slot * HALF : (slot + 1) * HALF]
 
 
+def fetch_kernel(held, out, sem):
+    copy = pltpu.make_async_copy(held, out, sem)
+    copy.start()
+    copy.wait()
+
+
 def per_device(inputs, cotangent, gate_weight, up_weight, down_weight):
     core = lax.axis_index("core")
     place = jnp.stack([lax.axis_index("y"), lax.axis_index("x"), core]).astype(jnp.int32)
@@ -200,6 +207,14 @@
     inp_blocks = around_in_halves(jnp.stack(inp_near), "y")
     cot_blocks = around_in_halves(jnp.stack(cot_near), "x")
 
+    w_own = pl.pallas_call(
+        fetch_kernel,
+        out_shape=jax.ShapeDtypeStruct((NZ, COLS, 256), jnp.bfloat16),
+        in_specs=[ANY],
+        out_specs=VMEM,
+        scratch_shapes=[pltpu.SemaphoreType.DMA],
+        compiler_params=pltpu.CompilerParams(vmem_limit_bytes=24 * 1024 * 1024),
+    )(w_own)
     w_other = lax.ppermute(w_own, "core", SWAP)
 
     def block(weights):

time: 181 us -> 181 us (level)
  no operation moved by 1% of the time
where the time goes in v5:
time: 181 us
  waiting for transfers between devices  78.1 us (43%)
  blocking collectives  31.9 us (18%)
  starting transfers between devices  30.8 us (17%)
  Pallas kernels  16.4 us (9%)
  between operations  14.2 us (8%)
  local copies, waits for them, and re-layouts  5.93 us (3%)
  other arithmetic  3.21 us (2%)
    all_gather x1, waiting for transfers between devices, per_device(): w_own = lax.all_gather(rows, 'z', axis=0, tiled=False)  42.7 us
    all_to_all x1, blocking collectives, per_device(): lax.all_to_all(partial, ('y', 'x'), split_axis=0, concat_axis=0, tiled=True)  31.9 us
    ppermute x20, starting transfers between devices, shift(): lax.ppermute(array, axis, [(i, (i + by) % RING) for i in range(RING)])  30.3 us
    ppermute x20, waiting for transfers between devices, shift(): lax.ppermute(array, axis, [(i, (i + by) % RING) for i in range(RING)])  27.5 us
    pallas_call x8, Pallas kernels, call(): pl.pallas_call(kernel, out_shape=[jax.ShapeDtypeStruct(s, dtype) for s in...  16.2 us
    unnamed x14, local copies, waits for them, and re-layouts  5.86 us
    ppermute x1, waiting for transfers between devices, per_device(): came = lax.ppermute(sent, 'core', SWAP)  3.68 us
  transfers between devices with their start and end apart: 26, of which 22 were waited for; matrix products, arithmetic and copies ran while one was open for 1% of the time, Pallas kernels for 4%

profile of v5, /device:TPU:2, one launch (start us, length us, event | category | flops | bytes accessed | tf_op | source)
XLA Modules:
  0.0 180.5 jit_solution(1156971432601143967)
XLA Ops:
  7.2 0.1 pad_add_fusion.place
  7.3 0.9 copy-done.4
  8.2 0.9 copy-done.5
  9.1 0.9 copy-done.6
  10.0 0.7 shard_map.85
  10.7 1.7 collective-permute-start.15
  12.4 1.7 collective-permute-start.16
  14.0 2.0 %collective-permute-start.17 = (bf16[64,528]{1,0:T(8,128)(2,1)S(1)}, bf16[64,528]{1,0:T(8,128)(2,1)S(1)}, u32[]{:S(2)}, u32[]{:S(2)}) collective-permute-start(bf16[64,528]{1,0:T(8,128)(2,1)S(1)} %get-tuple-element.26), channel_id=1, source_target_pairs={{0,16},{8,24},{16,0},{24,8},{1,17},{9,25},{17,1},{25,9},{2,18},{10... | collective-permute-start | bytes 202760 | tf_op jit(solution)/shard_map/ppermute | solution.py:41
  16.0 0.4 collective-permute-done.15.from_prev
  16.4 0.6 collective-permute-done.16.from_next
  17.1 2.9 %collective-permute-done.17.from_far = bf16[64,528]{1,0:T(8,128)(2,1)S(1)} collective-permute-done((bf16[64,528]{1,0:T(8,128)(2,1)S(1)}, bf16[64,528]{1,0:T(8,128)(2,1)S(1)}, u32[]{:S(2)}, u32[]{:S(2)}) %collective-permute-start.17) | collective-permute-done | bytes 67616 | tf_op jit(solution)/shard_map/ppermute | solution.py:41
  20.0 1.4 shard_map.86
  21.5 42.7 %all-gather.3.cloned.1.call-done = bf16[4224,256]{1,0:T(8,128)(2,1)} async-done(((bf16[528,256]{1,0:T(8,128)(2,1)}), bf16[4224,256]{1,0:T(8,128)(2,1)}) %all-gather.3.cloned.1.call-update) | async-done | bytes 2162704 | tf_op jit(solution)/shard_map/all_gather | solution.py:201
  64.2 1.6 copy-done
  65.8 0.2 shard_map.87.refs_10_.weights_b
  66.0 0.1 collective-permute-start.18
  66.1 0.6 copy-done.1
  66.8 0.1 collective-permute-start
  66.9 3.7 %collective-permute-done.came = bf16[2,128,256]{2,1,0:T(8,128)(2,1)S(1)} collective-permute-done((bf16[2,128,256]{2,1,0:T(8,128)(2,1)S(1)}, bf16[2,128,256]{2,1,0:T(8,128)(2,1)S(1)}, u32[]{:S(2)}, u32[]{:S(2)}) %collective-permute-start) | collective-permute-done | bytes 131104 | tf_op jit(solution)/shard_map/ppermute | solution.py:179
  70.6 0.6 shard_map.84
  71.1 3.1 %collective-permute-start.10 = (bf16[128,512]{1,0:T(8,128)(2,1)S(1)}, bf16[128,512]{1,0:T(8,128)(2,1)S(1)}, u32[]{:S(2)}, u32[]{:S(2)}) collective-permute-start(bf16[128,512]{1,0:T(8,128)(2,1)S(1)} %get-tuple-element.22), channel_id=1, source_target_pairs={{0,16},{8,24},{16,0},{24,8},{1,17},{9,25},{17,1},{25,9},{2,18},{10... | collective-permute-start | bytes 393224 | tf_op jit(solution)/shard_map/ppermute | solution.py:41
  74.2 1.1 collective-permute-start.9
  75.4 0.9 collective-permute-start.8
  76.3 2.1 %collective-permute-start.3 = (bf16[128,512]{1,0:T(8,128)(2,1)S(1)}, bf16[128,512]{1,0:T(8,128)(2,1)S(1)}, u32[]{:S(2)}, u32[]{:S(2)}) collective-permute-start(bf16[128,512]{1,0:T(8,128)(2,1)S(1)} %get-tuple-element.21), channel_id=1, source_target_pairs={{0,4},{2,6},{4,0},{6,2},{1,5},{3,7},{5,1},{7,3},{8,12},{10,14},{12... | collective-permute-start | bytes 393224 | tf_op jit(solution)/shard_map/ppermute | solution.py:41
  78.3 0.8 collective-permute-done.10
  79.1 0.7 collective-permute-start.2
  79.8 1.3 collective-permute-done.9
  81.1 1.5 collective-permute-start.1
  82.7 0.6 collective-permute-start.12
  83.3 0.5 collective-permute-done.3
  83.9 0.9 collective-permute-start.11
  84.8 1.4 collective-permute-done.2
  86.2 1.3 collective-permute-done.1
  87.6 2.7 %collective-permute-start.5 = (bf16[4,128,512]{2,1,0:T(8,128)(2,1)S(1)}, bf16[4,128,512]{2,1,0:T(8,128)(2,1)S(1)}, u32[]{:S(2)}, u32[]{:S(2)}) collective-permute-start(bf16[4,128,512]{2,1,0:T(8,128)(2,1)S(1)} %pad_maximum_fusion.refs_0_), channel_id=1, source_target_pairs={{0,24},{8,0},{16,8},{24,16},{1,25},{9,1},{17,9},{25,17},{2,26},{10... | collective-permute-start | bytes 1572872 | tf_op jit(solution)/shard_map/ppermute | solution.py:41
  90.3 6.2 %collective-permute-done.12.refs_7_ = bf16[4,128,512]{2,1,0:T(8,128)(2,1)S(1)} collective-permute-done((bf16[4,128,512]{2,1,0:T(8,128)(2,1)S(1)}, bf16[4,128,512]{2,1,0:T(8,128)(2,1)S(1)}, u32[]{:S(2)}, u32[]{:S(2)}) %collective-permute-start.12) | collective-permute-done | bytes 524320 | tf_op jit(solution)/shard_map/ppermute | solution.py:41
  96.5 0.7 collective-permute-start.14
  97.2 0.1 collective-permute-done.11.refs_6_
  97.3 1.7 collective-permute-start.13
  99.0 0.9 collective-permute-done.5.refs_2_
  99.9 3.8 %collective-permute-start.7 = (bf16[2,128,512]{2,1,0:T(8,128)(2,1)S(1)}, bf16[2,128,512]{2,1,0:T(8,128)(2,1)S(1)}, u32[]{:S(2)}, u32[]{:S(2)}) collective-permute-start(bf16[2,128,512]{2,1,0:T(8,128)(2,1)S(1)} %slice.35), channel_id=1, source_target_pairs={{0,24},{8,0},{16,8},{24,16},{1,25},{9,1},{17,9},{25,17},{2,26},{10... | collective-permute-start | bytes 786440 | tf_op jit(solution)/shard_map/ppermute | solution.py:41
  103.7 0.1 collective-permute-start.6
  103.9 1.1 collective-permute-done.13.refs_8_
  105.0 2.6 %collective-permute-done.7.refs_4_ = bf16[2,128,512]{2,1,0:T(8,128)(2,1)S(1)} collective-permute-done((bf16[2,128,512]{2,1,0:T(8,128)(2,1)S(1)}, bf16[2,128,512]{2,1,0:T(8,128)(2,1)S(1)}, u32[]{:S(2)}, u32[]{:S(2)}) %collective-permute-start.7) | collective-permute-done | bytes 262176 | tf_op jit(solution)/shard_map/ppermute | solution.py:41
  107.6 3.8 %collective-permute-done.6.refs_3_ = bf16[2,128,512]{2,1,0:T(8,128)(2,1)S(1)} collective-permute-done((bf16[2,128,512]{2,1,0:T(8,128)(2,1)S(1)}, bf16[2,128,512]{2,1,0:T(8,128)(2,1)S(1)}, u32[]{:S(2)}, u32[]{:S(2)}) %collective-permute-start.6) | collective-permute-done | bytes 262176 | tf_op jit(solution)/shard_map/ppermute | solution.py:41
  111.4 4.4 %shard_map.88 = (bf16[528,512]{1,0:T(8,128)(2,1)S(1)}, bf16[8,528,256]{2,1,0:T(8,128)(2,1)S(1)}) custom-call(s32[3]{0:T(128)S(1)} %pad_add_fusion.place, bf16[4,128,512]{2,1,0:T(8,128)(2,1)S(1)} %pad_maximum_fusion.refs_0_, bf16[4,128,512]{2,1,0:T(8,128)(2,1)S(1)} %collective-permute-done.4.refs_1_, bf16[4,128,512]{2,1,0:T(8,128)(2,1)S(1)} %collective-permute-done.5.refs_2_, ...), custom_call_target="tpu_custom_call" | custom-call | tf_op jit(solution)/shard_map/pallas_call | solution.py:30
  115.8 0.1 collective-permute-start.20
  115.9 3.3 %shard_map.89 = (bf16[528,512]{1,0:T(8,128)(2,1)S(1)}, bf16[8,528,256]{2,1,0:T(8,128)(2,1)S(1)}) custom-call(s32[3]{0:T(128)S(1)} %pad_add_fusion.place, bf16[4,128,512]{2,1,0:T(8,128)(2,1)S(1)} %pad_maximum_fusion.refs_0_, bf16[4,128,512]{2,1,0:T(8,128)(2,1)S(1)} %collective-permute-done.4.refs_1_, bf16[4,128,512]{2,1,0:T(8,128)(2,1)S(1)} %collective-permute-done.5.refs_2_, ...), custom_call_target="tpu_custom_call" | custom-call | tf_op jit(solution)/shard_map/pallas_call | solution.py:30
  119.2 0.9 collective-permute-done.20
  120.1 2.0 %add_convert_fusion = bf16[8,528,256]{2,1,0:T(8,128)(2,1)} fusion(bf16[8,528,256]{2,1,0:T(8,128)(2,1)S(1)} %collective-permute-done.20, bf16[8,528,256]{2,1,0:T(8,128)(2,1)S(1)} %get-tuple-element.29), kind=kLoop, calls=%fused_computation | loop fusion | flops 4325376 | bytes 6488064 | tf_op jit(solution)/shard_map/convert_element_type | solution.py:246
  122.1 3.6 %shard_map.90 = bf16[16,128,512]{2,1,0:T(8,128)(2,1)S(1)} custom-call(s32[3]{0:T(128)S(1)} %pad_add_fusion.place, bf16[528,512]{1,0:T(8,128)(2,1)S(1)} %get-tuple-element.27.hid_a, bf16[528,512]{1,0:T(8,128)(2,1)S(1)} %get-tuple-element.28.hid_b, bf16[8,528,256]{2,1,0:T(8,128)(2,1)} %collective-permute-done.18.refs_10_.weights_a, ...), custom_call_target="tpu_custom_call" | custom-call | tf_op jit(solution)/shard_map/pallas_call | solution.py:30
  125.7 31.9 %all_to_all.5 = bf16[16,128,512]{2,1,0:T(8,128)(2,1)S(1)} all-to-all(bf16[16,128,512]{2,1,0:T(8,128)(2,1)S(1)} %shard_map.90), channel_id=1, replica_groups=mesh['z'=8,'y'=4,'x'=4,'core'=2] {'y','x'}, dimensions={0} | all-to-all | bytes 4194304 | tf_op jit(solution)/shard_map/all_to_all | solution.py:262
  157.6 0.3 reduce_sum.12
  157.9 0.1 collective-permute-start.19
  158.0 1.2 collective-permute-done.19
  159.3 2.0 %reduce-scatter.2.cloned.1.call-done = bf16[1,528,256]{2,1,0:T(8,128)(2,1)} async-done(((bf16[8,528,256]{2,1,0:T(8,128)(2,1)}), bf16[1,528,256]{2,1,0:T(8,128)(2,1)}) %reduce-scatter.2.cloned.1.call-update) | async-done | bytes 270352 | tf_op jit(solution)/shard_map/reduce_scatter | solution.py:248
  161.3 1.0 copy-done.3
  162.2 0.7 shard_map.91
  162.9 1.5 collective-permute-start.21
  164.5 1.8 collective-permute-start.22
  166.2 1.8 %collective-permute-start.23 = (bf16[64,528]{1,0:T(8,128)(2,1)S(1)}, bf16[64,528]{1,0:T(8,128)(2,1)S(1)}, u32[]{:S(2)}, u32[]{:S(2)}) collective-permute-start(bf16[64,528]{1,0:T(8,128)(2,1)S(1)} %get-tuple-element.34), channel_id=1, source_target_pairs={{0,16},{8,24},{16,0},{24,8},{1,17},{9,25},{17,1},{25,9},{2,18},{10... | collective-permute-start | bytes 202760 | tf_op jit(solution)/shard_map/ppermute | solution.py:41
  168.1 0.7 pad_maximum_fusion.3
  168.7 0.8 collective-permute-done.21.from_prev
  169.5 2.6 %collective-permute-done.23.from_far = bf16[64,528]{1,0:T(8,128)(2,1)S(1)} collective-permute-done((bf16[64,528]{1,0:T(8,128)(2,1)S(1)}, bf16[64,528]{1,0:T(8,128)(2,1)S(1)}, u32[]{:S(2)}, u32[]{:S(2)}) %collective-permute-start.23) | collective-permute-done | bytes 67616 | tf_op jit(solution)/shard_map/ppermute | solution.py:41
  172.2 1.5 shard_map.92
  (27 shorter events, 0.5 us)
Async XLA Ops:
  7.2 57.0 %all-gather.3.cloned.1.call-start = ((), (), s32[]{:S(2)}) async-start(), calls=%async_computation.3 | async-start | bytes 2433024 | tf_op jit(solution)/shard_map/all_gather | solution.py:201
  7.3 0.9 copy-start.4
  8.2 0.9 copy-start.5
  9.1 0.9 copy-start.6
  10.7 5.7 %collective-permute-start.15 = (bf16[64,528]{1,0:T(8,128)(2,1)S(1)}, bf16[64,528]{1,0:T(8,128)(2,1)S(1)}, u32[]{:S(2)}, u32[]{:S(2)}) collective-permute-start(bf16[64,528]{1,0:T(8,128)(2,1)S(1)} %get-tuple-element.24), channel_id=1, source_target_pairs={{0,8},{8,16},{16,24},{24,0},{1,9},{9,17},{17,25},{25,1},{2,10},{10... | collective-permute-start | bytes 202760 | tf_op jit(solution)/shard_map/ppermute | solution.py:41
  12.4 4.7 %collective-permute-start.16 = (bf16[64,528]{1,0:T(8,128)(2,1)S(1)}, bf16[64,528]{1,0:T(8,128)(2,1)S(1)}, u32[]{:S(2)}, u32[]{:S(2)}) collective-permute-start(bf16[64,528]{1,0:T(8,128)(2,1)S(1)} %get-tuple-element.25), channel_id=1, source_target_pairs={{0,24},{8,0},{16,8},{24,16},{1,25},{9,1},{17,9},{25,17},{2,26},{10... | collective-permute-start | bytes 202760 | tf_op jit(solution)/shard_map/ppermute | solution.py:41
  14.0 5.9 %collective-permute-start.17 = (bf16[64,528]{1,0:T(8,128)(2,1)S(1)}, bf16[64,528]{1,0:T(8,128)(2,1)S(1)}, u32[]{:S(2)}, u32[]{:S(2)}) collective-permute-start(bf16[64,528]{1,0:T(8,128)(2,1)S(1)} %get-tuple-element.26), channel_id=1, source_target_pairs={{0,16},{8,24},{16,0},{24,8},{1,17},{9,25},{17,1},{25,9},{2,18},{10... | collective-permute-start | bytes 202760 | tf_op jit(solution)/shard_map/ppermute | solution.py:41
  21.4 139.9 %reduce-scatter.2.cloned.1.call-start = ((), (), s32[]{:S(2)}) async-start(), calls=%async_computation.2 | async-start | bytes 2433024 | tf_op jit(solution)/shard_map/reduce_scatter | solution.py:248
  64.2 1.6 copy-start
  65.8 0.9 copy-start.1
  65.8 1.0 copy-start.2
  66.0 45.3 %collective-permute-start.18 = (bf16[8,528,256]{2,1,0:T(8,128)(2,1)S(1)}, bf16[8,528,256]{2,1,0:T(8,128)(2,1)}, u32[]{:S(2)}, u32[]{:S(2)}) collective-permute-start(bf16[8,528,256]{2,1,0:T(8,128)(2,1)S(1)} %shard_map.87.refs_10_.weights_b), channel_id=1, source_target_pairs={{0,1},{1,0},{2,3},{3,2},{4,5},{5,4},{6,7},{7,6},{8,9},{9,8},{10,11... | collective-permute-start | bytes 6488072 | tf_op jit(solution)/shard_map/ppermute | solution.py:218
  66.8 3.8 %collective-permute-start = (bf16[2,128,256]{2,1,0:T(8,128)(2,1)S(1)}, bf16[2,128,256]{2,1,0:T(8,128)(2,1)S(1)}, u32[]{:S(2)}, u32[]{:S(2)}) collective-permute-start(bf16[2,128,256]{2,1,0:T(8,128)(2,1)S(1)} %fusion.2), channel_id=1, source_target_pairs={{0,1},{1,0},{2,3},{3,2},{4,5},{5,4},{6,7},{7,6},{8,9},{9,8},{10,11... | collective-permute-start | bytes 393224 | tf_op jit(solution)/shard_map/ppermute | solution.py:179
  71.1 8.0 %collective-permute-start.10 = (bf16[128,512]{1,0:T(8,128)(2,1)S(1)}, bf16[128,512]{1,0:T(8,128)(2,1)S(1)}, u32[]{:S(2)}, u32[]{:S(2)}) collective-permute-start(bf16[128,512]{1,0:T(8,128)(2,1)S(1)} %get-tuple-element.22), channel_id=1, source_target_pairs={{0,16},{8,24},{16,0},{24,8},{1,17},{9,25},{17,1},{25,9},{2,18},{10... | collective-permute-start | bytes 393224 | tf_op jit(solution)/shard_map/ppermute | solution.py:41
  74.2 6.9 %collective-permute-start.9 = (bf16[128,512]{1,0:T(8,128)(2,1)S(1)}, bf16[128,512]{1,0:T(8,128)(2,1)S(1)}, u32[]{:S(2)}, u32[]{:S(2)}) collective-permute-start(bf16[128,512]{1,0:T(8,128)(2,1)S(1)} %get-tuple-element.22), channel_id=1, source_target_pairs={{0,24},{8,0},{16,8},{24,16},{1,25},{9,1},{17,9},{25,17},{2,26},{10... | collective-permute-start | bytes 393224 | tf_op jit(solution)/shard_map/ppermute | solution.py:41
  75.4 7.2 %collective-permute-start.8 = (bf16[128,512]{1,0:T(8,128)(2,1)S(1)}, bf16[128,512]{1,0:T(8,128)(2,1)S(1)}, u32[]{:S(2)}, u32[]{:S(2)}) collective-permute-start(bf16[128,512]{1,0:T(8,128)(2,1)S(1)} %get-tuple-element.22), channel_id=1, source_target_pairs={{0,8},{8,16},{16,24},{24,0},{1,9},{9,17},{17,25},{25,1},{2,10},{10... | collective-permute-start | bytes 393224 | tf_op jit(solution)/shard_map/ppermute | solution.py:41
  76.3 7.6 %collective-permute-start.3 = (bf16[128,512]{1,0:T(8,128)(2,1)S(1)}, bf16[128,512]{1,0:T(8,128)(2,1)S(1)}, u32[]{:S(2)}, u32[]{:S(2)}) collective-permute-start(bf16[128,512]{1,0:T(8,128)(2,1)S(1)} %get-tuple-element.21), channel_id=1, source_target_pairs={{0,4},{2,6},{4,0},{6,2},{1,5},{3,7},{5,1},{7,3},{8,12},{10,14},{12... | collective-permute-start | bytes 393224 | tf_op jit(solution)/shard_map/ppermute | solution.py:41
  79.1 7.1 %collective-permute-start.2 = (bf16[128,512]{1,0:T(8,128)(2,1)S(1)}, bf16[128,512]{1,0:T(8,128)(2,1)S(1)}, u32[]{:S(2)}, u32[]{:S(2)}) collective-permute-start(bf16[128,512]{1,0:T(8,128)(2,1)S(1)} %get-tuple-element.21), channel_id=1, source_target_pairs={{0,6},{2,0},{4,2},{6,4},{1,7},{3,1},{5,3},{7,5},{8,14},{10,8},{12,... | collective-permute-start | bytes 393224 | tf_op jit(solution)/shard_map/ppermute | solution.py:41
  81.1 6.4 %collective-permute-start.1 = (bf16[128,512]{1,0:T(8,128)(2,1)S(1)}, bf16[128,512]{1,0:T(8,128)(2,1)S(1)}, u32[]{:S(2)}, u32[]{:S(2)}) collective-permute-start(bf16[128,512]{1,0:T(8,128)(2,1)S(1)} %get-tuple-element.21), channel_id=1, source_target_pairs={{0,2},{2,4},{4,6},{6,0},{1,3},{3,5},{5,7},{7,1},{8,10},{10,12},{12... | collective-permute-start | bytes 393224 | tf_op jit(solution)/shard_map/ppermute | solution.py:41
  82.7 13.8 %collective-permute-start.12 = (bf16[4,128,512]{2,1,0:T(8,128)(2,1)S(1)}, bf16[4,128,512]{2,1,0:T(8,128)(2,1)S(1)}, u32[]{:S(2)}, u32[]{:S(2)}) collective-permute-start(bf16[4,128,512]{2,1,0:T(8,128)(2,1)S(1)} %pad_maximum_fusion.1.refs_5_), channel_id=1, source_target_pairs={{0,6},{2,0},{4,2},{6,4},{1,7},{3,1},{5,3},{7,5},{8,14},{10,8},{12,... | collective-permute-start | bytes 1572872 | tf_op jit(solution)/shard_map/ppermute | solution.py:41
  83.9 13.4 %collective-permute-start.11 = (bf16[4,128,512]{2,1,0:T(8,128)(2,1)S(1)}, bf16[4,128,512]{2,1,0:T(8,128)(2,1)S(1)}, u32[]{:S(2)}, u32[]{:S(2)}) collective-permute-start(bf16[4,128,512]{2,1,0:T(8,128)(2,1)S(1)} %pad_maximum_fusion.1.refs_5_), channel_id=1, source_target_pairs={{0,2},{2,4},{4,6},{6,0},{1,3},{3,5},{5,7},{7,1},{8,10},{10,12},{12... | collective-permute-start | bytes 1572872 | tf_op jit(solution)/shard_map/ppermute | solution.py:41
  87.6 12.3 %collective-permute-start.5 = (bf16[4,128,512]{2,1,0:T(8,128)(2,1)S(1)}, bf16[4,128,512]{2,1,0:T(8,128)(2,1)S(1)}, u32[]{:S(2)}, u32[]{:S(2)}) collective-permute-start(bf16[4,128,512]{2,1,0:T(8,128)(2,1)S(1)} %pad_maximum_fusion.refs_0_), channel_id=1, source_target_pairs={{0,24},{8,0},{16,8},{24,16},{1,25},{9,1},{17,9},{25,17},{2,26},{10... | collective-permute-start | bytes 1572872 | tf_op jit(solution)/shard_map/ppermute | solution.py:41
  90.3 13.4 %collective-permute-start.4 = (bf16[4,128,512]{2,1,0:T(8,128)(2,1)S(1)}, bf16[4,128,512]{2,1,0:T(8,128)(2,1)S(1)}, u32[]{:S(2)}, u32[]{:S(2)}) collective-permute-start(bf16[4,128,512]{2,1,0:T(8,128)(2,1)S(1)} %pad_maximum_fusion.refs_0_), channel_id=1, source_target_pairs={{0,8},{8,16},{16,24},{24,0},{1,9},{9,17},{17,25},{25,1},{2,10},{10... | collective-permute-start | bytes 1572872 | tf_op jit(solution)/shard_map/ppermute | solution.py:41
  96.5 7.3 %collective-permute-start.14 = (bf16[2,128,512]{2,1,0:T(8,128)(2,1)S(1)}, bf16[2,128,512]{2,1,0:T(8,128)(2,1)S(1)}, u32[]{:S(2)}, u32[]{:S(2)}) collective-permute-start(bf16[2,128,512]{2,1,0:T(8,128)(2,1)S(1)} %slice.37), channel_id=1, source_target_pairs={{0,6},{2,0},{4,2},{6,4},{1,7},{3,1},{5,3},{7,5},{8,14},{10,8},{12,... | collective-permute-start | bytes 786440 | tf_op jit(solution)/shard_map/ppermute | solution.py:41
  97.3 7.7 %collective-permute-start.13 = (bf16[2,128,512]{2,1,0:T(8,128)(2,1)S(1)}, bf16[2,128,512]{2,1,0:T(8,128)(2,1)S(1)}, u32[]{:S(2)}, u32[]{:S(2)}) collective-permute-start(bf16[2,128,512]{2,1,0:T(8,128)(2,1)S(1)} %slice.36), channel_id=1, source_target_pairs={{0,2},{2,4},{4,6},{6,0},{1,3},{3,5},{5,7},{7,1},{8,10},{10,12},{12... | collective-permute-start | bytes 786440 | tf_op jit(solution)/shard_map/ppermute | solution.py:41
  99.9 7.7 %collective-permute-start.7 = (bf16[2,128,512]{2,1,0:T(8,128)(2,1)S(1)}, bf16[2,128,512]{2,1,0:T(8,128)(2,1)S(1)}, u32[]{:S(2)}, u32[]{:S(2)}) collective-permute-start(bf16[2,128,512]{2,1,0:T(8,128)(2,1)S(1)} %slice.35), channel_id=1, source_target_pairs={{0,24},{8,0},{16,8},{24,16},{1,25},{9,1},{17,9},{25,17},{2,26},{10... | collective-permute-start | bytes 786440 | tf_op jit(solution)/shard_map/ppermute | solution.py:41
  103.7 7.7 %collective-permute-start.6 = (bf16[2,128,512]{2,1,0:T(8,128)(2,1)S(1)}, bf16[2,128,512]{2,1,0:T(8,128)(2,1)S(1)}, u32[]{:S(2)}, u32[]{:S(2)}) collective-permute-start(bf16[2,128,512]{2,1,0:T(8,128)(2,1)S(1)} %slice.34), channel_id=1, source_target_pairs={{0,8},{8,16},{16,24},{24,0},{1,9},{9,17},{17,25},{25,1},{2,10},{10... | collective-permute-start | bytes 786440 | tf_op jit(solution)/shard_map/ppermute | solution.py:41
  115.8 4.3 %collective-permute-start.20 = (bf16[8,528,256]{2,1,0:T(8,128)(2,1)S(1)}, bf16[8,528,256]{2,1,0:T(8,128)(2,1)S(1)}, u32[]{:S(2)}, u32[]{:S(2)}) collective-permute-start(bf16[8,528,256]{2,1,0:T(8,128)(2,1)S(1)} %get-tuple-element.30), channel_id=1, source_target_pairs={{0,1},{1,0},{2,3},{3,2},{4,5},{5,4},{6,7},{7,6},{8,9},{9,8},{10,11... | collective-permute-start | bytes 6488072 | tf_op jit(solution)/shard_map/ppermute | solution.py:233
  157.9 1.3 collective-permute-start.19
  161.3 1.0 copy-start.3
  162.9 6.6 %collective-permute-start.21 = (bf16[64,528]{1,0:T(8,128)(2,1)S(1)}, bf16[64,528]{1,0:T(8,128)(2,1)S(1)}, u32[]{:S(2)}, u32[]{:S(2)}) collective-permute-start(bf16[64,528]{1,0:T(8,128)(2,1)S(1)} %get-tuple-element.32), channel_id=1, source_target_pairs={{0,8},{8,16},{16,24},{24,0},{1,9},{9,17},{17,25},{25,1},{2,10},{10... | collective-permute-start | bytes 202760 | tf_op jit(solution)/shard_map/ppermute | solution.py:41
  164.5 5.1 %collective-permute-start.22 = (bf16[64,528]{1,0:T(8,128)(2,1)S(1)}, bf16[64,528]{1,0:T(8,128)(2,1)S(1)}, u32[]{:S(2)}, u32[]{:S(2)}) collective-permute-start(bf16[64,528]{1,0:T(8,128)(2,1)S(1)} %get-tuple-element.33), channel_id=1, source_target_pairs={{0,24},{8,0},{16,8},{24,16},{1,25},{9,1},{17,9},{25,17},{2,26},{10... | collective-permute-start | bytes 202760 | tf_op jit(solution)/shard_map/ppermute | solution.py:41
  166.2 5.9 %collective-permute-start.23 = (bf16[64,528]{1,0:T(8,128)(2,1)S(1)}, bf16[64,528]{1,0:T(8,128)(2,1)S(1)}, u32[]{:S(2)}, u32[]{:S(2)}) collective-permute-start(bf16[64,528]{1,0:T(8,128)(2,1)S(1)} %get-tuple-element.34), channel_id=1, source_target_pairs={{0,16},{8,24},{16,0},{24,8},{1,17},{9,25},{17,1},{25,9},{2,18},{10... | collective-permute-start | bytes 202760 | tf_op jit(solution)/shard_map/ppermute | solution.py:41
Sparse Core Ops, SparseCore 0:
  21.5 42.5 all-gather.2
  122.2 38.9 reduce-scatter.1
